TPU v7x, 512 devices: a whole 4x4x16 slice. The times are simulated.
512 devices in a mesh: sp: 64 (over z, y), tp: 8 (over x, core).
Axes of the slice: x: 4, y: 4, z: 16, core: 2. Of those that a mesh axis runs over, the one named last changes fastest.
Arguments:
- queries: bfloat16 [8192, 1024], P('sp', 'tp'), may hold values from -6 to 6
- attn_out: bfloat16 [8192, 1024], P('sp', 'tp'), may hold values from -6 to 6
- out_grad: bfloat16 [8192, 1024], P('sp', 'tp'), may hold values from -384 to 384
- row_lse: float32 [8192, 8], P('sp', 'tp'), may hold values from 9.5 to 12.5
- source: bfloat16 [32768, 4096], P('sp', 'tp'), may hold values from -6 to 6
- saved_keys: bfloat16 [32768, 256], P('sp'), may hold values from -6 to 6
- saved_values: bfloat16 [32768, 256], P('sp'), may hold values from -6 to 6
- key_weight: bfloat16 [4096, 256], P('tp'), may hold values from -0.09375 to 0.09375
- value_weight: bfloat16 [4096, 256], P('tp'), may hold values from -0.09375 to 0.09375
Outputs:
- query_grad: float32 [8192, 1024], P('sp', 'tp')
- source_grad: float32 [32768, 4096], P('sp', 'tp')
- key_grad: float32 [256, 4096], P('sp', 'tp')
All inputs are finite; a program needn't handle non-finite values.
Results may differ from a plain program's by a relative error of at most 0.012.
Values may be sent and summed in bfloat16 or wider, within the bound.
No kernel may reach another device: no remote copies, remote signals or barrier semaphores. Data moves between devices by JAX's collectives and lax.ppermute only.
A program may use at most 64 MiB of HBM per device.

v0:
```python
import math

import jax
import jax.numpy as jnp
from jax import lax
from jax.sharding import Mesh
from jax.sharding import PartitionSpec as P

HEADS = 8
KV_HEADS = 2
HEAD_DIM = 128
SP = ("sp_0", "sp_1")


def copy_for_each(value, axis):
    size = lax.axis_size(axis)
    return lax.all_to_all(
        jnp.broadcast_to(value[None], (size, *value.shape)), axis, 0, 0, tiled=True
    )


def joined_along(pieces, dim):
    pieces = jnp.moveaxis(pieces, 0, dim)
    lengths = pieces.shape
    return pieces.reshape(*lengths[:dim], lengths[dim] * lengths[dim + 1], *lengths[dim + 2 :])


def gather_directly(value, axis, dim):
    pieces = copy_for_each(value, axis)
    return joined_along(pieces, dim)


def gather_axes(value, axes, dim):
    for axis in reversed(axes):
        value = lax.all_gather(value, axis, axis=dim, tiled=True)
    return value


def together(arrays, axis):
    ends = [0]
    for a in arrays:
        ends.append(ends[-1] + a.size)
    subtotal = lax.psum(jnp.concatenate([a.ravel() for a in arrays]), axis)
    return tuple((subtotal[b:e].reshape(a.shape) for a, b, e in zip(arrays, ends, ends[1:])))


def split_up(value, dim, size):
    before, after = (value.shape[:dim], value.shape[dim + 1 :])
    return jnp.moveaxis(value.reshape(*before, size, -1, *after), dim, 0)


def sum_at_owner(value, axis, dim):
    pieces = split_up(value, dim, lax.axis_size(axis))
    arrived = lax.all_to_all(pieces, axis, split_axis=0, concat_axis=0, tiled=True)
    return arrived.astype(jnp.float32).sum(axis=0)


def contract_rows(left, right):
    return lax.dot_general(
        left, right, (((0,), (0,)), ((), ())), preferred_element_type=jnp.float32
    )


def contract_cols(left, right):
    return lax.dot_general(
        left, right, (((1,), (1,)), ((), ())), preferred_element_type=jnp.float32
    )


def shards(
    queries, attn_out, out_grad, row_lse, source, saved_keys, saved_values, key_weight, value_weight
):
    local_heads = row_lse.shape[1]
    tgt_rows = queries.shape[0]
    width = queries.shape[1]
    src_rows = source.shape[0]
    sp_count = lax.axis_size(SP)
    first_head = lax.axis_index("tp") * local_heads
    per_key = HEADS // KV_HEADS
    score_scale = 1.0 / math.sqrt(HEAD_DIM)
    row_delta = jnp.sum(
        (out_grad.astype(jnp.float32) * attn_out.astype(jnp.float32)).reshape(
            tgt_rows, local_heads, HEAD_DIM
        ),
        axis=2,
    )
    row_blocks = jnp.stack([queries, out_grad])
    row_stats = jnp.stack([row_lse, row_delta])
    whole_stats = gather_directly(row_stats, SP, 1)
    kv_starts = [(first_head + 0) // per_key * HEAD_DIM]
    key_heads = [lax.dynamic_slice_in_dim(saved_keys, start, HEAD_DIM, 1) for start in kv_starts]
    value_heads = [
        lax.dynamic_slice_in_dim(saved_values, start, HEAD_DIM, 1) for start in kv_starts
    ]
    total_rows = tgt_rows * sp_count
    initial = (
        jnp.zeros((total_rows, width), jnp.float32),
        jnp.zeros((src_rows, KV_HEADS * HEAD_DIM), jnp.float32),
        jnp.zeros((src_rows, KV_HEADS * HEAD_DIM), jnp.float32),
    )
    blocks = gather_axes(row_blocks, SP, 1)
    rows = blocks.shape[1]
    span = math.gcd(rows, 1024)
    count = rows // span

    def step(turn, inner):
        query_buf, key_acc, value_acc = inner
        begin = turn * span
        block_rows = lax.dynamic_slice_in_dim(blocks, begin, span, 1)
        block_stats = lax.dynamic_slice_in_dim(whole_stats, begin, span, 1)
        query_head = block_rows[0, :, 0:HEAD_DIM]
        grad_head = block_rows[1, :, 0:HEAD_DIM]
        lse_col = block_stats[0, :, 0:1]
        delta_col = block_stats[1, :, 0:1]
        scores = contract_cols(query_head, key_heads[0]) * score_scale
        attn_probs = jnp.exp(scores - lse_col)
        dprobs = contract_cols(grad_head, value_heads[0])
        dscores = (attn_probs * (dprobs - delta_col) * score_scale).astype(jnp.bfloat16)
        parts = [jnp.dot(dscores, key_heads[0], preferred_element_type=jnp.float32)]
        key_part = contract_rows(dscores, query_head)
        value_part = contract_rows(attn_probs.astype(jnp.bfloat16), grad_head)
        kv_start = kv_starts[0]
        key_acc = lax.dynamic_update_slice_in_dim(
            key_acc,
            lax.dynamic_slice_in_dim(key_acc, kv_start, HEAD_DIM, 1) + key_part,
            kv_start,
            1,
        )
        value_acc = lax.dynamic_update_slice_in_dim(
            value_acc,
            lax.dynamic_slice_in_dim(value_acc, kv_start, HEAD_DIM, 1) + value_part,
            kv_start,
            1,
        )
        query_buf = lax.dynamic_update_slice_in_dim(
            query_buf, jnp.concatenate(parts, axis=1), begin, 0
        )
        return (query_buf, key_acc, value_acc)

    partials, key_acc, value_acc = lax.fori_loop(0, count, step, initial)
    stacked = partials.reshape(sp_count, tgt_rows, width)
    received = lax.all_to_all(
        stacked.astype(jnp.bfloat16), SP, split_axis=0, concat_axis=0, tiled=True
    ).astype(stacked.dtype)
    query_grad = jnp.sum(received, axis=0)
    key_acc, value_acc = tuple(
        (
            part.astype(jnp.float32)
            for part in together(
                (key_acc.astype(jnp.bfloat16), value_acc.astype(jnp.bfloat16)), "tp"
            )
        )
    )
    key_half = key_acc.astype(jnp.bfloat16)
    value_half = value_acc.astype(jnp.bfloat16)
    source_grad = contract_cols(key_half, key_weight) + contract_cols(value_half, value_weight)
    weight_scale = 1.0 / math.sqrt(src_rows * sp_count)
    key_grad = sum_at_owner(
        (contract_rows(key_half, source) * weight_scale).astype(jnp.bfloat16), SP, 0
    )
    return (query_grad, source_grad, key_grad)


def solution(mesh):
    split = Mesh(mesh.devices.reshape(16, 4, mesh.shape["tp"]), ("sp_0", "sp_1", "tp"))
    return jax.shard_map(
        shards,
        mesh=split,
        in_specs=(
            P(SP, "tp"),
            P(SP, "tp"),
            P(SP, "tp"),
            P(SP, "tp"),
            P(SP, "tp"),
            P(SP, None),
            P(SP, None),
            P("tp", None),
            P("tp", None),
        ),
        out_specs=(P(SP, "tp"), P(SP, "tp"), P(SP, "tp")),
        check_vma=False,
    )
```

profile of v0, /device:TPU:6, one launch (start us, length us, event | category | flops | bytes accessed | tf_op | source)
XLA Modules:
  0.0 390.1 jit_solution(9942946184266667918)
XLA Ops:
  8.1 13.5 %all_gather.6 = bf16[2,512,128]{2,1,0:T(8,128)(2,1)} all-gather(bf16[2,128,128]{2,1,0:T(8,128)(2,1)S(1)} %pad_maximum_fusion.1), channel_id=1, replica_groups=mesh['sp_0'=16,'sp_1'=4,'tp'=8] {'sp_1'}, dimensions={1}, use_global_device_ids=true | all-gather | bytes 327680 | tf_op jit(solution)/shard_map/all_gather | solution.py:35
  23.8 18.2 %all-to-all-start = ((f32[64,2,128,1]{2,1,3,0:T(2,128)}), f32[64,2,128,1]{2,1,3,0:T(2,128)S(1)}, u32[]{:S(2)}, u32[]{:S(2)}) async-start(f32[64,2,128,1]{2,1,3,0:T(2,128)} %broadcast_in_dim.13), calls=%async_computation | async-start | bytes 131072 | tf_op jit(solution)/shard_map/all_to_all | solution.py:17
  43.0 14.7 %all-to-all-done = f32[64,2,128,1]{2,1,3,0:T(2,128)S(1)} async-done(((f32[64,2,128,1]{2,1,3,0:T(2,128)}), f32[64,2,128,1]{2,1,3,0:T(2,128)S(1)}, u32[]{:S(2)}, u32[]{:S(2)}) %all-to-all-start) | async-done | bytes 65568 | tf_op jit(solution)/shard_map/all_to_all | solution.py:17
  57.8 47.4 %all-gather.2.cloned.1.call-done = bf16[2,8192,128]{2,1,0:T(8,128)(2,1)} async-done(((bf16[2,512,128]{2,1,0:T(8,128)(2,1)}), bf16[2,8192,128]{2,1,0:T(8,128)(2,1)}) %all-gather.2.cloned.1.call-update) | async-done | bytes 4194320 | tf_op jit(solution)/shard_map/all_gather | solution.py:35
  105.3 1.5 broadcast_in_dim.11
  106.7 58.4 %while.19 = (s32[]{:T(128)}, bf16[8192,128]{1,0:T(8,128)(2,1)}, f32[512,256]{1,0:T(8,128)S(1)}, f32[512,256]{1,0:T(8,128)S(1)}, bf16[2,8192,128]{2,1,0:T(8,128)(...) while((s32[]{:T(128)}, bf16[8192,128]{1,0:T(8,128)(2,1)}, ...), condition=%wide.region_2.3_spmd, body=%wide.region_1.2_spmd.sunk | while | flops 675938304 | bytes 12481763 | solution.py:140
  106.7 1.4 fusion.41
  108.1 1.7 fusion.43
  109.8 1.6 multiply_convert_fusion.2
  111.4 1.4 fusion.42
  114.0 1.4 fusion.41
  115.4 1.7 fusion.43
  117.1 1.6 multiply_convert_fusion.2
  118.7 1.4 fusion.42
  120.2 1.2 convolution_dynamic-update-slice_fusion.2
  121.3 1.4 fusion.41
  122.7 1.7 fusion.43
  124.4 1.6 multiply_convert_fusion.2
  126.1 1.4 fusion.42
  127.5 1.2 convolution_dynamic-update-slice_fusion.2
  128.7 1.4 fusion.41
  130.0 1.7 fusion.43
  131.7 1.6 multiply_convert_fusion.2
  133.4 1.4 fusion.42
  134.8 1.2 convolution_dynamic-update-slice_fusion.2
  136.0 1.4 fusion.41
  137.4 1.7 fusion.43
  139.1 1.6 multiply_convert_fusion.2
  140.7 1.4 fusion.42
  143.3 1.4 fusion.41
  144.6 1.7 fusion.43
  146.3 1.6 multiply_convert_fusion.2
  148.0 1.4 fusion.42
  149.4 1.1 convolution_dynamic-update-slice_fusion.2
  150.6 1.4 fusion.41
  151.9 1.7 fusion.43
  153.6 1.6 multiply_convert_fusion.2
  155.3 1.4 fusion.42
  157.8 1.4 fusion.41
  159.2 1.7 fusion.43
  160.9 1.6 multiply_convert_fusion.2
  162.6 1.4 fusion.42
  166.5 70.1 %all-reduce.2.cloned.1.call-done = bf16[262144]{0:T(1024)(128)(2,1)} async-done(((bf16[262144]{0:T(1024)(128)(2,1)}), bf16[262144]{0:T(1024)(128)(2,1)}) %all-reduce.2.cloned.1.call-update) | async-done | bytes 524304 | tf_op jit(solution)/shard_map/psum | solution.py:43
  238.6 38.4 %all_to_all.15 = bf16[64,4,512]{2,1,0:T(4,128)(2,1)S(1)} all-to-all(bf16[64,4,512]{2,1,0:T(4,128)(2,1)S(1)} %reshape.49), channel_id=1, replica_groups=mesh['sp_0'=16,'sp_1'=4,'tp'=8] {'sp_0','sp_1'}, dimensions={0} | all-to-all | bytes 524288 | tf_op jit(solution)/shard_map/all_to_all | solution.py:54
  277.0 5.4 %all-to-all-start.1 = ((bf16[64,128,128]{2,1,0:T(8,128)(2,1)}), bf16[64,128,128]{2,1,0:T(8,128)(2,1)S(1)}, u32[]{:S(2)}, u32[]{:S(2)}) async-start(bf16[64,128,128]{2,1,0:T(8,128)(2,1)} %bitcast.58), calls=%async_computation.1 | async-start | bytes 4194304 | tf_op jit(solution)/shard_map/all_to_all | solution.py:142
  282.5 1.4 fusion.14
  283.9 2.3 convolution_add_fusion.2
  286.8 95.4 %all-to-all-done.1 = bf16[64,128,128]{2,1,0:T(8,128)(2,1)S(1)} async-done(((bf16[64,128,128]{2,1,0:T(8,128)(2,1)}), bf16[64,128,128]{2,1,0:T(8,128)(2,1)S(1)}, u32[]{:S(2)}, u32[]{:S(2)}) %all-to-all-start.1) | async-done | bytes 2097184 | tf_op jit(solution)/shard_map/all_to_all | solution.py:142
  (40 shorter events, 13.8 us)
Async XLA Ops:
  7.2 230.6 %copy-start = (bf16[512,512]{1,0:T(8,128)(2,1)S(1)}, bf16[512,512]{1,0:T(8,128)(2,1)}, u32[]{:S(2)}) copy-start(bf16[512,512]{1,0:T(8,128)(2,1)} %param.15) | copy-start | bytes 1572868
  7.2 98.0 %all-gather.2.cloned.1.call-start = ((), (), s32[]{:S(2)}) async-start(), calls=%async_computation.3 | async-start | bytes 4456448 | tf_op jit(solution)/shard_map/all_gather | solution.py:35
  23.8 34.0 %all-to-all-start = ((f32[64,2,128,1]{2,1,3,0:T(2,128)}), f32[64,2,128,1]{2,1,3,0:T(2,128)S(1)}, u32[]{:S(2)}, u32[]{:S(2)}) async-start(f32[64,2,128,1]{2,1,3,0:T(2,128)} %broadcast_in_dim.13), calls=%async_computation | async-start | bytes 131072 | tf_op jit(solution)/shard_map/all_to_all | solution.py:17
  42.0 194.6 %all-reduce.2.cloned.1.call-start = ((), (), s32[]{:S(2)}) async-start(), calls=%async_computation.4 | async-start | bytes 1048576 | tf_op jit(solution)/shard_map/psum | solution.py:43
  237.8 0.7 copy-start.1
  277.0 105.3 %all-to-all-start.1 = ((bf16[64,128,128]{2,1,0:T(8,128)(2,1)}), bf16[64,128,128]{2,1,0:T(8,128)(2,1)S(1)}, u32[]{:S(2)}, u32[]{:S(2)}) async-start(bf16[64,128,128]{2,1,0:T(8,128)(2,1)} %bitcast.58), calls=%async_computation.1 | async-start | bytes 4194304 | tf_op jit(solution)/shard_map/all_to_all | solution.py:142
Sparse Core Ops, SparseCore 0:
  21.7 83.4 all-gather.1
  166.6 69.9 all-reduce.1
where the time goes:
time: 392 us; the launch traced here: 390 us
  waiting for transfers between devices  228 us (58%)
  matrix products  62.1 us (16%)
  blocking collectives  51.9 us (13%)
  starting transfers between devices  23.6 us (6%)
  between operations  14.2 us (4%)
  local copies, waits for them, and re-layouts  5.3 us (1%)
  other arithmetic  4.95 us (1%)
    all_to_all x1, waiting for transfers between devices, shards(): lax.all_to_all(stacked.astype(jnp.bfloat16), SP, split_axis=0, concat_axi...  95.4 us
    psum x1, waiting for transfers between devices, together(): subtotal = lax.psum(jnp.concatenate([a.ravel() for a in arrays]), axis)  70.1 us
    all_gather x1, waiting for transfers between devices, gather_axes(): value = lax.all_gather(value, axis, axis=dim, tiled=True)  47.4 us
    all_to_all x1, blocking collectives, sum_at_owner(): lax.all_to_all(pieces, axis, split_axis=0, concat_axis=0, tiled=True)  38.4 us
    dot_general x18, matrix products, contract_cols(): lax.dot_general(left, right, (((1,), (1,)), ((), ())), preferred_element_...  27.6 us
    dot_general x17, matrix products, contract_rows(): lax.dot_general(left, right, (((0,), (0,)), ((), ())), preferred_element_...  25.4 us
    all_to_all x1, starting transfers between devices, copy_for_each(): lax.all_to_all(jnp.broadcast_to(value[None], (size, *value.shape)), axis,...  18.2 us
    all_to_all x1, waiting for transfers between devices, copy_for_each(): lax.all_to_all(jnp.broadcast_to(value[None], (size, *value.shape)), axis,...  14.7 us
  transfers between devices with their start and end apart: 4, of which 4 were waited for; matrix products, arithmetic and copies ran while one was open for 2% of the time, Pallas kernels for 0%

commit v1 on v0

v1 whole, which is shorter than its diff:
```python
import math

import jax
import jax.numpy as jnp
from jax import lax
from jax.experimental import pallas as pl
from jax.experimental.pallas import tpu as pltpu
from jax.sharding import Mesh
from jax.sharding import PartitionSpec as P

HEAD_DIM = 128
SP = ("z", "y")
TP = ("g", "h", "c")
TEAM = ("y", "h", "c")
SPLIT = (16, 4, 2, 2, 2)
F32 = jnp.float32
BF16 = jnp.bfloat16
HEAD_ROWS = 112
STAT_ROWS = 16
VMEM_LIMIT = 56 * 2**20


def in_vmem():
    return pl.BlockSpec(memory_space=pltpu.VMEM)


def pieces(value):
    high = value.astype(BF16)
    rest = value - high.astype(F32)
    middle = rest.astype(BF16)
    low = (rest - middle.astype(F32)).astype(BF16)
    return [high, middle, low]


def pack_rows(queries, attn_out, out_grad, row_lse, saved_keys, saved_values):
    rows, width = queries.shape
    src = saved_keys.shape[0]
    z_count, y_count = (SPLIT[0], SPLIT[1])
    tail = rows - HEAD_ROWS

    def kernel(head_ref, q_ref, o_ref, do_ref, lse_ref, k_ref, v_ref, main_ref, small_ref, kv_ref):
        second = head_ref[0] > 0
        main_ref[:rows, :] = q_ref[...]
        main_ref[rows:, :] = do_ref[:HEAD_ROWS, :]
        product = do_ref[...].astype(F32) * o_ref[...].astype(F32)
        delta = jnp.sum(product.T, axis=0, keepdims=True)
        eye = lax.broadcasted_iota(jnp.int32, (rows, rows), 0) == lax.broadcasted_iota(
            jnp.int32, (rows, rows), 1
        )
        lse = jnp.sum(jnp.where(eye, lse_ref[...], 0.0), axis=0, keepdims=True)
        stats = pieces(lse * math.sqrt(HEAD_DIM)) + pieces(delta)
        line = lax.broadcasted_iota(jnp.int32, (STAT_ROWS, rows), 0)
        block = jnp.zeros((STAT_ROWS, rows), F32)
        for i, s in enumerate(stats):
            block = jnp.where(line == i, s.astype(F32), block)
        block = block.astype(BF16)
        last = do_ref[HEAD_ROWS:, :]
        for z in range(z_count):
            small_ref[z, :tail, :] = last
            small_ref[z, tail:, :] = block
        k = jnp.where(second, k_ref[:, HEAD_DIM:], k_ref[:, :HEAD_DIM])
        v = jnp.where(second, v_ref[:, HEAD_DIM:], v_ref[:, :HEAD_DIM])
        for y in range(y_count):
            kv_ref[y, :src, :] = k
            kv_ref[y, src:, :] = v

    return pl.pallas_call(
        kernel,
        in_specs=[pl.BlockSpec(memory_space=pltpu.SMEM)] + [in_vmem()] * 6,
        out_specs=[in_vmem()] * 3,
        out_shape=[
            jax.ShapeDtypeStruct((rows + HEAD_ROWS, width), BF16),
            jax.ShapeDtypeStruct((z_count, tail + STAT_ROWS, width), BF16),
            jax.ShapeDtypeStruct((y_count, 2 * src, HEAD_DIM), BF16),
        ],
        name="pack_rows",
    )(
        lax.axis_index("g").reshape(1),
        queries,
        attn_out,
        out_grad,
        row_lse,
        saved_keys,
        saved_values,
    )


def dot(left, right):
    return jnp.dot(left, right, preferred_element_type=F32)


def attention_backward(main, small, keyvals):
    z_count, main_rows, dim = main.shape
    y_count, src = (keyvals.shape[0], keyvals.shape[1] // 2)
    tail = small.shape[1] - STAT_ROWS
    rows = main_rows - (HEAD_DIM - tail)
    sources = y_count * src
    targets = z_count * rows
    scale = 1.0 / math.sqrt(HEAD_DIM)
    exp_scale = math.log2(math.e) * scale
    src_tile, tgt_tile, unroll = (512, 512, 4)
    src_tiles, tgt_tiles = (sources // src_tile, targets // tgt_tile)

    def kernel(
        main_ref, small_ref, kv_ref, dq_ref, dk_ref, dv_ref,
        k_wide, v_wide, k_turned, q_turned, do_turned, q_rows, do_rows, dk_acc, dv_acc, dq_acc,
    ):
        lane = lax.broadcasted_iota(jnp.int32, (src, dim), 1)
        lse_lanes = jnp.where(lane < 3, -1.0, 0.0).astype(BF16)
        delta_lanes = jnp.where((lane >= 3) & (lane < 6), -1.0, 0.0).astype(BF16)
        for y in range(y_count):
            at = slice(y * src, (y + 1) * src)
            k = kv_ref[y, :src, :]
            k_wide[at, :dim] = k
            k_wide[at, dim:] = lse_lanes
            v_wide[at, :dim] = kv_ref[y, src:, :]
            v_wide[at, dim:] = delta_lanes
            k_turned[:, at] = k.T
        for z in range(z_count):
            at = slice(z * rows, (z + 1) * rows)
            q = main_ref[z, :rows, :]
            do = jnp.concatenate([main_ref[z, rows:, :], small_ref[z, :tail, :]], axis=0)
            stats = small_ref[z, tail:, :]
            q_rows[at, :] = q
            do_rows[at, :] = do
            q_turned[:dim, at] = q.T
            do_turned[:dim, at] = do.T
            q_turned[dim : dim + STAT_ROWS, at] = stats
            do_turned[dim : dim + STAT_ROWS, at] = stats
        blank = jnp.zeros((dim - STAT_ROWS, targets), BF16)
        q_turned[dim + STAT_ROWS :, :] = blank
        do_turned[dim + STAT_ROWS :, :] = blank
        dk_acc[...] = jnp.zeros_like(dk_acc)
        dv_acc[...] = jnp.zeros_like(dv_acc)
        dq_acc[...] = jnp.zeros_like(dq_acc)

        def tile(s0, t0):
            s, t = (pl.ds(s0, src_tile), pl.ds(t0, tgt_tile))
            scores = dot(k_wide[s, :], q_turned[:, t])
            dprobs = dot(v_wide[s, :], do_turned[:, t])
            probs = jnp.exp2(scores * exp_scale)
            dscores = (probs * dprobs).astype(BF16)
            dv_acc[s, :] += dot(probs.astype(BF16), do_rows[t, :])
            dk_acc[s, :] += dot(dscores, q_rows[t, :])
            dq_acc[:, t] += dot(k_turned[:, s], dscores)

        def step(i, carry):
            s, t = (i // (tgt_tiles // unroll), i % (tgt_tiles // unroll))
            for u in range(unroll):
                tile(
                    pl.multiple_of(s * src_tile, src_tile),
                    pl.multiple_of((t * unroll + u) * tgt_tile, tgt_tile),
                )
            return carry

        lax.fori_loop(0, src_tiles * tgt_tiles // unroll, step, 0)
        dk_ref[...] = (dk_acc[...] * scale).astype(BF16)
        dv_ref[...] = dv_acc[...].astype(BF16)
        for z in range(z_count):
            dq_ref[z] = (dq_acc[:, z * rows : (z + 1) * rows] * scale).T.astype(BF16)

    return pl.pallas_call(
        kernel,
        in_specs=[in_vmem()] * 3,
        out_specs=[in_vmem()] * 3,
        out_shape=[
            jax.ShapeDtypeStruct((z_count, rows, dim), BF16),
            jax.ShapeDtypeStruct((sources, dim), BF16),
            jax.ShapeDtypeStruct((sources, dim), BF16),
        ],
        scratch_shapes=[
            pltpu.VMEM((sources, 2 * dim), BF16),
            pltpu.VMEM((sources, 2 * dim), BF16),
            pltpu.VMEM((dim, sources), BF16),
            pltpu.VMEM((2 * dim, targets), BF16),
            pltpu.VMEM((2 * dim, targets), BF16),
            pltpu.VMEM((targets, dim), BF16),
            pltpu.VMEM((targets, dim), BF16),
            pltpu.VMEM((sources, dim), F32),
            pltpu.VMEM((sources, dim), F32),
            pltpu.VMEM((dim, targets), F32),
        ],
        compiler_params=pltpu.CompilerParams(vmem_limit_bytes=VMEM_LIMIT),
        name="attention_backward",
    )(main, small, keyvals)


def added_up(arrived, copies):
    total = jnp.sum(arrived.astype(F32), axis=0).astype(BF16)
    return jnp.broadcast_to(total[None], (copies, *total.shape))


def exchanged(value, axes):
    return lax.all_to_all(value, axes, 0, 0, tiled=True)


def shards(
    queries, attn_out, out_grad, row_lse, source, saved_keys, saved_values, key_weight, value_weight
):
    src = source.shape[0]
    team = SPLIT[1] * SPLIT[3] * SPLIT[4]
    tp_count = SPLIT[2] * SPLIT[3] * SPLIT[4]
    sp_count = SPLIT[0] * SPLIT[1]
    weight_scale = 1.0 / math.sqrt(src * sp_count)
    main, small, keyvals = pack_rows(
        queries, attn_out, out_grad, row_lse, saved_keys, saved_values
    )
    keyvals = exchanged(keyvals, "y")
    small = exchanged(small, "z")
    main = lax.all_gather(main, "z", axis=0, tiled=False)
    dq, dk, dv = attention_backward(main, small, keyvals)

    dk_pieces = exchanged(dk.reshape(team, -1, HEAD_DIM), TEAM)
    key_half = exchanged(added_up(dk_pieces, tp_count), TP)
    dq_pieces = exchanged(dq, "z")
    dv_pieces = exchanged(dv.reshape(team, -1, HEAD_DIM), TEAM)
    value_half = exchanged(added_up(dv_pieces, tp_count), TP)

    key_half = key_half.reshape(2, src, HEAD_DIM)
    value_half = value_half.reshape(2, src, HEAD_DIM)
    key_terms = lax.dot_general(
        key_half, source, (((1,), (0,)), ((), ())), preferred_element_type=F32
    )
    key_terms = (key_terms * weight_scale).astype(BF16).reshape(sp_count, -1, source.shape[1])
    key_grad = jnp.sum(exchanged(key_terms, SP).astype(F32), axis=0)
    halves = [key_half[0], key_half[1], value_half[0], value_half[1]]
    weights = jnp.concatenate([key_weight, value_weight], axis=1)
    source_grad = lax.dot_general(
        jnp.concatenate(halves, axis=1),
        weights,
        (((1,), (1,)), ((), ())),
        preferred_element_type=F32,
    )
    query_grad = jnp.sum(dq_pieces.astype(F32), axis=0)
    return (query_grad, source_grad, key_grad)


def solution(mesh):
    split = Mesh(mesh.devices.reshape(SPLIT), ("z", "y", "g", "h", "c"))
    return jax.shard_map(
        shards,
        mesh=split,
        in_specs=(
            P(SP, TP),
            P(SP, TP),
            P(SP, TP),
            P(SP, TP),
            P(SP, TP),
            P(SP, None),
            P(SP, None),
            P(TP, None),
            P(TP, None),
        ),
        out_specs=(P(SP, TP), P(SP, TP), P(SP, TP)),
        check_vma=False,
    )
```

time: 392 us -> 206 us (0.53)
  waiting for transfers between devices: 228 us -> 43 us
  matrix products: 62.1 us -> 1.76 us
  blocking collectives: 51.9 us -> 110 us
  Pallas kernels: 0 us -> 17 us
  between operations: 14.2 us -> 0.72 us
    psum x1 -> x0, waiting for transfers between devices: 70.1 us -> none  [together(): subtotal = lax.psum(jnp.concatenate([a.ravel() for a in arrays]), axis)]
    all_to_all x2 -> x5, waiting for transfers between devices: 110 us -> 43 us  [exchanged(): return lax.all_to_all(value, axes, 0, 0, tiled=True)]
    dot_general x43 -> x2, matrix products: 62.1 us -> 1.76 us  [the longest x1 1.44 us: shards(): lax.dot_general(jnp.concatenate(halves, axis=1), weights, (((1,), (1,)),...]
    all_gather x1 -> x0, waiting for transfers between devices: 47.4 us -> none  [gather_axes(): value = lax.all_gather(value, axis, axis=dim, tiled=True)]
    all_to_all x1 -> x3, blocking collectives: 38.4 us -> 73.9 us  [exchanged(): return lax.all_to_all(value, axes, 0, 0, tiled=True)]
    all_gather x1, blocking collectives: 13.5 us -> 36.2 us  [shards(): main = lax.all_gather(main, 'z', axis=0, tiled=False)]
    pallas_call x0 -> x2, Pallas kernels: none -> 17 us  [the longest x1 14.6 us: attention_backward(): pl.pallas_call(kernel, in_specs=[in_vmem()] * 3, out_specs=[in_vmem()] *...]
    all_to_all x2 -> x5, starting transfers between devices: 23.6 us -> 23.4 us  [exchanged(): return lax.all_to_all(value, axes, 0, 0, tiled=True)]
  transfers between devices with their start and end apart: 4 -> 5, of which waited for: 4 -> 4; matrix products, arithmetic and copies ran while one was open for 2% -> 1% of each run, Pallas kernels for 0% -> 0%
where the time goes in v1:
time: 206 us; the launch traced here: 203 us
  blocking collectives  110 us (53%)
  waiting for transfers between devices  43 us (21%)
  starting transfers between devices  23.4 us (11%)
  Pallas kernels  17 us (8%)
  local copies, waits for them, and re-layouts  5 us (2%)
    all_to_all x3, blocking collectives, exchanged(): return lax.all_to_all(value, axes, 0, 0, tiled=True)  73.9 us
    all_to_all x5, waiting for transfers between devices, exchanged(): return lax.all_to_all(value, axes, 0, 0, tiled=True)  43 us
    all_gather x1, blocking collectives, shards(): main = lax.all_gather(main, 'z', axis=0, tiled=False)  36.2 us
    all_to_all x5, starting transfers between devices, exchanged(): return lax.all_to_all(value, axes, 0, 0, tiled=True)  23.4 us
    pallas_call x1, Pallas kernels, attention_backward(): pl.pallas_call(kernel, in_specs=[in_vmem()] * 3, out_specs=[in_vmem()] *...  14.6 us
  transfers between devices with their start and end apart: 5, of which 4 were waited for; matrix products, arithmetic and copies ran while one was open for 1% of the time, Pallas kernels for 0%

profile of v1, /device:TPU:6, one launch (start us, length us, event | category | flops | bytes accessed | tf_op | source)
XLA Modules:
  0.0 202.5 jit_solution(8643535316919632290)
XLA Ops:
  0.6 0.0 copy-start
  0.6 0.0 copy-start.3
  0.7 0.7 copy-done.3
  1.4 0.7 copy.13.lse_ref
  2.1 2.4 %pack_rows.1 = (bf16[240,128]{1,0:T(8,128)(2,1)}, bf16[16,32,128]{2,1,0:T(8,128)(2,1)}, bf16[4,1024,128]{2,1,0:T(8,128)(2,1)}) custom-call(s32[1]{0:T(128)} %bitcast.head_ref, bf16[128,128]{1,0:T(8,128)(2,1)} %q_ref.1, bf16[128,128]{1,0:T(8,128)(2,1)} %o_ref.1, bf16[128,128]{1,0:T(8,128)(2,1)} %do_ref.1, f32[128,1]{1,0:T(8,128)} %copy.13.lse_ref, ...), custom_call_target="tpu_custom_call" | custom-call | tf_op jit(solution)/shard_map/pack_rows/pallas_call | solution.py:67
  4.5 30.1 %all_to_all.40.small_ref = bf16[16,32,128]{2,1,0:T(8,128)(2,1)} all-to-all(bf16[16,32,128]{2,1,0:T(8,128)(2,1)} %get-tuple-element.10), channel_id=1, replica_groups=mesh['z'=16,'y'=4,'g'=2,'h'=2,'c'=2] {'z'}, dimensions={0} | all-to-all | bytes 262144 | tf_op jit(solution)/shard_map/all_to_all | solution.py:194
  34.5 0.0 copy-start.2
  34.5 4.6 %all-to-all-start.1 = ((bf16[4,1024,128]{2,1,0:T(8,128)(2,1)}), bf16[4,1024,128]{2,1,0:T(8,128)(2,1)S(1)}, u32[]{:S(2)}, u32[]{:S(2)}) async-start(bf16[4,1024,128]{2,1,0:T(8,128)(2,1)} %get-tuple-element.11), calls=%async_computation.1 | async-start | bytes 2097152 | tf_op jit(solution)/shard_map/all_to_all | solution.py:194
  39.1 0.0 copy-done.2
  39.1 36.2 %all-gather = bf16[3840,128]{1,0:T(8,128)(2,1)} all-gather(bf16[240,128]{1,0:T(8,128)(2,1)S(1)} %copy-done.2), channel_id=2, replica_groups=mesh['z'=16,'y'=4,'g'=2,'h'=2,'c'=2] {'z'}, dimensions={0}, use_global_device_ids=true | all-gather | bytes 1044480 | tf_op jit(solution)/shard_map/all_gather | solution.py:210
  75.3 0.0 all-to-all-done.1.kv_ref
  75.3 0.0 copy-start.1
  75.3 1.0 copy-done.1
  76.3 14.6 %attention_backward.1 = (bf16[16,128,128]{2,1,0:T(8,128)(2,1)}, bf16[2048,128]{1,0:T(8,128)(2,1)}, bf16[2048,128]{1,0:T(8,128)(2,1)}) custom-call(bf16[16,240,128]{2,1,0:T(8,128)(2,1)} %bitcast.13, bf16[16,32,128]{2,1,0:T(8,128)(2,1)} %all_to_all.40.small_ref, bf16[4,1024,128]{2,1,0:T(8,128)(2,1)} %copy-done.1), custom_call_target="tpu_custom_call" | custom-call | tf_op jit(solution)/shard_map/attention_backward/pallas_call | solution.py:162
  90.9 16.0 %all_to_all.41 = bf16[16,128,128]{2,1,0:T(8,128)(2,1)S(1)} all-to-all(bf16[16,128,128]{2,1,0:T(8,128)(2,1)} %bitcast.15), channel_id=1, replica_groups=mesh['z'=16,'y'=4,'g'=2,'h'=2,'c'=2] {'y','h','c'}, dimensions={0} | all-to-all | bytes 1048576 | tf_op jit(solution)/shard_map/all_to_all | solution.py:194
  106.9 4.6 %all-to-all-start.5 = ((bf16[16,128,128]{2,1,0:T(8,128)(2,1)}), bf16[16,128,128]{2,1,0:T(8,128)(2,1)S(1)}, u32[]{:S(2)}, u32[]{:S(2)}) async-start(bf16[16,128,128]{2,1,0:T(8,128)(2,1)} %bitcast.5), calls=%async_computation.5 | async-start | bytes 1048576 | tf_op jit(solution)/shard_map/all_to_all | solution.py:194
  111.5 0.1 reduce_sum.43
  111.6 9.7 %all-to-all-done.5 = bf16[16,128,128]{2,1,0:T(8,128)(2,1)S(1)} async-done(((bf16[16,128,128]{2,1,0:T(8,128)(2,1)}), bf16[16,128,128]{2,1,0:T(8,128)(2,1)S(1)}, u32[]{:S(2)}, u32[]{:S(2)}) %all-to-all-start.5) | async-done | bytes 524320 | tf_op jit(solution)/shard_map/all_to_all | solution.py:194
  121.3 0.7 broadcast_in_dim.4
  122.0 5.2 %all-to-all-start.4 = ((bf16[8,128,128]{2,1,0:T(8,128)(2,1)}), bf16[8,128,128]{2,1,0:T(8,128)(2,1)S(1)}, u32[]{:S(2)}, u32[]{:S(2)}) async-start(bf16[8,128,128]{2,1,0:T(8,128)(2,1)} %broadcast_in_dim.4), calls=%async_computation.4 | async-start | bytes 524288 | tf_op jit(solution)/shard_map/all_to_all | solution.py:194
  127.2 0.1 reduce_sum.44
  127.3 5.4 %all-to-all-done.4 = bf16[8,128,128]{2,1,0:T(8,128)(2,1)S(1)} async-done(((bf16[8,128,128]{2,1,0:T(8,128)(2,1)}), bf16[8,128,128]{2,1,0:T(8,128)(2,1)S(1)}, u32[]{:S(2)}, u32[]{:S(2)}) %all-to-all-start.4) | async-done | bytes 262176 | tf_op jit(solution)/shard_map/all_to_all | solution.py:194
  132.6 0.7 broadcast_in_dim.5
  133.4 5.4 %all-to-all-start.6 = ((bf16[8,128,128]{2,1,0:T(8,128)(2,1)}), bf16[8,128,128]{2,1,0:T(8,128)(2,1)S(1)}, u32[]{:S(2)}, u32[]{:S(2)}) async-start(bf16[8,128,128]{2,1,0:T(8,128)(2,1)} %broadcast_in_dim.5), calls=%async_computation.6 | async-start | bytes 524288 | tf_op jit(solution)/shard_map/all_to_all | solution.py:194
  138.8 0.0 copy-done
  138.8 0.3 fusion
  139.1 0.1 reshape.36
  139.2 5.0 %all-to-all-done.6 = bf16[8,128,128]{2,1,0:T(8,128)(2,1)S(1)} async-done(((bf16[8,128,128]{2,1,0:T(8,128)(2,1)}), bf16[8,128,128]{2,1,0:T(8,128)(2,1)S(1)}, u32[]{:S(2)}, u32[]{:S(2)}) %all-to-all-start.6) | async-done | bytes 262176 | tf_op jit(solution)/shard_map/all_to_all | solution.py:194
  144.2 27.8 %all_to_all.42 = bf16[64,4,512]{2,1,0:T(4,128)(2,1)S(1)} all-to-all(bf16[64,4,512]{2,1,0:T(4,128)(2,1)S(1)} %reshape.36), channel_id=1, replica_groups=mesh['z'=16,'y'=4,'g'=2,'h'=2,'c'=2] {'z','y'}, dimensions={0} | all-to-all | bytes 524288 | tf_op jit(solution)/shard_map/all_to_all | solution.py:194
  172.0 3.6 %all-to-all-start.2 = ((bf16[16,128,128]{2,1,0:T(8,128)(2,1)}), bf16[16,128,128]{2,1,0:T(8,128)(2,1)S(1)}, u32[]{:S(2)}, u32[]{:S(2)}) async-start(bf16[16,128,128]{2,1,0:T(8,128)(2,1)} %get-tuple-element.12), calls=%async_computation.2 | async-start | bytes 1048576 | tf_op jit(solution)/shard_map/all_to_all | solution.py:194
  175.6 0.0 copy-start.4
  175.6 0.0 copy-start.5
  175.7 0.9 copy-done.4
  176.6 0.1 copy-done.5
  176.7 1.4 fusion.1
  178.1 0.7 convert_reduce_fusion.1
  178.9 23.0 %all-to-all-done.2 = bf16[16,128,128]{2,1,0:T(8,128)(2,1)S(1)} async-done(((bf16[16,128,128]{2,1,0:T(8,128)(2,1)}), bf16[16,128,128]{2,1,0:T(8,128)(2,1)S(1)}, u32[]{:S(2)}, u32[]{:S(2)}) %all-to-all-start.2) | async-done | bytes 524320 | tf_op jit(solution)/shard_map/all_to_all | solution.py:194
  201.8 0.7 convert_reduce_fusion
  (2 shorter events, 0.0 us)
Async XLA Ops:
  0.6 138.2 %copy-start = (bf16[512,512]{1,0:T(8,128)(2,1)S(1)}, bf16[512,512]{1,0:T(8,128)(2,1)}, u32[]{:S(2)}) copy-start(bf16[512,512]{1,0:T(8,128)(2,1)} %param.13) | copy-start | bytes 1572868
  0.6 0.7 copy-start.3
  34.5 4.6 %copy-start.2 = (bf16[240,128]{1,0:T(8,128)(2,1)S(1)}, bf16[240,128]{1,0:T(8,128)(2,1)}, u32[]{:S(2)}) copy-start(bf16[240,128]{1,0:T(8,128)(2,1)} %get-tuple-element.9) | copy-start | bytes 184324
  34.5 40.8 %all-to-all-start.1 = ((bf16[4,1024,128]{2,1,0:T(8,128)(2,1)}), bf16[4,1024,128]{2,1,0:T(8,128)(2,1)S(1)}, u32[]{:S(2)}, u32[]{:S(2)}) async-start(bf16[4,1024,128]{2,1,0:T(8,128)(2,1)} %get-tuple-element.11), calls=%async_computation.1 | async-start | bytes 2097152 | tf_op jit(solution)/shard_map/all_to_all | solution.py:194
  75.3 1.0 copy-start.1
  106.9 14.3 %all-to-all-start.5 = ((bf16[16,128,128]{2,1,0:T(8,128)(2,1)}), bf16[16,128,128]{2,1,0:T(8,128)(2,1)S(1)}, u32[]{:S(2)}, u32[]{:S(2)}) async-start(bf16[16,128,128]{2,1,0:T(8,128)(2,1)} %bitcast.5), calls=%async_computation.5 | async-start | bytes 1048576 | tf_op jit(solution)/shard_map/all_to_all | solution.py:194
  122.0 10.7 %all-to-all-start.4 = ((bf16[8,128,128]{2,1,0:T(8,128)(2,1)}), bf16[8,128,128]{2,1,0:T(8,128)(2,1)S(1)}, u32[]{:S(2)}, u32[]{:S(2)}) async-start(bf16[8,128,128]{2,1,0:T(8,128)(2,1)} %broadcast_in_dim.4), calls=%async_computation.4 | async-start | bytes 524288 | tf_op jit(solution)/shard_map/all_to_all | solution.py:194
  133.4 10.8 %all-to-all-start.6 = ((bf16[8,128,128]{2,1,0:T(8,128)(2,1)}), bf16[8,128,128]{2,1,0:T(8,128)(2,1)S(1)}, u32[]{:S(2)}, u32[]{:S(2)}) async-start(bf16[8,128,128]{2,1,0:T(8,128)(2,1)} %broadcast_in_dim.5), calls=%async_computation.6 | async-start | bytes 524288 | tf_op jit(solution)/shard_map/all_to_all | solution.py:194
  172.0 29.8 %all-to-all-start.2 = ((bf16[16,128,128]{2,1,0:T(8,128)(2,1)}), bf16[16,128,128]{2,1,0:T(8,128)(2,1)S(1)}, u32[]{:S(2)}, u32[]{:S(2)}) async-start(bf16[16,128,128]{2,1,0:T(8,128)(2,1)} %get-tuple-element.12), calls=%async_computation.2 | async-start | bytes 1048576 | tf_op jit(solution)/shard_map/all_to_all | solution.py:194
  175.6 1.0 copy-start.4
  175.6 1.0 copy-start.5

commit v2 on v1

--- a/solution.py
+++ b/solution.py
@@ -7,6 +7,7 @@
 from jax.experimental.pallas import tpu as pltpu
 from jax.sharding import Mesh
 from jax.sharding import PartitionSpec as P
+
 
 HEAD_DIM = 128
 SP = ("z", "y")
@@ -35,7 +36,7 @@
 def pack_rows(queries, attn_out, out_grad, row_lse, saved_keys, saved_values):
     rows, width = queries.shape
     src = saved_keys.shape[0]
-    z_count, y_count = (SPLIT[0], SPLIT[1])
+    z_count = SPLIT[0]
     tail = rows - HEAD_ROWS
 
     def kernel(head_ref, q_ref, o_ref, do_ref, lse_ref, k_ref, v_ref, main_ref, small_ref, kv_ref):
@@ -44,11 +45,7 @@
         main_ref[rows:, :] = do_ref[:HEAD_ROWS, :]
         product = do_ref[...].astype(F32) * o_ref[...].astype(F32)
         delta = jnp.sum(product.T, axis=0, keepdims=True)
-        eye = lax.broadcasted_iota(jnp.int32, (rows, rows), 0) == lax.broadcasted_iota(
-            jnp.int32, (rows, rows), 1
-        )
-        lse = jnp.sum(jnp.where(eye, lse_ref[...], 0.0), axis=0, keepdims=True)
-        stats = pieces(lse * math.sqrt(HEAD_DIM)) + pieces(delta)
+        stats = pieces(lse_ref[...] * math.sqrt(HEAD_DIM)) + pieces(delta)
         line = lax.broadcasted_iota(jnp.int32, (STAT_ROWS, rows), 0)
         block = jnp.zeros((STAT_ROWS, rows), F32)
         for i, s in enumerate(stats):
@@ -58,11 +55,8 @@
         for z in range(z_count):
             small_ref[z, :tail, :] = last
             small_ref[z, tail:, :] = block
-        k = jnp.where(second, k_ref[:, HEAD_DIM:], k_ref[:, :HEAD_DIM])
-        v = jnp.where(second, v_ref[:, HEAD_DIM:], v_ref[:, :HEAD_DIM])
-        for y in range(y_count):
-            kv_ref[y, :src, :] = k
-            kv_ref[y, src:, :] = v
+        kv_ref[:src, :] = jnp.where(second, k_ref[:, HEAD_DIM:], k_ref[:, :HEAD_DIM])
+        kv_ref[src:, :] = jnp.where(second, v_ref[:, HEAD_DIM:], v_ref[:, :HEAD_DIM])
 
     return pl.pallas_call(
         kernel,
@@ -71,7 +65,7 @@
         out_shape=[
             jax.ShapeDtypeStruct((rows + HEAD_ROWS, width), BF16),
             jax.ShapeDtypeStruct((z_count, tail + STAT_ROWS, width), BF16),
-            jax.ShapeDtypeStruct((y_count, 2 * src, HEAD_DIM), BF16),
+            jax.ShapeDtypeStruct((2 * src, HEAD_DIM), BF16),
         ],
         name="pack_rows",
     )(
@@ -79,7 +73,7 @@
         queries,
         attn_out,
         out_grad,
-        row_lse,
+        row_lse.reshape(1, rows),
         saved_keys,
         saved_values,
     )
@@ -89,9 +83,9 @@
     return jnp.dot(left, right, preferred_element_type=F32)
 
 
-def attention_backward(main, small, keyvals):
+def attention_backward(place, main, small, keyvals):
     z_count, main_rows, dim = main.shape
-    y_count, src = (keyvals.shape[0], keyvals.shape[1] // 2)
+    y_count, src = (len(keyvals), keyvals[0].shape[0] // 2)
     tail = small.shape[1] - STAT_ROWS
     rows = main_rows - (HEAD_DIM - tail)
     sources = y_count * src
@@ -100,20 +94,23 @@
     exp_scale = math.log2(math.e) * scale
     src_tile, tgt_tile, unroll = (512, 512, 4)
     src_tiles, tgt_tiles = (sources // src_tile, targets // tgt_tile)
+    per_y = SPLIT[3] * SPLIT[4]
+    team = y_count * per_y
+    bits = z_count.bit_length() - 1
 
     def kernel(
-        main_ref, small_ref, kv_ref, dq_ref, dk_ref, dv_ref,
+        place_ref, main_ref, small_ref, kv0_ref, kv1_ref, kv2_ref, kv3_ref, send_ref, keep_ref, dkv_ref,
         k_wide, v_wide, k_turned, q_turned, do_turned, q_rows, do_rows, dk_acc, dv_acc, dq_acc,
     ):
         lane = lax.broadcasted_iota(jnp.int32, (src, dim), 1)
         lse_lanes = jnp.where(lane < 3, -1.0, 0.0).astype(BF16)
         delta_lanes = jnp.where((lane >= 3) & (lane < 6), -1.0, 0.0).astype(BF16)
-        for y in range(y_count):
+        for y, kv_ref in enumerate((kv0_ref, kv1_ref, kv2_ref, kv3_ref)):
             at = slice(y * src, (y + 1) * src)
-            k = kv_ref[y, :src, :]
+            k = kv_ref[:src, :]
             k_wide[at, :dim] = k
             k_wide[at, dim:] = lse_lanes
-            v_wide[at, :dim] = kv_ref[y, src:, :]
+            v_wide[at, :dim] = kv_ref[src:, :]
             v_wide[at, dim:] = delta_lanes
             k_turned[:, at] = k.T
         for z in range(z_count):
@@ -154,20 +151,27 @@
             return carry
 
         lax.fori_loop(0, src_tiles * tgt_tiles // unroll, step, 0)
-        dk_ref[...] = (dk_acc[...] * scale).astype(BF16)
-        dv_ref[...] = dv_acc[...].astype(BF16)
-        for z in range(z_count):
-            dq_ref[z] = (dq_acc[:, z * rows : (z + 1) * rows] * scale).T.astype(BF16)
-
+        me, y_me = (place_ref[0], place_ref[1])
+        piece = sources // team
+        for i in range(team):
+            at = pl.multiple_of(((i // per_y + y_count - y_me) % y_count * per_y + i % per_y) * piece, piece)
+            dkv_ref[i, :piece, :] = (dk_acc[pl.ds(at, piece), :] * scale).astype(BF16)
+            dkv_ref[i, piece:, :] = dv_acc[pl.ds(at, piece), :].astype(BF16)
+        for p in range(z_count):
+            turned = sum(((p >> b) & 1) << (bits - 1 - b) for b in range(bits))
+            at = pl.multiple_of(jnp.bitwise_xor(me, turned) * rows, rows)
+            out = (dq_acc[:, pl.ds(at, rows)] * scale).T.astype(BF16)
+            if p < z_count // 2:
+                keep_ref[p] = out
+            else:
+                send_ref[p - z_count // 2] = out
+
+    half = jax.ShapeDtypeStruct((z_count // 2, rows, dim), BF16)
     return pl.pallas_call(
         kernel,
-        in_specs=[in_vmem()] * 3,
+        in_specs=[pl.BlockSpec(memory_space=pltpu.SMEM)] + [in_vmem()] * 6,
         out_specs=[in_vmem()] * 3,
-        out_shape=[
-            jax.ShapeDtypeStruct((z_count, rows, dim), BF16),
-            jax.ShapeDtypeStruct((sources, dim), BF16),
-            jax.ShapeDtypeStruct((sources, dim), BF16),
-        ],
+        out_shape=[half, half, jax.ShapeDtypeStruct((team, 2 * sources // team, dim), BF16)],
         scratch_shapes=[
             pltpu.VMEM((sources, 2 * dim), BF16),
             pltpu.VMEM((sources, 2 * dim), BF16),
@@ -182,7 +186,7 @@
         ],
         compiler_params=pltpu.CompilerParams(vmem_limit_bytes=VMEM_LIMIT),
         name="attention_backward",
-    )(main, small, keyvals)
+    )(place, main, small, *keyvals)
 
 
 def added_up(arrived, copies):
@@ -192,46 +196,65 @@
 
 def exchanged(value, axes):
     return lax.all_to_all(value, axes, 0, 0, tiled=True)
+
+
+def shifted(value, axis, distance):
+    size = lax.axis_size(axis)
+    return lax.ppermute(value, axis, [((i + distance) % size, i) for i in range(size)])
+
+
+def swapped(value, axis, distance):
+    pairs = [(i, i ^ distance) for i in range(lax.axis_size(axis))]
+    return lax.ppermute(value, axis, pairs)
+
+
+def summed_to_owner(send, keep):
+    distance = 1
+    while True:
+        arrived = swapped(send, "z", distance)
+        total = keep.astype(F32) + arrived.astype(F32)
+        count = total.shape[0] // 2
+        if count == 0:
+            return total[0]
+        total = total.astype(BF16)
+        keep, send = (total[:count], total[count:])
+        distance *= 2
 
 
 def shards(
     queries, attn_out, out_grad, row_lse, source, saved_keys, saved_values, key_weight, value_weight
 ):
     src = source.shape[0]
-    team = SPLIT[1] * SPLIT[3] * SPLIT[4]
     tp_count = SPLIT[2] * SPLIT[3] * SPLIT[4]
     sp_count = SPLIT[0] * SPLIT[1]
     weight_scale = 1.0 / math.sqrt(src * sp_count)
     main, small, keyvals = pack_rows(
         queries, attn_out, out_grad, row_lse, saved_keys, saved_values
     )
-    keyvals = exchanged(keyvals, "y")
     small = exchanged(small, "z")
+    keyvals = [keyvals] + [shifted(keyvals, "y", d) for d in range(1, SPLIT[1])]
     main = lax.all_gather(main, "z", axis=0, tiled=False)
-    dq, dk, dv = attention_backward(main, small, keyvals)
-
-    dk_pieces = exchanged(dk.reshape(team, -1, HEAD_DIM), TEAM)
-    key_half = exchanged(added_up(dk_pieces, tp_count), TP)
-    dq_pieces = exchanged(dq, "z")
-    dv_pieces = exchanged(dv.reshape(team, -1, HEAD_DIM), TEAM)
-    value_half = exchanged(added_up(dv_pieces, tp_count), TP)
-
-    key_half = key_half.reshape(2, src, HEAD_DIM)
-    value_half = value_half.reshape(2, src, HEAD_DIM)
+    place = jnp.stack([lax.axis_index("z"), lax.axis_index("y")])
+    dq_send, dq_keep, dkv = attention_backward(place, main, small, keyvals)
+
+    dkv = exchanged(dkv, TEAM)
+    halves = added_up(dkv, tp_count)
+    halves = exchanged(halves, TP).reshape(2, tp_count // 2, 2, -1, HEAD_DIM)
+    key_half, value_half = (halves[:, :, i].reshape(2, src, HEAD_DIM) for i in range(2))
+    query_grad = summed_to_owner(dq_send, dq_keep)
     key_terms = lax.dot_general(
         key_half, source, (((1,), (0,)), ((), ())), preferred_element_type=F32
     )
     key_terms = (key_terms * weight_scale).astype(BF16).reshape(sp_count, -1, source.shape[1])
-    key_grad = jnp.sum(exchanged(key_terms, SP).astype(F32), axis=0)
-    halves = [key_half[0], key_half[1], value_half[0], value_half[1]]
+    key_terms = exchanged(key_terms, SP)
+    key_grad = jnp.sum(key_terms.astype(F32), axis=0)
     weights = jnp.concatenate([key_weight, value_weight], axis=1)
     source_grad = lax.dot_general(
-        jnp.concatenate(halves, axis=1),
+        jnp.concatenate([key_half[0], key_half[1], value_half[0], value_half[1]], axis=1),
         weights,
         (((1,), (1,)), ((), ())),
         preferred_element_type=F32,
     )
-    query_grad = jnp.sum(dq_pieces.astype(F32), axis=0)
     return (query_grad, source_grad, key_grad)
 
 

time: 206 us -> 175 us (0.85)
  blocking collectives: 110 us -> 39.2 us
  starting transfers between devices: 23.4 us -> 69.4 us
  waiting for transfers between devices: 43 us -> 38.8 us
    all_to_all x3 -> x0, blocking collectives: 73.9 us -> none  [exchanged(): return lax.all_to_all(value, axes, 0, 0, tiled=True)]
    ppermute x0 -> x7, starting transfers between devices: none -> 32.7 us  [the longest x4 21.1 us: swapped(): return lax.ppermute(value, axis, pairs)]
    all_to_all x5 -> x4, waiting for transfers between devices: 43 us -> 17.1 us  [exchanged(): return lax.all_to_all(value, axes, 0, 0, tiled=True)]
    ppermute x0 -> x7, waiting for transfers between devices: none -> 21.7 us  [the longest x4 21.7 us: swapped(): return lax.ppermute(value, axis, pairs)]
    all_to_all x5 -> x4, starting transfers between devices: 23.4 us -> 36.7 us  [exchanged(): return lax.all_to_all(value, axes, 0, 0, tiled=True)]
    all_gather x1, blocking collectives: 36.2 us -> 39.2 us  [shards(): main = lax.all_gather(main, 'z', axis=0, tiled=False)]
  transfers between devices with their start and end apart: 5 -> 11, of which waited for: 4 -> 4; matrix products, arithmetic and copies ran while one was open for 1% -> 3% of each run, Pallas kernels for 0% -> 0%
where the time goes in v2:
time: 175 us; the launch traced here: 172 us
  starting transfers between devices  69.4 us (40%)
  blocking collectives  39.2 us (22%)
  waiting for transfers between devices  38.8 us (22%)
  Pallas kernels  16.4 us (9%)
  local copies, waits for them, and re-layouts  3.62 us (2%)
  other arithmetic  2.32 us (1%)
  matrix products  1.76 us (1%)
    all_gather x1, blocking collectives, shards(): main = lax.all_gather(main, 'z', axis=0, tiled=False)  39.2 us
    all_to_all x4, starting transfers between devices, exchanged(): return lax.all_to_all(value, axes, 0, 0, tiled=True)  36.7 us
    ppermute x4, waiting for transfers between devices, swapped(): return lax.ppermute(value, axis, pairs)  21.7 us
    ppermute x4, starting transfers between devices, swapped(): return lax.ppermute(value, axis, pairs)  21.1 us
    all_to_all x4, waiting for transfers between devices, exchanged(): return lax.all_to_all(value, axes, 0, 0, tiled=True)  17.1 us
    pallas_call x1, Pallas kernels, attention_backward(): pl.pallas_call(kernel, in_specs=[pl.BlockSpec(memory_space=pltpu.SMEM)] +...  14.4 us
    ppermute x3, starting transfers between devices, shifted(): lax.ppermute(value, axis, [((i + distance) % size, i) for i in range(size)])  11.5 us
  transfers between devices with their start and end apart: 11, of which 4 were waited for; matrix products, arithmetic and copies ran while one was open for 3% of the time, Pallas kernels for 0%

profile of v2, /device:TPU:6, one launch (start us, length us, event | category | flops | bytes accessed | tf_op | source)
XLA Modules:
  0.0 172.4 jit_solution(3968445714989357166)
XLA Ops:
  0.6 0.0 copy-start
  0.7 2.0 %pack_rows.1 = (bf16[240,128]{1,0:T(8,128)(2,1)}, bf16[16,32,128]{2,1,0:T(8,128)(2,1)}, bf16[1024,128]{1,0:T(8,128)(2,1)}) custom-call(s32[1]{0:T(128)} %bitcast.2.head_ref, bf16[128,128]{1,0:T(8,128)(2,1)} %q_ref.1, bf16[128,128]{1,0:T(8,128)(2,1)} %o_ref.1, bf16[128,128]{1,0:T(8,128)(2,1)} %do_ref.1, f32[1,128]{1,0:T(1,128)} %bitcast.25, ...), custom_call_target="tpu_custom_call" | custom-call | tf_op jit(solution)/shard_map/pack_rows/pallas_call | solution.py:61
  2.7 3.5 %collective-permute-start.2 = (bf16[1024,128]{1,0:T(8,128)(2,1)}, bf16[1024,128]{1,0:T(8,128)(2,1)S(1)}, u32[]{:S(2)}, u32[]{:S(2)}) collective-permute-start(bf16[1024,128]{1,0:T(8,128)(2,1)} %get-tuple-element.11.kv0_ref), channel_id=1, source_target_pairs={{24,0},{0,8},{8,16},{16,24},{25,1},{1,9},{9,17},{17,25},{26,2},{2,... | collective-permute-start | bytes 786440 | tf_op jit(solution)/shard_map/ppermute | solution.py:203
  6.2 4.8 %collective-permute-start.1 = (bf16[1024,128]{1,0:T(8,128)(2,1)}, bf16[1024,128]{1,0:T(8,128)(2,1)S(1)}, u32[]{:S(2)}, u32[]{:S(2)}) collective-permute-start(bf16[1024,128]{1,0:T(8,128)(2,1)} %get-tuple-element.11.kv0_ref), channel_id=1, source_target_pairs={{16,0},{24,8},{0,16},{8,24},{17,1},{25,9},{1,17},{9,25},{18,2},{26... | collective-permute-start | bytes 786440 | tf_op jit(solution)/shard_map/ppermute | solution.py:203
  11.0 3.3 %collective-permute-start = (bf16[1024,128]{1,0:T(8,128)(2,1)}, bf16[1024,128]{1,0:T(8,128)(2,1)S(1)}, u32[]{:S(2)}, u32[]{:S(2)}) collective-permute-start(bf16[1024,128]{1,0:T(8,128)(2,1)} %get-tuple-element.11.kv0_ref), channel_id=1, source_target_pairs={{8,0},{16,8},{24,16},{0,24},{9,1},{17,9},{25,17},{1,25},{10,2},{18... | collective-permute-start | bytes 786440 | tf_op jit(solution)/shard_map/ppermute | solution.py:203
  14.2 0.0 copy-start.6
  14.3 15.3 %all-to-all-start = ((bf16[16,32,128]{2,1,0:T(8,128)(2,1)}), bf16[16,32,128]{2,1,0:T(8,128)(2,1)S(1)}, u32[]{:S(2)}, u32[]{:S(2)}) async-start(bf16[16,32,128]{2,1,0:T(8,128)(2,1)} %get-tuple-element.10), calls=%async_computation | async-start | bytes 262144 | tf_op jit(solution)/shard_map/all_to_all | solution.py:198
  29.6 0.0 copy-done.6
  29.6 39.2 %all-gather = bf16[3840,128]{1,0:T(8,128)(2,1)} all-gather(bf16[240,128]{1,0:T(8,128)(2,1)S(1)} %copy-done.6), channel_id=2, replica_groups=mesh['z'=16,'y'=4,'g'=2,'h'=2,'c'=2] {'z'}, dimensions={0}, use_global_device_ids=true | all-gather | bytes 1044480 | tf_op jit(solution)/shard_map/all_gather | solution.py:236
  68.8 0.7 pad_add_fusion.place_ref
  69.5 0.0 collective-permute-done.2.kv3_ref
  69.5 0.0 collective-permute-done.1.kv2_ref
  69.5 0.0 copy-start.3
  69.5 0.0 collective-permute-done.kv1_ref
  69.5 0.0 copy-start.4
  69.5 0.0 all-to-all-done.small_ref
  69.5 0.0 copy-start.1
  69.5 0.7 copy-done.2
  70.2 0.1 copy-done.3
  70.3 0.1 copy-done.4
  70.4 0.1 copy-done.1
  70.4 14.4 %attention_backward.1 = (bf16[8,128,128]{2,1,0:T(8,128)(2,1)}, bf16[8,128,128]{2,1,0:T(8,128)(2,1)}, bf16[16,256,128]{2,1,0:T(8,128)(2,1)}) custom-call(s32[2]{0:T(128)} %pad_add_fusion.place_ref, bf16[16,240,128]{2,1,0:T(8,128)(2,1)} %bitcast.17, bf16[16,32,128]{2,1,0:T(8,128)(2,1)} %copy-done.1, bf16[1024,128]{1,0:T(8,128)(2,1)} %get-tuple-element.11.kv0_ref, ...), custom_call_target="tpu_custom_call" | custom-call | tf_op jit(solution)/shard_map/attention_backward/pallas_call | solution.py:170
  84.8 4.4 %all-to-all-start.1 = ((bf16[16,256,128]{2,1,0:T(8,128)(2,1)}), bf16[16,256,128]{2,1,0:T(8,128)(2,1)S(1)}, u32[]{:S(2)}, u32[]{:S(2)}) async-start(bf16[16,256,128]{2,1,0:T(8,128)(2,1)} %get-tuple-element.14), calls=%async_computation.1 | async-start | bytes 2097152 | tf_op jit(solution)/shard_map/all_to_all | solution.py:198
  89.2 0.0 copy-done.9
  89.2 2.9 %collective-permute-start.3 = (bf16[8,128,128]{2,1,0:T(8,128)(2,1)S(1)}, bf16[8,128,128]{2,1,0:T(8,128)(2,1)S(1)}, u32[]{:S(2)}, u32[]{:S(2)}) collective-permute-start(bf16[8,128,128]{2,1,0:T(8,128)(2,1)S(1)} %copy-done.9), channel_id=1, source_target_pairs={{0,32},{32,0},{64,96},{96,64},{128,160},{160,128},{192,224},{224,1... | collective-permute-start | bytes 786440 | tf_op jit(solution)/shard_map/ppermute | solution.py:208
  92.1 12.5 %all-to-all-done.1 = bf16[16,256,128]{2,1,0:T(8,128)(2,1)S(1)} async-done(((bf16[16,256,128]{2,1,0:T(8,128)(2,1)}), bf16[16,256,128]{2,1,0:T(8,128)(2,1)S(1)}, u32[]{:S(2)}, u32[]{:S(2)}) %all-to-all-start.1) | async-done | bytes 1048608 | tf_op jit(solution)/shard_map/all_to_all | solution.py:198
  104.6 0.1 reduce_sum.21
  104.7 0.9 broadcast_in_dim.2
  105.6 5.4 %all-to-all-start.2 = ((bf16[8,256,128]{2,1,0:T(8,128)(2,1)}), bf16[8,256,128]{2,1,0:T(8,128)(2,1)S(1)}, u32[]{:S(2)}, u32[]{:S(2)}) async-start(bf16[8,256,128]{2,1,0:T(8,128)(2,1)} %broadcast_in_dim.2), calls=%async_computation.2 | async-start | bytes 1048576 | tf_op jit(solution)/shard_map/all_to_all | solution.py:198
  111.0 0.0 collective-permute-done.3
  111.0 0.0 copy-done.5
  111.0 0.1 add_convert_fusion
  111.1 3.5 %collective-permute-start.4 = (bf16[4,128,128]{2,1,0:T(8,128)(2,1)S(1)}, bf16[4,128,128]{2,1,0:T(8,128)(2,1)S(1)}, u32[]{:S(2)}, u32[]{:S(2)}) collective-permute-start(bf16[4,128,128]{2,1,0:T(8,128)(2,1)S(1)} %slice.54), channel_id=1, source_target_pairs={{0,64},{32,96},{64,0},{96,32},{128,192},{160,224},{192,128},{224,1... | collective-permute-start | bytes 393224 | tf_op jit(solution)/shard_map/ppermute | solution.py:208
  114.6 4.6 %all-to-all-done.2 = bf16[8,256,128]{2,1,0:T(8,128)(2,1)S(1)} async-done(((bf16[8,256,128]{2,1,0:T(8,128)(2,1)}), bf16[8,256,128]{2,1,0:T(8,128)(2,1)S(1)}, u32[]{:S(2)}, u32[]{:S(2)}) %all-to-all-start.2) | async-done | bytes 524320 | tf_op jit(solution)/shard_map/all_to_all | solution.py:198
  119.3 0.3 fusion
  119.6 0.8 reshape.30
  120.4 11.5 %all-to-all-start.3 = ((bf16[64,4,512]{2,1,0:T(4,128)(2,1)}), bf16[64,4,512]{2,1,0:T(4,128)(2,1)S(1)}, u32[]{:S(2)}, u32[]{:S(2)}) async-start(bf16[64,4,512]{2,1,0:T(4,128)(2,1)} %reshape.30), calls=%async_computation.3 | async-start | bytes 524288 | tf_op jit(solution)/shard_map/all_to_all | solution.py:198
  131.9 0.0 collective-permute-done.4
  132.0 7.4 %collective-permute-start.5 = (bf16[2,128,128]{2,1,0:T(8,128)(2,1)S(1)}, bf16[2,128,128]{2,1,0:T(8,128)(2,1)S(1)}, u32[]{:S(2)}, u32[]{:S(2)}) collective-permute-start(bf16[2,128,128]{2,1,0:T(8,128)(2,1)S(1)} %slice.56), channel_id=1, source_target_pairs={{0,128},{32,160},{64,192},{96,224},{128,0},{160,32},{192,64},{224,... | collective-permute-start | bytes 196616 | tf_op jit(solution)/shard_map/ppermute | solution.py:208
  139.4 14.5 %collective-permute-done.5 = bf16[2,128,128]{2,1,0:T(8,128)(2,1)S(1)} collective-permute-done((bf16[2,128,128]{2,1,0:T(8,128)(2,1)S(1)}, bf16[2,128,128]{2,1,0:T(8,128)(2,1)S(1)}, u32[]{:S(2)}, u32[]{:S(2)}) %collective-permute-start.5) | collective-permute-done | bytes 65568 | tf_op jit(solution)/shard_map/ppermute | solution.py:208
  154.0 7.4 %collective-permute-start.6 = (bf16[1,128,128]{2,1,0:T(8,128)(2,1)S(1)}, bf16[1,128,128]{2,1,0:T(8,128)(2,1)S(1)}, u32[]{:S(2)}, u32[]{:S(2)}) collective-permute-start(bf16[1,128,128]{2,1,0:T(8,128)(2,1)S(1)} %slice.58), channel_id=1, source_target_pairs={{0,256},{32,288},{64,320},{96,352},{128,384},{160,416},{192,448},{... | collective-permute-start | bytes 98312 | tf_op jit(solution)/shard_map/ppermute | solution.py:208
  161.4 7.1 %collective-permute-done.6 = bf16[1,128,128]{2,1,0:T(8,128)(2,1)S(1)} collective-permute-done((bf16[1,128,128]{2,1,0:T(8,128)(2,1)S(1)}, bf16[1,128,128]{2,1,0:T(8,128)(2,1)S(1)}, u32[]{:S(2)}, u32[]{:S(2)}) %collective-permute-start.6) | collective-permute-done | bytes 32800 | tf_op jit(solution)/shard_map/ppermute | solution.py:208
  168.5 0.6 add_bitcast_fusion
  169.2 0.9 copy-done.7
  170.1 0.1 copy-done.8
  170.2 1.4 fusion.1
  171.6 0.0 all-to-all-done.3
  171.6 0.7 convert_reduce_fusion
  (13 shorter events, 0.1 us)
Async XLA Ops:
  0.6 118.7 %copy-start = (bf16[512,512]{1,0:T(8,128)(2,1)S(1)}, bf16[512,512]{1,0:T(8,128)(2,1)}, u32[]{:S(2)}) copy-start(bf16[512,512]{1,0:T(8,128)(2,1)} %param.13) | copy-start | bytes 1572868
  2.7 66.8 %collective-permute-start.2 = (bf16[1024,128]{1,0:T(8,128)(2,1)}, bf16[1024,128]{1,0:T(8,128)(2,1)S(1)}, u32[]{:S(2)}, u32[]{:S(2)}) collective-permute-start(bf16[1024,128]{1,0:T(8,128)(2,1)} %get-tuple-element.11.kv0_ref), channel_id=1, source_target_pairs={{24,0},{0,8},{8,16},{16,24},{25,1},{1,9},{9,17},{17,25},{26,2},{2,... | collective-permute-start | bytes 786440 | tf_op jit(solution)/shard_map/ppermute | solution.py:203
  6.2 63.3 %collective-permute-start.1 = (bf16[1024,128]{1,0:T(8,128)(2,1)}, bf16[1024,128]{1,0:T(8,128)(2,1)S(1)}, u32[]{:S(2)}, u32[]{:S(2)}) collective-permute-start(bf16[1024,128]{1,0:T(8,128)(2,1)} %get-tuple-element.11.kv0_ref), channel_id=1, source_target_pairs={{16,0},{24,8},{0,16},{8,24},{17,1},{25,9},{1,17},{9,25},{18,2},{26... | collective-permute-start | bytes 786440 | tf_op jit(solution)/shard_map/ppermute | solution.py:203
  11.0 58.5 %collective-permute-start = (bf16[1024,128]{1,0:T(8,128)(2,1)}, bf16[1024,128]{1,0:T(8,128)(2,1)S(1)}, u32[]{:S(2)}, u32[]{:S(2)}) collective-permute-start(bf16[1024,128]{1,0:T(8,128)(2,1)} %get-tuple-element.11.kv0_ref), channel_id=1, source_target_pairs={{8,0},{16,8},{24,16},{0,24},{9,1},{17,9},{25,17},{1,25},{10,2},{18... | collective-permute-start | bytes 786440 | tf_op jit(solution)/shard_map/ppermute | solution.py:203
  14.2 15.4 %copy-start.6 = (bf16[240,128]{1,0:T(8,128)(2,1)S(1)}, bf16[240,128]{1,0:T(8,128)(2,1)}, u32[]{:S(2)}) copy-start(bf16[240,128]{1,0:T(8,128)(2,1)} %get-tuple-element.9) | copy-start | bytes 184324
  14.3 55.2 %all-to-all-start = ((bf16[16,32,128]{2,1,0:T(8,128)(2,1)}), bf16[16,32,128]{2,1,0:T(8,128)(2,1)S(1)}, u32[]{:S(2)}, u32[]{:S(2)}) async-start(bf16[16,32,128]{2,1,0:T(8,128)(2,1)} %get-tuple-element.10), calls=%async_computation | async-start | bytes 262144 | tf_op jit(solution)/shard_map/all_to_all | solution.py:198
  69.5 0.7 copy-start.2
  69.5 0.8 copy-start.3
  69.5 0.9 copy-start.4
  69.5 0.9 copy-start.1
  84.8 4.4 %copy-start.9 = (bf16[8,128,128]{2,1,0:T(8,128)(2,1)S(1)}, bf16[8,128,128]{2,1,0:T(8,128)(2,1)}, u32[]{:S(2)}) copy-start(bf16[8,128,128]{2,1,0:T(8,128)(2,1)} %get-tuple-element.13) | copy-start | bytes 786436
  84.8 19.8 %all-to-all-start.1 = ((bf16[16,256,128]{2,1,0:T(8,128)(2,1)}), bf16[16,256,128]{2,1,0:T(8,128)(2,1)S(1)}, u32[]{:S(2)}, u32[]{:S(2)}) async-start(bf16[16,256,128]{2,1,0:T(8,128)(2,1)} %get-tuple-element.14), calls=%async_computation.1 | async-start | bytes 2097152 | tf_op jit(solution)/shard_map/all_to_all | solution.py:198
  89.2 21.8 %collective-permute-start.3 = (bf16[8,128,128]{2,1,0:T(8,128)(2,1)S(1)}, bf16[8,128,128]{2,1,0:T(8,128)(2,1)S(1)}, u32[]{:S(2)}, u32[]{:S(2)}) collective-permute-start(bf16[8,128,128]{2,1,0:T(8,128)(2,1)S(1)} %copy-done.9), channel_id=1, source_target_pairs={{0,32},{32,0},{64,96},{96,64},{128,160},{160,128},{192,224},{224,1... | collective-permute-start | bytes 786440 | tf_op jit(solution)/shard_map/ppermute | solution.py:208
  105.6 5.4 %copy-start.5 = (bf16[8,128,128]{2,1,0:T(8,128)(2,1)S(1)}, bf16[8,128,128]{2,1,0:T(8,128)(2,1)}, u32[]{:S(2)}) copy-start(bf16[8,128,128]{2,1,0:T(8,128)(2,1)} %get-tuple-element.12) | copy-start | bytes 786436
  105.6 13.7 %all-to-all-start.2 = ((bf16[8,256,128]{2,1,0:T(8,128)(2,1)}), bf16[8,256,128]{2,1,0:T(8,128)(2,1)S(1)}, u32[]{:S(2)}, u32[]{:S(2)}) async-start(bf16[8,256,128]{2,1,0:T(8,128)(2,1)} %broadcast_in_dim.2), calls=%async_computation.2 | async-start | bytes 1048576 | tf_op jit(solution)/shard_map/all_to_all | solution.py:198
  111.1 20.8 %collective-permute-start.4 = (bf16[4,128,128]{2,1,0:T(8,128)(2,1)S(1)}, bf16[4,128,128]{2,1,0:T(8,128)(2,1)S(1)}, u32[]{:S(2)}, u32[]{:S(2)}) collective-permute-start(bf16[4,128,128]{2,1,0:T(8,128)(2,1)S(1)} %slice.54), channel_id=1, source_target_pairs={{0,64},{32,96},{64,0},{96,32},{128,192},{160,224},{192,128},{224,1... | collective-permute-start | bytes 393224 | tf_op jit(solution)/shard_map/ppermute | solution.py:208
  120.4 51.2 %all-to-all-start.3 = ((bf16[64,4,512]{2,1,0:T(4,128)(2,1)}), bf16[64,4,512]{2,1,0:T(4,128)(2,1)S(1)}, u32[]{:S(2)}, u32[]{:S(2)}) async-start(bf16[64,4,512]{2,1,0:T(4,128)(2,1)} %reshape.30), calls=%async_computation.3 | async-start | bytes 524288 | tf_op jit(solution)/shard_map/all_to_all | solution.py:198
  132.0 21.9 %collective-permute-start.5 = (bf16[2,128,128]{2,1,0:T(8,128)(2,1)S(1)}, bf16[2,128,128]{2,1,0:T(8,128)(2,1)S(1)}, u32[]{:S(2)}, u32[]{:S(2)}) collective-permute-start(bf16[2,128,128]{2,1,0:T(8,128)(2,1)S(1)} %slice.56), channel_id=1, source_target_pairs={{0,128},{32,160},{64,192},{96,224},{128,0},{160,32},{192,64},{224,... | collective-permute-start | bytes 196616 | tf_op jit(solution)/shard_map/ppermute | solution.py:208
  154.0 14.5 %collective-permute-start.6 = (bf16[1,128,128]{2,1,0:T(8,128)(2,1)S(1)}, bf16[1,128,128]{2,1,0:T(8,128)(2,1)S(1)}, u32[]{:S(2)}, u32[]{:S(2)}) collective-permute-start(bf16[1,128,128]{2,1,0:T(8,128)(2,1)S(1)} %slice.58), channel_id=1, source_target_pairs={{0,256},{32,288},{64,320},{96,352},{128,384},{160,416},{192,448},{... | collective-permute-start | bytes 98312 | tf_op jit(solution)/shard_map/ppermute | solution.py:208
  169.2 0.9 copy-start.7
  169.2 1.0 copy-start.8

commit v3 on v2

v3 whole, which is shorter than its diff:
```python
import math

import jax
import jax.numpy as jnp
from jax import lax
from jax.experimental import pallas as pl
from jax.experimental.pallas import tpu as pltpu
from jax.sharding import Mesh
from jax.sharding import PartitionSpec as P


HEAD_DIM = 128
SP = ("z", "y")
TP = ("g", "h", "c")
TEAM = ("y", "h", "c")
SPLIT = (16, 4, 2, 2, 2)
F32 = jnp.float32
BF16 = jnp.bfloat16
FIRST = 96
STAT_ROWS = 16
VMEM_LIMIT = 56 * 2**20


def in_vmem():
    return pl.BlockSpec(memory_space=pltpu.VMEM)


def pieces(value):
    high = value.astype(BF16)
    rest = value - high.astype(F32)
    middle = rest.astype(BF16)
    low = (rest - middle.astype(F32)).astype(BF16)
    return [high, middle, low]


def pack_rows(queries, attn_out, out_grad, row_lse, saved_keys, saved_values):
    rows, width = queries.shape
    src = saved_keys.shape[0]
    z_count, y_count = (SPLIT[0], SPLIT[1])

    def kernel(head_ref, q_ref, o_ref, do_ref, lse_ref, k_ref, v_ref, main_ref, last_ref, kv_ref):
        second = head_ref[0] > 0
        main_ref[:rows, :] = q_ref[...]
        main_ref[rows : rows + FIRST, :] = do_ref[:FIRST, :]
        product = do_ref[...].astype(F32) * o_ref[...].astype(F32)
        delta = jnp.sum(product.T, axis=0, keepdims=True)
        stats = pieces(lse_ref[...] * math.sqrt(HEAD_DIM)) + pieces(delta)
        line = lax.broadcasted_iota(jnp.int32, (STAT_ROWS, rows), 0)
        block = jnp.zeros((STAT_ROWS, rows), F32)
        for i, s in enumerate(stats):
            block = jnp.where(line == i, s.astype(F32), block)
        main_ref[rows + FIRST :, :] = block.astype(BF16)
        last = do_ref[FIRST:, :]
        for z in range(z_count):
            last_ref[z] = last
        k = jnp.where(second, k_ref[:, HEAD_DIM:], k_ref[:, :HEAD_DIM])
        v = jnp.where(second, v_ref[:, HEAD_DIM:], v_ref[:, :HEAD_DIM])
        for y in range(y_count):
            kv_ref[y, :src, :] = k
            kv_ref[y, src:, :] = v

    return pl.pallas_call(
        kernel,
        in_specs=[pl.BlockSpec(memory_space=pltpu.SMEM)] + [in_vmem()] * 6,
        out_specs=[in_vmem()] * 3,
        out_shape=[
            jax.ShapeDtypeStruct((rows + FIRST + STAT_ROWS, width), BF16),
            jax.ShapeDtypeStruct((z_count, rows - FIRST, width), BF16),
            jax.ShapeDtypeStruct((y_count, 2 * src, HEAD_DIM), BF16),
        ],
        name="pack_rows",
    )(
        lax.axis_index("g").reshape(1),
        queries,
        attn_out,
        out_grad,
        row_lse.reshape(1, rows),
        saved_keys,
        saved_values,
    )


def dot(left, right):
    return jnp.dot(left, right, preferred_element_type=F32)


def attention_backward(main, keyvals, last=None, before=None, me=None):
    z_count, main_rows, dim = main.shape
    y_count, src = (keyvals.shape[0], keyvals.shape[1] // 2)
    rows = main_rows - FIRST - STAT_ROWS
    low, high = (0, FIRST) if last is None else (FIRST, rows)
    each = high - low
    sources, targets = (y_count * src, z_count * each)
    scale = 1.0 / math.sqrt(HEAD_DIM)
    exp_scale = math.log2(math.e) * scale
    src_tile, tgt_tile = (512, 512)
    team = y_count * SPLIT[3] * SPLIT[4]
    piece = sources // team
    bits = z_count.bit_length() - 1

    def prepare(main_ref, kv_ref, last_ref, k_wide, v_wide, k_turned, q_turned, do_turned, q_rows, do_rows):
        lane = lax.broadcasted_iota(jnp.int32, (src, dim), 1)
        lse_lanes = jnp.where(lane < 3, -1.0, 0.0).astype(BF16)
        delta_lanes = jnp.where((lane >= 3) & (lane < 6), -1.0, 0.0).astype(BF16)
        for y in range(y_count):
            at = slice(y * src, (y + 1) * src)
            k = kv_ref[y, :src, :]
            k_wide[at, :dim] = k
            k_wide[at, dim:] = lse_lanes
            v_wide[at, :dim] = kv_ref[y, src:, :]
            v_wide[at, dim:] = delta_lanes
            k_turned[:, at] = k.T
        blank = jnp.zeros((dim - STAT_ROWS, dim), BF16)
        for z in range(z_count):
            at = slice(z * each, (z + 1) * each)
            q_rows[at, :dim] = main_ref[z, low:high, :]
            stats = jnp.concatenate([main_ref[z, rows + FIRST :, :], blank], axis=0)
            q_rows[at, dim:] = stats.T[low:high, :]
            do_rows[at, :] = main_ref[z, rows : rows + FIRST, :] if last_ref is None else last_ref[z]
        for b in range(0, targets, dim):
            at = slice(b, b + dim)
            q_turned[:dim, at] = q_rows[at, :dim].T
            stats = q_rows[at, dim:].T
            q_turned[dim:, at] = stats
            do_turned[:dim, at] = do_rows[at, :].T
            do_turned[dim:, at] = stats

    def work(k_wide, v_wide, k_turned, q_turned, do_turned, q_rows, do_rows, dk_acc, dv_acc, dq_acc):
        def step(i, carry):
            s = pl.ds(pl.multiple_of(i * src_tile, src_tile), src_tile)
            for t0 in range(0, targets, tgt_tile):
                t = slice(t0, t0 + tgt_tile)
                scores = dot(k_wide[s, :], q_turned[:, t])
                dprobs = dot(v_wide[s, :], do_turned[:, t])
                probs = jnp.exp2(scores * exp_scale)
                dscores = (probs * dprobs).astype(BF16)
                dv_acc[s, :] += dot(probs.astype(BF16), do_rows[t, :])
                dk_acc[s, :] += dot(dscores, q_rows[t, :dim])
                dq_acc[:, t] += dot(k_turned[:, s], dscores)
            return carry

        dq_acc[...] = jnp.zeros_like(dq_acc)
        lax.fori_loop(0, sources // src_tile, step, 0)

    def first_kernel(main_ref, kv_ref, dk_ref, dv_ref, dq_ref, *scratch):
        prepare(main_ref, kv_ref, None, *scratch[:-1])
        dk_ref[...] = jnp.zeros_like(dk_ref)
        dv_ref[...] = jnp.zeros_like(dv_ref)
        work(*scratch[:-1], dk_ref, dv_ref, scratch[-1])
        for z in range(z_count // 4):
            at = slice(z * 4 * each, (z + 1) * 4 * each)
            turned = (scratch[-1][:, at] * scale).T.astype(BF16)
            for i in range(4):
                dq_ref[z * 4 + i] = turned[i * each : (i + 1) * each, :]

    def last_kernel(
        me_ref, main_ref, kv_ref, last_ref, dk_in, dv_in, dq_in, send_ref, keep_ref, dkv_ref, *scratch
    ):
        prepare(main_ref, kv_ref, last_ref, *scratch[:-4])
        dk_acc, dv_acc, dq_acc, dq_rows = scratch[-4:]
        dk_acc[...] = dk_in[...]
        dv_acc[...] = dv_in[...]
        work(*scratch[:-4], dk_acc, dv_acc, dq_acc)
        for i in range(team):
            at = slice(i * piece, (i + 1) * piece)
            dkv_ref[i, :piece, :] = (dk_acc[at, :] * scale).astype(BF16)
            dkv_ref[i, piece:, :] = dv_acc[at, :].astype(BF16)
        for z in range(z_count // 4):
            at = slice(z * 4 * each, (z + 1) * 4 * each)
            turned = (dq_acc[:, at] * scale).T.astype(BF16)
            for i in range(4):
                dq_rows[z * 4 + i] = turned[i * each : (i + 1) * each, :]
        for p in range(z_count):
            turned = sum(((p >> b) & 1) << (bits - 1 - b) for b in range(bits))
            z = jnp.bitwise_xor(me_ref[0], turned)
            out = keep_ref if p < z_count // 2 else send_ref
            out[p % (z_count // 2), :FIRST, :] = dq_in[z]
            out[p % (z_count // 2), FIRST:, :] = dq_rows[z]

    sums = jax.ShapeDtypeStruct((sources, dim), F32)
    scratch = [
        pltpu.VMEM((sources, 2 * dim), BF16),
        pltpu.VMEM((sources, 2 * dim), BF16),
        pltpu.VMEM((dim, sources), BF16),
        pltpu.VMEM((2 * dim, targets), BF16),
        pltpu.VMEM((2 * dim, targets), BF16),
        pltpu.VMEM((targets, 2 * dim), BF16),
        pltpu.VMEM((targets, dim), BF16),
    ]
    params = pltpu.CompilerParams(vmem_limit_bytes=VMEM_LIMIT)
    if last is None:
        return pl.pallas_call(
            first_kernel,
            in_specs=[in_vmem()] * 2,
            out_specs=[in_vmem()] * 3,
            out_shape=[sums, sums, jax.ShapeDtypeStruct((z_count, each, dim), BF16)],
            scratch_shapes=scratch + [pltpu.VMEM((dim, targets), F32)],
            compiler_params=params,
            name="attention_first",
        )(main, keyvals)
    half = jax.ShapeDtypeStruct((z_count // 2, rows, dim), BF16)
    return pl.pallas_call(
        last_kernel,
        in_specs=[pl.BlockSpec(memory_space=pltpu.SMEM)] + [in_vmem()] * 6,
        out_specs=[in_vmem()] * 3,
        out_shape=[half, half, jax.ShapeDtypeStruct((team, 2 * piece, dim), BF16)],
        scratch_shapes=scratch
        + [
            pltpu.VMEM((sources, dim), F32),
            pltpu.VMEM((sources, dim), F32),
            pltpu.VMEM((dim, targets), F32),
            pltpu.VMEM((z_count, each, dim), BF16),
        ],
        compiler_params=params,
        name="attention_last",
    )(me, main, keyvals, last, *before)


def added_up(arrived, copies):
    total = jnp.sum(arrived.astype(F32), axis=0).astype(BF16)
    return jnp.broadcast_to(total[None], (copies, *total.shape))


def exchanged(value, axes):
    return lax.all_to_all(value, axes, 0, 0, tiled=True)


def swapped(value, axis, distance):
    pairs = [(i, i ^ distance) for i in range(lax.axis_size(axis))]
    return lax.ppermute(value, axis, pairs)


def summed_to_owner(send, keep):
    distance = 1
    while True:
        arrived = swapped(send, "z", distance)
        total = keep.astype(F32) + arrived.astype(F32)
        count = total.shape[0] // 2
        if count == 0:
            return total[0]
        total = total.astype(BF16)
        keep, send = (total[:count], total[count:])
        distance *= 2


def shards(
    queries, attn_out, out_grad, row_lse, source, saved_keys, saved_values, key_weight, value_weight
):
    src = source.shape[0]
    tp_count = SPLIT[2] * SPLIT[3] * SPLIT[4]
    sp_count = SPLIT[0] * SPLIT[1]
    weight_scale = 1.0 / math.sqrt(src * sp_count)
    main, last, keyvals = pack_rows(
        queries, attn_out, out_grad, row_lse, saved_keys, saved_values
    )
    keyvals = exchanged(keyvals, "y")
    main = lax.all_gather(main, "z", axis=0, tiled=False)
    last = exchanged(last, "z")
    before = attention_backward(main, keyvals)
    me = lax.axis_index("z").reshape(1)
    dq_send, dq_keep, dkv = attention_backward(main, keyvals, last, before, me)

    dkv = exchanged(dkv, TEAM)
    halves = added_up(dkv, tp_count)
    halves = exchanged(halves, TP).reshape(2, tp_count // 2, 2, -1, HEAD_DIM)
    key_half, value_half = (halves[:, :, i].reshape(2, src, HEAD_DIM) for i in range(2))
    query_grad = summed_to_owner(dq_send, dq_keep)
    key_terms = lax.dot_general(
        key_half, source, (((1,), (0,)), ((), ())), preferred_element_type=F32
    )
    key_terms = (key_terms * weight_scale).astype(BF16).reshape(sp_count, -1, source.shape[1])
    key_terms = exchanged(key_terms, SP)
    key_grad = jnp.sum(key_terms.astype(F32), axis=0)
    weights = jnp.concatenate([key_weight, value_weight], axis=1)
    source_grad = lax.dot_general(
        jnp.concatenate([key_half[0], key_half[1], value_half[0], value_half[1]], axis=1),
        weights,
        (((1,), (1,)), ((), ())),
        preferred_element_type=F32,
    )
    return (query_grad, source_grad, key_grad)


def solution(mesh):
    split = Mesh(mesh.devices.reshape(SPLIT), ("z", "y", "g", "h", "c"))
    return jax.shard_map(
        shards,
        mesh=split,
        in_specs=(
            P(SP, TP),
            P(SP, TP),
            P(SP, TP),
            P(SP, TP),
            P(SP, TP),
            P(SP, None),
            P(SP, None),
            P(TP, None),
            P(TP, None),
        ),
        out_specs=(P(SP, TP), P(SP, TP), P(SP, TP)),
        check_vma=False,
    )
```

time: 175 us -> 187 us (1.069)
  blocking collectives: 39.2 us -> 58.7 us
  starting transfers between devices: 69.4 us -> 57.6 us
  Pallas kernels: 16.4 us -> 21.8 us
    all_to_all x0 -> x1, blocking collectives: none -> 19.7 us  [exchanged(): return lax.all_to_all(value, axes, 0, 0, tiled=True)]
    ppermute x3 -> x0, starting transfers between devices: 11.5 us -> none  [shifted(): lax.ppermute(value, axis, [((i + distance) % size, i) for i in range(size)])]
    pallas_call x1 -> x2, Pallas kernels: 14.4 us -> 19.5 us  [the longest x1 12 us: attention_backward(): pl.pallas_call(first_kernel, in_specs=[in_vmem()] * 2, out_specs=[in_vmem...]
  transfers between devices with their start and end apart: 11 -> 8, of which waited for: 4 -> 4; matrix products, arithmetic and copies ran while one was open for 3% -> 2% of each run, Pallas kernels for 0% -> 6%
where the time goes in v3:
time: 187 us; the launch traced here: 185 us
  blocking collectives  58.7 us (31%)
  starting transfers between devices  57.6 us (31%)
  waiting for transfers between devices  39 us (21%)
  Pallas kernels  21.8 us (12%)
  local copies, waits for them, and re-layouts  3.34 us (2%)
    all_gather x1, blocking collectives, shards(): main = lax.all_gather(main, 'z', axis=0, tiled=False)  39 us
    all_to_all x4, starting transfers between devices, exchanged(): return lax.all_to_all(value, axes, 0, 0, tiled=True)  36.6 us
    ppermute x4, waiting for transfers between devices, swapped(): return lax.ppermute(value, axis, pairs)  21.7 us
    ppermute x4, starting transfers between devices, swapped(): return lax.ppermute(value, axis, pairs)  21 us
    all_to_all x1, blocking collectives, exchanged(): return lax.all_to_all(value, axes, 0, 0, tiled=True)  19.7 us
    all_to_all x4, waiting for transfers between devices, exchanged(): return lax.all_to_all(value, axes, 0, 0, tiled=True)  17.3 us
    pallas_call x1, Pallas kernels, attention_backward(): pl.pallas_call(first_kernel, in_specs=[in_vmem()] * 2, out_specs=[in_vmem...  12 us
    pallas_call x1, Pallas kernels, attention_backward(): pl.pallas_call(last_kernel, in_specs=[pl.BlockSpec(memory_space=pltpu.SME...  7.53 us
  transfers between devices with their start and end apart: 8, of which 4 were waited for; matrix products, arithmetic and copies ran while one was open for 2% of the time, Pallas kernels for 6%

profile of v3, /device:TPU:6, one launch (start us, length us, event | category | flops | bytes accessed | tf_op | source)
XLA Modules:
  0.0 184.6 jit_solution(1769560327011753375)
XLA Ops:
  0.6 0.0 copy-start
  0.7 2.3 %pack_rows.1 = (bf16[240,128]{1,0:T(8,128)(2,1)}, bf16[16,32,128]{2,1,0:T(8,128)(2,1)}, bf16[4,1024,128]{2,1,0:T(8,128)(2,1)}) custom-call(s32[1]{0:T(128)} %bitcast.1.head_ref, bf16[128,128]{1,0:T(8,128)(2,1)} %q_ref.1, bf16[128,128]{1,0:T(8,128)(2,1)} %o_ref.1, bf16[128,128]{1,0:T(8,128)(2,1)} %do_ref.1, f32[1,128]{1,0:T(1,128)} %bitcast.25, ...), custom_call_target="tpu_custom_call" | custom-call | tf_op jit(solution)/shard_map/pack_rows/pallas_call | solution.py:62
  2.9 19.7 %all_to_all.25.kv_ref = bf16[4,1024,128]{2,1,0:T(8,128)(2,1)} all-to-all(bf16[4,1024,128]{2,1,0:T(8,128)(2,1)} %get-tuple-element.13), channel_id=1, replica_groups=mesh['z'=16,'y'=4,'g'=2,'h'=2,'c'=2] {'y'}, dimensions={0} | all-to-all | bytes 2097152 | tf_op jit(solution)/shard_map/all_to_all | solution.py:225
  22.6 0.0 copy-start.3
  22.6 15.3 %all-to-all-start.1 = ((bf16[16,32,128]{2,1,0:T(8,128)(2,1)}), bf16[16,32,128]{2,1,0:T(8,128)(2,1)S(1)}, u32[]{:S(2)}, u32[]{:S(2)}) async-start(bf16[16,32,128]{2,1,0:T(8,128)(2,1)} %get-tuple-element.14), calls=%async_computation.1 | async-start | bytes 262144 | tf_op jit(solution)/shard_map/all_to_all | solution.py:225
  38.0 0.0 copy-done.3
  38.0 39.0 %all-gather = bf16[3840,128]{1,0:T(8,128)(2,1)} all-gather(bf16[240,128]{1,0:T(8,128)(2,1)S(1)} %copy-done.3), channel_id=2, replica_groups=mesh['z'=16,'y'=4,'g'=2,'h'=2,'c'=2] {'z'}, dimensions={0}, use_global_device_ids=true | all-gather | bytes 1044480 | tf_op jit(solution)/shard_map/all_gather | solution.py:257
  76.9 12.0 %attention_first.1 = (f32[2048,128]{1,0:T(8,128)}, f32[2048,128]{1,0:T(8,128)}, bf16[16,96,128]{2,1,0:T(8,128)(2,1)}) custom-call(bf16[16,240,128]{2,1,0:T(8,128)(2,1)} %bitcast.16, bf16[4,1024,128]{2,1,0:T(8,128)(2,1)} %all_to_all.25.kv_ref), custom_call_target="tpu_custom_call" | custom-call | tf_op jit(solution)/shard_map/attention_first/pallas_call | solution.py:192
  88.9 0.0 all-to-all-done.1.last_ref
  88.9 0.0 copy-start.1
  88.9 0.6 copy-done.1
  89.6 7.5 %attention_last.1 = (bf16[8,128,128]{2,1,0:T(8,128)(2,1)}, bf16[8,128,128]{2,1,0:T(8,128)(2,1)}, bf16[16,256,128]{2,1,0:T(8,128)(2,1)}) custom-call(s32[1]{0:T(128)} %bitcast.me_ref, bf16[16,240,128]{2,1,0:T(8,128)(2,1)} %bitcast.17, bf16[4,1024,128]{2,1,0:T(8,128)(2,1)} %all_to_all.25.kv_ref, bf16[16,32,128]{2,1,0:T(8,128)(2,1)} %copy-done.1, ...), custom_call_target="tpu_custom_call" | custom-call | tf_op jit(solution)/shard_map/attention_last/pallas_call | solution.py:202
  97.1 0.0 copy-start.6
  97.1 4.4 %all-to-all-start.2 = ((bf16[16,256,128]{2,1,0:T(8,128)(2,1)}), bf16[16,256,128]{2,1,0:T(8,128)(2,1)S(1)}, u32[]{:S(2)}, u32[]{:S(2)}) async-start(bf16[16,256,128]{2,1,0:T(8,128)(2,1)} %get-tuple-element.20), calls=%async_computation.2 | async-start | bytes 2097152 | tf_op jit(solution)/shard_map/all_to_all | solution.py:225
  101.5 0.0 copy-done.6
  101.5 2.9 %collective-permute-start = (bf16[8,128,128]{2,1,0:T(8,128)(2,1)S(1)}, bf16[8,128,128]{2,1,0:T(8,128)(2,1)S(1)}, u32[]{:S(2)}, u32[]{:S(2)}) collective-permute-start(bf16[8,128,128]{2,1,0:T(8,128)(2,1)S(1)} %copy-done.6), channel_id=1, source_target_pairs={{0,32},{32,0},{64,96},{96,64},{128,160},{160,128},{192,224},{224,1... | collective-permute-start | bytes 786440 | tf_op jit(solution)/shard_map/ppermute | solution.py:230
  104.4 12.5 %all-to-all-done.2 = bf16[16,256,128]{2,1,0:T(8,128)(2,1)S(1)} async-done(((bf16[16,256,128]{2,1,0:T(8,128)(2,1)}), bf16[16,256,128]{2,1,0:T(8,128)(2,1)S(1)}, u32[]{:S(2)}, u32[]{:S(2)}) %all-to-all-start.2) | async-done | bytes 1048608 | tf_op jit(solution)/shard_map/all_to_all | solution.py:225
  116.9 0.1 reduce_sum.21
  117.0 0.9 broadcast_in_dim.2
  117.9 0.0 copy-start.2
  117.9 5.4 %all-to-all-start.3 = ((bf16[8,256,128]{2,1,0:T(8,128)(2,1)}), bf16[8,256,128]{2,1,0:T(8,128)(2,1)S(1)}, u32[]{:S(2)}, u32[]{:S(2)}) async-start(bf16[8,256,128]{2,1,0:T(8,128)(2,1)} %broadcast_in_dim.2), calls=%async_computation.3 | async-start | bytes 1048576 | tf_op jit(solution)/shard_map/all_to_all | solution.py:225
  123.3 0.0 collective-permute-done
  123.3 0.0 copy-done.2
  123.3 0.1 add_convert_fusion
  123.4 3.3 %collective-permute-start.1 = (bf16[4,128,128]{2,1,0:T(8,128)(2,1)S(1)}, bf16[4,128,128]{2,1,0:T(8,128)(2,1)S(1)}, u32[]{:S(2)}, u32[]{:S(2)}) collective-permute-start(bf16[4,128,128]{2,1,0:T(8,128)(2,1)S(1)} %slice.54), channel_id=1, source_target_pairs={{0,64},{32,96},{64,0},{96,32},{128,192},{160,224},{192,128},{224,1... | collective-permute-start | bytes 393224 | tf_op jit(solution)/shard_map/ppermute | solution.py:230
  126.7 4.8 %all-to-all-done.3 = bf16[8,256,128]{2,1,0:T(8,128)(2,1)S(1)} async-done(((bf16[8,256,128]{2,1,0:T(8,128)(2,1)}), bf16[8,256,128]{2,1,0:T(8,128)(2,1)S(1)}, u32[]{:S(2)}, u32[]{:S(2)}) %all-to-all-start.3) | async-done | bytes 524320 | tf_op jit(solution)/shard_map/all_to_all | solution.py:225
  131.6 0.0 copy-done
  131.6 0.3 fusion
  131.9 0.8 reshape.34
  132.7 11.4 %all-to-all-start.4 = ((bf16[64,4,512]{2,1,0:T(4,128)(2,1)}), bf16[64,4,512]{2,1,0:T(4,128)(2,1)S(1)}, u32[]{:S(2)}, u32[]{:S(2)}) async-start(bf16[64,4,512]{2,1,0:T(4,128)(2,1)} %reshape.34), calls=%async_computation.4 | async-start | bytes 524288 | tf_op jit(solution)/shard_map/all_to_all | solution.py:225
  144.2 0.0 collective-permute-done.1
  144.2 7.4 %collective-permute-start.2 = (bf16[2,128,128]{2,1,0:T(8,128)(2,1)S(1)}, bf16[2,128,128]{2,1,0:T(8,128)(2,1)S(1)}, u32[]{:S(2)}, u32[]{:S(2)}) collective-permute-start(bf16[2,128,128]{2,1,0:T(8,128)(2,1)S(1)} %slice.56), channel_id=1, source_target_pairs={{0,128},{32,160},{64,192},{96,224},{128,0},{160,32},{192,64},{224,... | collective-permute-start | bytes 196616 | tf_op jit(solution)/shard_map/ppermute | solution.py:230
  151.6 14.5 %collective-permute-done.2 = bf16[2,128,128]{2,1,0:T(8,128)(2,1)S(1)} collective-permute-done((bf16[2,128,128]{2,1,0:T(8,128)(2,1)S(1)}, bf16[2,128,128]{2,1,0:T(8,128)(2,1)S(1)}, u32[]{:S(2)}, u32[]{:S(2)}) %collective-permute-start.2) | collective-permute-done | bytes 65568 | tf_op jit(solution)/shard_map/ppermute | solution.py:230
  166.2 7.4 %collective-permute-start.3 = (bf16[1,128,128]{2,1,0:T(8,128)(2,1)S(1)}, bf16[1,128,128]{2,1,0:T(8,128)(2,1)S(1)}, u32[]{:S(2)}, u32[]{:S(2)}) collective-permute-start(bf16[1,128,128]{2,1,0:T(8,128)(2,1)S(1)} %slice.58), channel_id=1, source_target_pairs={{0,256},{32,288},{64,320},{96,352},{128,384},{160,416},{192,448},{... | collective-permute-start | bytes 98312 | tf_op jit(solution)/shard_map/ppermute | solution.py:230
  173.6 7.1 %collective-permute-done.3 = bf16[1,128,128]{2,1,0:T(8,128)(2,1)S(1)} collective-permute-done((bf16[1,128,128]{2,1,0:T(8,128)(2,1)S(1)}, bf16[1,128,128]{2,1,0:T(8,128)(2,1)S(1)}, u32[]{:S(2)}, u32[]{:S(2)}) %collective-permute-start.3) | collective-permute-done | bytes 32800 | tf_op jit(solution)/shard_map/ppermute | solution.py:230
  180.7 0.6 add_bitcast_fusion
  181.4 0.0 copy-start.4
  181.4 0.0 copy-start.5
  181.4 0.9 copy-done.4
  182.3 0.1 copy-done.5
  182.4 1.4 fusion.1
  183.8 0.0 all-to-all-done.4
  183.8 0.7 convert_reduce_fusion
  (7 shorter events, 0.1 us)
Async XLA Ops:
  0.6 131.0 %copy-start = (bf16[512,512]{1,0:T(8,128)(2,1)S(1)}, bf16[512,512]{1,0:T(8,128)(2,1)}, u32[]{:S(2)}) copy-start(bf16[512,512]{1,0:T(8,128)(2,1)} %param.13) | copy-start | bytes 1572868
  22.6 15.3 %copy-start.3 = (bf16[240,128]{1,0:T(8,128)(2,1)S(1)}, bf16[240,128]{1,0:T(8,128)(2,1)}, u32[]{:S(2)}) copy-start(bf16[240,128]{1,0:T(8,128)(2,1)} %get-tuple-element.12) | copy-start | bytes 184324
  22.6 66.3 %all-to-all-start.1 = ((bf16[16,32,128]{2,1,0:T(8,128)(2,1)}), bf16[16,32,128]{2,1,0:T(8,128)(2,1)S(1)}, u32[]{:S(2)}, u32[]{:S(2)}) async-start(bf16[16,32,128]{2,1,0:T(8,128)(2,1)} %get-tuple-element.14), calls=%async_computation.1 | async-start | bytes 262144 | tf_op jit(solution)/shard_map/all_to_all | solution.py:225
  88.9 0.6 copy-start.1
  97.1 4.4 %copy-start.6 = (bf16[8,128,128]{2,1,0:T(8,128)(2,1)S(1)}, bf16[8,128,128]{2,1,0:T(8,128)(2,1)}, u32[]{:S(2)}) copy-start(bf16[8,128,128]{2,1,0:T(8,128)(2,1)} %get-tuple-element.19) | copy-start | bytes 786436
  97.1 19.8 %all-to-all-start.2 = ((bf16[16,256,128]{2,1,0:T(8,128)(2,1)}), bf16[16,256,128]{2,1,0:T(8,128)(2,1)S(1)}, u32[]{:S(2)}, u32[]{:S(2)}) async-start(bf16[16,256,128]{2,1,0:T(8,128)(2,1)} %get-tuple-element.20), calls=%async_computation.2 | async-start | bytes 2097152 | tf_op jit(solution)/shard_map/all_to_all | solution.py:225
  101.5 21.8 %collective-permute-start = (bf16[8,128,128]{2,1,0:T(8,128)(2,1)S(1)}, bf16[8,128,128]{2,1,0:T(8,128)(2,1)S(1)}, u32[]{:S(2)}, u32[]{:S(2)}) collective-permute-start(bf16[8,128,128]{2,1,0:T(8,128)(2,1)S(1)} %copy-done.6), channel_id=1, source_target_pairs={{0,32},{32,0},{64,96},{96,64},{128,160},{160,128},{192,224},{224,1... | collective-permute-start | bytes 786440 | tf_op jit(solution)/shard_map/ppermute | solution.py:230
  117.9 5.4 %copy-start.2 = (bf16[8,128,128]{2,1,0:T(8,128)(2,1)S(1)}, bf16[8,128,128]{2,1,0:T(8,128)(2,1)}, u32[]{:S(2)}) copy-start(bf16[8,128,128]{2,1,0:T(8,128)(2,1)} %get-tuple-element.18) | copy-start | bytes 786436
  117.9 13.7 %all-to-all-start.3 = ((bf16[8,256,128]{2,1,0:T(8,128)(2,1)}), bf16[8,256,128]{2,1,0:T(8,128)(2,1)S(1)}, u32[]{:S(2)}, u32[]{:S(2)}) async-start(bf16[8,256,128]{2,1,0:T(8,128)(2,1)} %broadcast_in_dim.2), calls=%async_computation.3 | async-start | bytes 1048576 | tf_op jit(solution)/shard_map/all_to_all | solution.py:225
  123.4 20.7 %collective-permute-start.1 = (bf16[4,128,128]{2,1,0:T(8,128)(2,1)S(1)}, bf16[4,128,128]{2,1,0:T(8,128)(2,1)S(1)}, u32[]{:S(2)}, u32[]{:S(2)}) collective-permute-start(bf16[4,128,128]{2,1,0:T(8,128)(2,1)S(1)} %slice.54), channel_id=1, source_target_pairs={{0,64},{32,96},{64,0},{96,32},{128,192},{160,224},{192,128},{224,1... | collective-permute-start | bytes 393224 | tf_op jit(solution)/shard_map/ppermute | solution.py:230
  132.7 51.1 %all-to-all-start.4 = ((bf16[64,4,512]{2,1,0:T(4,128)(2,1)}), bf16[64,4,512]{2,1,0:T(4,128)(2,1)S(1)}, u32[]{:S(2)}, u32[]{:S(2)}) async-start(bf16[64,4,512]{2,1,0:T(4,128)(2,1)} %reshape.34), calls=%async_computation.4 | async-start | bytes 524288 | tf_op jit(solution)/shard_map/all_to_all | solution.py:225
  144.2 21.9 %collective-permute-start.2 = (bf16[2,128,128]{2,1,0:T(8,128)(2,1)S(1)}, bf16[2,128,128]{2,1,0:T(8,128)(2,1)S(1)}, u32[]{:S(2)}, u32[]{:S(2)}) collective-permute-start(bf16[2,128,128]{2,1,0:T(8,128)(2,1)S(1)} %slice.56), channel_id=1, source_target_pairs={{0,128},{32,160},{64,192},{96,224},{128,0},{160,32},{192,64},{224,... | collective-permute-start | bytes 196616 | tf_op jit(solution)/shard_map/ppermute | solution.py:230
  166.2 14.5 %collective-permute-start.3 = (bf16[1,128,128]{2,1,0:T(8,128)(2,1)S(1)}, bf16[1,128,128]{2,1,0:T(8,128)(2,1)S(1)}, u32[]{:S(2)}, u32[]{:S(2)}) collective-permute-start(bf16[1,128,128]{2,1,0:T(8,128)(2,1)S(1)} %slice.58), channel_id=1, source_target_pairs={{0,256},{32,288},{64,320},{96,352},{128,384},{160,416},{192,448},{... | collective-permute-start | bytes 98312 | tf_op jit(solution)/shard_map/ppermute | solution.py:230
  181.4 0.9 copy-start.4
  181.4 1.0 copy-start.5

commit v4 on v3

--- a/solution.py
+++ b/solution.py
@@ -18,7 +18,8 @@
 BF16 = jnp.bfloat16
 FIRST = 96
 STAT_ROWS = 16
-VMEM_LIMIT = 56 * 2**20
+VMEM_LIMIT = 18 * 2**20
+PACK_VMEM_LIMIT = 8 * 2**20
 
 
 def in_vmem():
@@ -68,6 +69,7 @@
             jax.ShapeDtypeStruct((z_count, rows - FIRST, width), BF16),
             jax.ShapeDtypeStruct((y_count, 2 * src, HEAD_DIM), BF16),
         ],
+        compiler_params=pltpu.CompilerParams(vmem_limit_bytes=PACK_VMEM_LIMIT),
         name="pack_rows",
     )(
         lax.axis_index("g").reshape(1),
@@ -234,12 +236,12 @@
     distance = 1
     while True:
         arrived = swapped(send, "z", distance)
-        total = keep.astype(F32) + arrived.astype(F32)
-        count = total.shape[0] // 2
+        count = keep.shape[0] // 2
         if count == 0:
-            return total[0]
-        total = total.astype(BF16)
-        keep, send = (total[:count], total[count:])
+            return keep[0].astype(F32) + arrived[0].astype(F32)
+        send = (keep[count:].astype(F32) + arrived[count:].astype(F32)).astype(BF16)
+        keep, arrived = lax.optimization_barrier((keep, arrived))
+        keep = (keep[:count].astype(F32) + arrived[:count].astype(F32)).astype(BF16)
         distance *= 2
 
 

time: 187 us -> 174 us (0.930)
  waiting for transfers between devices: 39 us -> 22 us
  local copies, waits for them, and re-layouts: 3.34 us -> 13.7 us
  Pallas kernels: 21.8 us -> 14.1 us
  starting transfers between devices: 57.6 us -> 62 us
  blocking collectives: 58.7 us -> 56 us
    all_to_all x4, waiting for transfers between devices: 17.3 us -> 3 us  [exchanged(): return lax.all_to_all(value, axes, 0, 0, tiled=True)]
    unnamed x14 -> x32, local copies, waits for them, and re-layouts: 1.65 us -> 12 us
    ppermute x4, starting transfers between devices: 21 us -> 25.5 us  [swapped(): return lax.ppermute(value, axis, pairs)]
    pallas_call x1, Pallas kernels: 7.53 us -> 4.15 us  [attention_backward(): pl.pallas_call(last_kernel, in_specs=[pl.BlockSpec(memory_space=pltpu.SME...]
    pallas_call x1, Pallas kernels: 12 us -> 9.19 us  [attention_backward(): pl.pallas_call(first_kernel, in_specs=[in_vmem()] * 2, out_specs=[in_vmem...]
    ppermute x4, waiting for transfers between devices: 21.7 us -> 19 us  [swapped(): return lax.ppermute(value, axis, pairs)]
    all_gather x1, blocking collectives: 39 us -> 36.6 us  [shards(): main = lax.all_gather(main, 'z', axis=0, tiled=False)]
  transfers between devices with their start and end apart: 8 -> 8, of which waited for: 4 -> 4; matrix products, arithmetic and copies ran while one was open for 2% -> 3% of each run, Pallas kernels for 6% -> 5%
where the time goes in v4:
time: 174 us; the launch traced here: 172 us
  starting transfers between devices  62 us (36%)
  blocking collectives  56 us (32%)
  waiting for transfers between devices  22 us (13%)
  Pallas kernels  14.1 us (8%)
  local copies, waits for them, and re-layouts  13.7 us (8%)
  matrix products  1.77 us (1%)
    all_gather x1, blocking collectives, shards(): main = lax.all_gather(main, 'z', axis=0, tiled=False)  36.6 us
    all_to_all x4, starting transfers between devices, exchanged(): return lax.all_to_all(value, axes, 0, 0, tiled=True)  36.4 us
    ppermute x4, starting transfers between devices, swapped(): return lax.ppermute(value, axis, pairs)  25.5 us
    all_to_all x1, blocking collectives, exchanged(): return lax.all_to_all(value, axes, 0, 0, tiled=True)  19.3 us
    ppermute x4, waiting for transfers between devices, swapped(): return lax.ppermute(value, axis, pairs)  19 us
    unnamed x32, local copies, waits for them, and re-layouts  12 us
    pallas_call x1, Pallas kernels, attention_backward(): pl.pallas_call(first_kernel, in_specs=[in_vmem()] * 2, out_specs=[in_vmem...  9.19 us
    pallas_call x1, Pallas kernels, attention_backward(): pl.pallas_call(last_kernel, in_specs=[pl.BlockSpec(memory_space=pltpu.SME...  4.15 us
  transfers between devices with their start and end apart: 8, of which 4 were waited for; matrix products, arithmetic and copies ran while one was open for 3% of the time, Pallas kernels for 5%

profile of v4, /device:TPU:6, one launch (start us, length us, event | category | flops | bytes accessed | tf_op | source)
XLA Modules:
  0.0 172.0 jit_solution(4415338147046220203)
XLA Ops:
  0.6 0.0 copy-start
  0.7 0.0 copy-start.11
  0.7 0.7 copy-done.11
  1.4 0.9 copy-done.6
  2.3 0.9 copy-done.7
  3.3 0.8 copy-done.8
  4.0 0.8 copy-done.9
  4.8 0.8 copy-done.10
  5.5 0.8 pack_rows.1
  6.3 19.3 %all_to_all.25.kv_ref = bf16[4,1024,128]{2,1,0:T(8,128)(2,1)S(1)} all-to-all(bf16[4,1024,128]{2,1,0:T(8,128)(2,1)S(1)} %get-tuple-element.19), channel_id=1, replica_groups=mesh['z'=16,'y'=4,'g'=2,'h'=2,'c'=2] {'y'}, dimensions={0} | all-to-all | bytes 2097152 | tf_op jit(solution)/shard_map/all_to_all | solution.py:227
  25.7 15.2 %all-to-all-start.1 = ((bf16[16,32,128]{2,1,0:T(8,128)(2,1)}), bf16[16,32,128]{2,1,0:T(8,128)(2,1)S(1)}, u32[]{:S(2)}, u32[]{:S(2)}) async-start(bf16[16,32,128]{2,1,0:T(8,128)(2,1)} %get-tuple-element.20), calls=%async_computation.1 | async-start | bytes 262144 | tf_op jit(solution)/shard_map/all_to_all | solution.py:227
  40.9 36.6 %all-gather = bf16[3840,128]{1,0:T(8,128)(2,1)S(1)} all-gather(bf16[240,128]{1,0:T(8,128)(2,1)S(1)} %get-tuple-element.18), channel_id=2, replica_groups=mesh['z'=16,'y'=4,'g'=2,'h'=2,'c'=2] {'z'}, dimensions={0}, use_global_device_ids=true | all-gather | bytes 1044480 | tf_op jit(solution)/shard_map/all_gather | solution.py:259
  77.5 9.2 %attention_first.1 = (f32[2048,128]{1,0:T(8,128)S(1)}, f32[2048,128]{1,0:T(8,128)S(1)}, bf16[16,96,128]{2,1,0:T(8,128)(2,1)S(1)}) custom-call(bf16[16,240,128]{2,1,0:T(8,128)(2,1)S(1)} %bitcast.16, bf16[4,1024,128]{2,1,0:T(8,128)(2,1)S(1)} %all_to_all.25.kv_ref), custom_call_target="tpu_custom_call" | custom-call | tf_op jit(solution)/shard_map/attention_first/pallas_call | solution.py:194
  86.7 0.0 copy-start.1
  86.7 1.0 copy-done.1
  87.7 1.0 copy-done.3
  88.7 0.0 all-to-all-done.1.last_ref
  88.7 1.2 copy-done.2
  90.0 1.2 copy-done.4
  91.2 4.2 %attention_last.1 = (bf16[8,128,128]{2,1,0:T(8,128)(2,1)S(1)}, bf16[8,128,128]{2,1,0:T(8,128)(2,1)S(1)}, bf16[16,256,128]{2,1,0:T(8,128)(2,1)S(1)}) custom-call(s32[1]{0:T(128)} %bitcast.me_ref, bf16[16,240,128]{2,1,0:T(8,128)(2,1)S(1)} %bitcast.17, bf16[4,1024,128]{2,1,0:T(8,128)(2,1)S(1)} %all_to_all.25.kv_ref, ...), custom_call_target="tpu_custom_call" | custom-call | tf_op jit(solution)/shard_map/attention_last/pallas_call | solution.py:204
  95.3 0.0 copy-start.5
  95.4 1.0 copy-done.5
  96.3 0.7 copy-done.12
  97.0 4.4 %all-to-all-start.2 = ((bf16[16,256,128]{2,1,0:T(8,128)(2,1)}), bf16[16,256,128]{2,1,0:T(8,128)(2,1)S(1)}, u32[]{:S(2)}, u32[]{:S(2)}) async-start(bf16[16,256,128]{2,1,0:T(8,128)(2,1)} %copy-done.5), calls=%async_computation.2 | async-start | bytes 2097152 | tf_op jit(solution)/shard_map/all_to_all | solution.py:227
  101.4 0.0 copy-done.13
  101.4 3.0 %collective-permute-start = (bf16[8,128,128]{2,1,0:T(8,128)(2,1)S(1)}, bf16[8,128,128]{2,1,0:T(8,128)(2,1)S(1)}, u32[]{:S(2)}, u32[]{:S(2)}) collective-permute-start(bf16[8,128,128]{2,1,0:T(8,128)(2,1)S(1)} %copy-done.13), channel_id=1, source_target_pairs={{0,32},{32,0},{64,96},{96,64},{128,160},{160,128},{192,224},{224,1... | collective-permute-start | bytes 786440 | tf_op jit(solution)/shard_map/ppermute | solution.py:232
  104.4 7.2 %collective-permute-done = bf16[8,128,128]{2,1,0:T(8,128)(2,1)S(1)} collective-permute-done((bf16[8,128,128]{2,1,0:T(8,128)(2,1)S(1)}, bf16[8,128,128]{2,1,0:T(8,128)(2,1)S(1)}, u32[]{:S(2)}, u32[]{:S(2)}) %collective-permute-start) | collective-permute-done | bytes 262176 | tf_op jit(solution)/shard_map/ppermute | solution.py:232
  111.7 3.5 %collective-permute-start.1 = (bf16[4,128,128]{2,1,0:T(8,128)(2,1)S(1)}, bf16[4,128,128]{2,1,0:T(8,128)(2,1)S(1)}, u32[]{:S(2)}, u32[]{:S(2)}) collective-permute-start(bf16[4,128,128]{2,1,0:T(8,128)(2,1)S(1)} %add_convert_fusion), channel_id=1, source_target_pairs={{0,64},{32,96},{64,0},{96,32},{128,192},{160,224},{192,128},{224,1... | collective-permute-start | bytes 393224 | tf_op jit(solution)/shard_map/ppermute | solution.py:232
  115.3 1.5 all-to-all-done.2
  116.8 0.1 reduce_sum.21
  116.9 0.9 broadcast_in_dim.2
  117.8 5.3 %all-to-all-start.3 = ((bf16[8,256,128]{2,1,0:T(8,128)(2,1)}), bf16[8,256,128]{2,1,0:T(8,128)(2,1)S(1)}, u32[]{:S(2)}, u32[]{:S(2)}) async-start(bf16[8,256,128]{2,1,0:T(8,128)(2,1)} %broadcast_in_dim.2), calls=%async_computation.3 | async-start | bytes 1048576 | tf_op jit(solution)/shard_map/all_to_all | solution.py:227
  123.1 0.0 collective-permute-done.1
  123.2 6.7 %collective-permute-start.2 = (bf16[2,128,128]{2,1,0:T(8,128)(2,1)S(1)}, bf16[2,128,128]{2,1,0:T(8,128)(2,1)S(1)}, u32[]{:S(2)}, u32[]{:S(2)}) collective-permute-start(bf16[2,128,128]{2,1,0:T(8,128)(2,1)S(1)} %add_convert_fusion.2), channel_id=1, source_target_pairs={{0,128},{32,160},{64,192},{96,224},{128,0},{160,32},{192,64},{224,... | collective-permute-start | bytes 196616 | tf_op jit(solution)/shard_map/ppermute | solution.py:232
  129.9 1.5 all-to-all-done.3
  131.4 0.0 copy-done
  131.4 0.3 fusion
  131.7 0.8 reshape.37
  132.5 11.5 %all-to-all-start.4 = ((bf16[64,4,512]{2,1,0:T(4,128)(2,1)}), bf16[64,4,512]{2,1,0:T(4,128)(2,1)S(1)}, u32[]{:S(2)}, u32[]{:S(2)}) async-start(bf16[64,4,512]{2,1,0:T(4,128)(2,1)} %reshape.37), calls=%async_computation.4 | async-start | bytes 524288 | tf_op jit(solution)/shard_map/all_to_all | solution.py:227
  144.1 0.0 collective-permute-done.2
  144.1 12.3 %collective-permute-start.3 = (bf16[1,128,128]{2,1,0:T(8,128)(2,1)S(1)}, bf16[1,128,128]{2,1,0:T(8,128)(2,1)S(1)}, u32[]{:S(2)}, u32[]{:S(2)}) collective-permute-start(bf16[1,128,128]{2,1,0:T(8,128)(2,1)S(1)} %add_convert_fusion.4), channel_id=1, source_target_pairs={{0,256},{32,288},{64,320},{96,352},{128,384},{160,416},{192,448},{... | collective-permute-start | bytes 98312 | tf_op jit(solution)/shard_map/ppermute | solution.py:232
  156.4 11.7 %collective-permute-done.3 = bf16[1,128,128]{2,1,0:T(8,128)(2,1)S(1)} collective-permute-done((bf16[1,128,128]{2,1,0:T(8,128)(2,1)S(1)}, bf16[1,128,128]{2,1,0:T(8,128)(2,1)S(1)}, u32[]{:S(2)}, u32[]{:S(2)}) %collective-permute-start.3) | collective-permute-done | bytes 32800 | tf_op jit(solution)/shard_map/ppermute | solution.py:232
  168.1 0.6 add_bitcast_fusion
  168.8 0.9 copy-done.14
  169.7 0.1 copy-done.15
  169.8 1.4 fusion.1
  171.2 0.0 all-to-all-done.4
  171.2 0.7 convert_reduce_fusion
  (19 shorter events, 0.2 us)
Async XLA Ops:
  0.6 130.7 %copy-start = (bf16[512,512]{1,0:T(8,128)(2,1)S(1)}, bf16[512,512]{1,0:T(8,128)(2,1)}, u32[]{:S(2)}) copy-start(bf16[512,512]{1,0:T(8,128)(2,1)} %param.13) | copy-start | bytes 1572868
  0.7 0.7 copy-start.11
  1.4 0.9 copy-start.6
  2.3 0.9 copy-start.7
  3.3 0.8 copy-start.8
  4.0 0.8 copy-start.9
  4.8 0.8 copy-start.10
  25.7 63.0 %all-to-all-start.1 = ((bf16[16,32,128]{2,1,0:T(8,128)(2,1)}), bf16[16,32,128]{2,1,0:T(8,128)(2,1)S(1)}, u32[]{:S(2)}, u32[]{:S(2)}) async-start(bf16[16,32,128]{2,1,0:T(8,128)(2,1)} %get-tuple-element.20), calls=%async_computation.1 | async-start | bytes 262144 | tf_op jit(solution)/shard_map/all_to_all | solution.py:227
  86.7 1.0 copy-start.1
  87.7 1.0 copy-start.3
  88.7 1.2 copy-start.2
  90.0 1.2 copy-start.4
  95.3 1.0 copy-start.5
  96.3 0.7 copy-start.12
  97.0 4.4 %copy-start.13 = (bf16[8,128,128]{2,1,0:T(8,128)(2,1)S(1)}, bf16[8,128,128]{2,1,0:T(8,128)(2,1)}, u32[]{:S(2)}) copy-start(bf16[8,128,128]{2,1,0:T(8,128)(2,1)} %copy-done.12) | copy-start | bytes 786436
  97.0 19.8 %all-to-all-start.2 = ((bf16[16,256,128]{2,1,0:T(8,128)(2,1)}), bf16[16,256,128]{2,1,0:T(8,128)(2,1)S(1)}, u32[]{:S(2)}, u32[]{:S(2)}) async-start(bf16[16,256,128]{2,1,0:T(8,128)(2,1)} %copy-done.5), calls=%async_computation.2 | async-start | bytes 2097152 | tf_op jit(solution)/shard_map/all_to_all | solution.py:227
  101.4 10.2 %collective-permute-start = (bf16[8,128,128]{2,1,0:T(8,128)(2,1)S(1)}, bf16[8,128,128]{2,1,0:T(8,128)(2,1)S(1)}, u32[]{:S(2)}, u32[]{:S(2)}) collective-permute-start(bf16[8,128,128]{2,1,0:T(8,128)(2,1)S(1)} %copy-done.13), channel_id=1, source_target_pairs={{0,32},{32,0},{64,96},{96,64},{128,160},{160,128},{192,224},{224,1... | collective-permute-start | bytes 786440 | tf_op jit(solution)/shard_map/ppermute | solution.py:232
  111.7 11.4 %collective-permute-start.1 = (bf16[4,128,128]{2,1,0:T(8,128)(2,1)S(1)}, bf16[4,128,128]{2,1,0:T(8,128)(2,1)S(1)}, u32[]{:S(2)}, u32[]{:S(2)}) collective-permute-start(bf16[4,128,128]{2,1,0:T(8,128)(2,1)S(1)} %add_convert_fusion), channel_id=1, source_target_pairs={{0,64},{32,96},{64,0},{96,32},{128,192},{160,224},{192,128},{224,1... | collective-permute-start | bytes 393224 | tf_op jit(solution)/shard_map/ppermute | solution.py:232
  117.8 13.6 %all-to-all-start.3 = ((bf16[8,256,128]{2,1,0:T(8,128)(2,1)}), bf16[8,256,128]{2,1,0:T(8,128)(2,1)S(1)}, u32[]{:S(2)}, u32[]{:S(2)}) async-start(bf16[8,256,128]{2,1,0:T(8,128)(2,1)} %broadcast_in_dim.2), calls=%async_computation.3 | async-start | bytes 1048576 | tf_op jit(solution)/shard_map/all_to_all | solution.py:227
  123.2 20.9 %collective-permute-start.2 = (bf16[2,128,128]{2,1,0:T(8,128)(2,1)S(1)}, bf16[2,128,128]{2,1,0:T(8,128)(2,1)S(1)}, u32[]{:S(2)}, u32[]{:S(2)}) collective-permute-start(bf16[2,128,128]{2,1,0:T(8,128)(2,1)S(1)} %add_convert_fusion.2), channel_id=1, source_target_pairs={{0,128},{32,160},{64,192},{96,224},{128,0},{160,32},{192,64},{224,... | collective-permute-start | bytes 196616 | tf_op jit(solution)/shard_map/ppermute | solution.py:232
  132.5 38.7 %all-to-all-start.4 = ((bf16[64,4,512]{2,1,0:T(4,128)(2,1)}), bf16[64,4,512]{2,1,0:T(4,128)(2,1)S(1)}, u32[]{:S(2)}, u32[]{:S(2)}) async-start(bf16[64,4,512]{2,1,0:T(4,128)(2,1)} %reshape.37), calls=%async_computation.4 | async-start | bytes 524288 | tf_op jit(solution)/shard_map/all_to_all | solution.py:227
  144.1 24.0 %collective-permute-start.3 = (bf16[1,128,128]{2,1,0:T(8,128)(2,1)S(1)}, bf16[1,128,128]{2,1,0:T(8,128)(2,1)S(1)}, u32[]{:S(2)}, u32[]{:S(2)}) collective-permute-start(bf16[1,128,128]{2,1,0:T(8,128)(2,1)S(1)} %add_convert_fusion.4), channel_id=1, source_target_pairs={{0,256},{32,288},{64,320},{96,352},{128,384},{160,416},{192,448},{... | collective-permute-start | bytes 98312 | tf_op jit(solution)/shard_map/ppermute | solution.py:232
  168.8 0.9 copy-start.14
  168.8 1.0 copy-start.15

commit v5 on v4

--- a/solution.py
+++ b/solution.py
@@ -18,8 +18,8 @@
 BF16 = jnp.bfloat16
 FIRST = 96
 STAT_ROWS = 16
-VMEM_LIMIT = 18 * 2**20
-PACK_VMEM_LIMIT = 8 * 2**20
+FIRST_VMEM_LIMIT = 18 * 2**20
+LAST_VMEM_LIMIT = 56 * 2**20
 
 
 def in_vmem():
@@ -69,7 +69,6 @@
             jax.ShapeDtypeStruct((z_count, rows - FIRST, width), BF16),
             jax.ShapeDtypeStruct((y_count, 2 * src, HEAD_DIM), BF16),
         ],
-        compiler_params=pltpu.CompilerParams(vmem_limit_bytes=PACK_VMEM_LIMIT),
         name="pack_rows",
     )(
         lax.axis_index("g").reshape(1),
@@ -141,32 +140,37 @@
                 dq_acc[:, t] += dot(k_turned[:, s], dscores)
             return carry
 
+        dk_acc[...] = jnp.zeros_like(dk_acc)
+        dv_acc[...] = jnp.zeros_like(dv_acc)
         dq_acc[...] = jnp.zeros_like(dq_acc)
         lax.fori_loop(0, sources // src_tile, step, 0)
 
-    def first_kernel(main_ref, kv_ref, dk_ref, dv_ref, dq_ref, *scratch):
-        prepare(main_ref, kv_ref, None, *scratch[:-1])
-        dk_ref[...] = jnp.zeros_like(dk_ref)
-        dv_ref[...] = jnp.zeros_like(dv_ref)
-        work(*scratch[:-1], dk_ref, dv_ref, scratch[-1])
-        for z in range(z_count // 4):
-            at = slice(z * 4 * each, (z + 1) * 4 * each)
-            turned = (scratch[-1][:, at] * scale).T.astype(BF16)
-            for i in range(4):
-                dq_ref[z * 4 + i] = turned[i * each : (i + 1) * each, :]
-
-    def last_kernel(
-        me_ref, main_ref, kv_ref, last_ref, dk_in, dv_in, dq_in, send_ref, keep_ref, dkv_ref, *scratch
-    ):
-        prepare(main_ref, kv_ref, last_ref, *scratch[:-4])
-        dk_acc, dv_acc, dq_acc, dq_rows = scratch[-4:]
-        dk_acc[...] = dk_in[...]
-        dv_acc[...] = dv_in[...]
-        work(*scratch[:-4], dk_acc, dv_acc, dq_acc)
+    def first_kernel(main_ref, kv_ref, dkv_ref, dq_ref, *scratch):
+        dk_acc, dv_acc, dq_acc = scratch[-3:]
+        prepare(main_ref, kv_ref, None, *scratch[:-3])
+        work(*scratch)
         for i in range(team):
             at = slice(i * piece, (i + 1) * piece)
             dkv_ref[i, :piece, :] = (dk_acc[at, :] * scale).astype(BF16)
             dkv_ref[i, piece:, :] = dv_acc[at, :].astype(BF16)
+        for z in range(z_count // 4):
+            at = slice(z * 4 * each, (z + 1) * 4 * each)
+            turned = (dq_acc[:, at] * scale).T.astype(BF16)
+            for i in range(4):
+                dq_ref[z * 4 + i] = turned[i * each : (i + 1) * each, :]
+
+    def last_kernel(
+        me_ref, main_ref, kv_ref, last_ref, dkv_in, dq_in, send_ref, keep_ref, dkv_ref, *scratch
+    ):
+        dk_acc, dv_acc, dq_acc, dq_rows = scratch[-4:]
+        prepare(main_ref, kv_ref, last_ref, *scratch[:-4])
+        work(*scratch[:-1])
+        for i in range(team):
+            at = slice(i * piece, (i + 1) * piece)
+            dk_before = dkv_in[i, :piece, :].astype(F32)
+            dv_before = dkv_in[i, piece:, :].astype(F32)
+            dkv_ref[i, :piece, :] = (dk_acc[at, :] * scale + dk_before).astype(BF16)
+            dkv_ref[i, piece:, :] = (dv_acc[at, :] + dv_before).astype(BF16)
         for z in range(z_count // 4):
             at = slice(z * 4 * each, (z + 1) * 4 * each)
             turned = (dq_acc[:, at] * scale).T.astype(BF16)
@@ -179,7 +183,7 @@
             out[p % (z_count // 2), :FIRST, :] = dq_in[z]
             out[p % (z_count // 2), FIRST:, :] = dq_rows[z]
 
-    sums = jax.ShapeDtypeStruct((sources, dim), F32)
+    dkv = jax.ShapeDtypeStruct((team, 2 * piece, dim), BF16)
     scratch = [
         pltpu.VMEM((sources, 2 * dim), BF16),
         pltpu.VMEM((sources, 2 * dim), BF16),
@@ -188,32 +192,28 @@
         pltpu.VMEM((2 * dim, targets), BF16),
         pltpu.VMEM((targets, 2 * dim), BF16),
         pltpu.VMEM((targets, dim), BF16),
+        pltpu.VMEM((sources, dim), F32),
+        pltpu.VMEM((sources, dim), F32),
+        pltpu.VMEM((dim, targets), F32),
     ]
-    params = pltpu.CompilerParams(vmem_limit_bytes=VMEM_LIMIT)
     if last is None:
         return pl.pallas_call(
             first_kernel,
             in_specs=[in_vmem()] * 2,
-            out_specs=[in_vmem()] * 3,
-            out_shape=[sums, sums, jax.ShapeDtypeStruct((z_count, each, dim), BF16)],
-            scratch_shapes=scratch + [pltpu.VMEM((dim, targets), F32)],
-            compiler_params=params,
+            out_specs=[in_vmem()] * 2,
+            out_shape=[dkv, jax.ShapeDtypeStruct((z_count, each, dim), BF16)],
+            scratch_shapes=scratch,
+            compiler_params=pltpu.CompilerParams(vmem_limit_bytes=FIRST_VMEM_LIMIT),
             name="attention_first",
         )(main, keyvals)
     half = jax.ShapeDtypeStruct((z_count // 2, rows, dim), BF16)
     return pl.pallas_call(
         last_kernel,
-        in_specs=[pl.BlockSpec(memory_space=pltpu.SMEM)] + [in_vmem()] * 6,
+        in_specs=[pl.BlockSpec(memory_space=pltpu.SMEM)] + [in_vmem()] * 5,
         out_specs=[in_vmem()] * 3,
-        out_shape=[half, half, jax.ShapeDtypeStruct((team, 2 * piece, dim), BF16)],
-        scratch_shapes=scratch
-        + [
-            pltpu.VMEM((sources, dim), F32),
-            pltpu.VMEM((sources, dim), F32),
-            pltpu.VMEM((dim, targets), F32),
-            pltpu.VMEM((z_count, each, dim), BF16),
-        ],
-        compiler_params=params,
+        out_shape=[half, half, dkv],
+        scratch_shapes=scratch + [pltpu.VMEM((z_count, each, dim), BF16)],
+        compiler_params=pltpu.CompilerParams(vmem_limit_bytes=LAST_VMEM_LIMIT),
         name="attention_last",
     )(me, main, keyvals, last, *before)
 
@@ -233,16 +233,19 @@
 
 
 def summed_to_owner(send, keep):
-    distance = 1
-    while True:
+    for distance in (1, 2):
         arrived = swapped(send, "z", distance)
         count = keep.shape[0] // 2
-        if count == 0:
-            return keep[0].astype(F32) + arrived[0].astype(F32)
         send = (keep[count:].astype(F32) + arrived[count:].astype(F32)).astype(BF16)
-        keep, arrived = lax.optimization_barrier((keep, arrived))
-        keep = (keep[:count].astype(F32) + arrived[:count].astype(F32)).astype(BF16)
-        distance *= 2
+        if count == 4:
+            keep, arrived = lax.optimization_barrier((keep, arrived))
+        else:
+            middle = (keep[1:2].astype(F32) + arrived[1:2].astype(F32)).astype(BF16)
+            keep, arrived = lax.optimization_barrier((keep[:1], arrived[:1]))
+        keep = keep[: send.shape[0]].astype(F32) + arrived[: send.shape[0]].astype(F32)
+        keep = keep.astype(BF16) if count == 4 else keep[0]
+    arrived = [swapped(send[:1], "z", 4), swapped(middle, "z", 8), swapped(send[1:], "z", 12)]
+    return keep + sum(a[0].astype(F32) for a in arrived)
 
 
 def shards(

time: 174 us -> 177 us (1.017)
  local copies, waits for them, and re-layouts: 13.7 us -> 5.14 us
  waiting for transfers between devices: 22 us -> 30.2 us
  Pallas kernels: 14.1 us -> 18.8 us
  starting transfers between devices: 62 us -> 60.1 us
    unnamed x32 -> x24, local copies, waits for them, and re-layouts: 12 us -> 3.44 us
    all_to_all x4, waiting for transfers between devices: 3 us -> 9.69 us  [exchanged(): return lax.all_to_all(value, axes, 0, 0, tiled=True)]
    pallas_call x1, Pallas kernels: 4.15 us -> 7.21 us  [attention_backward(): pl.pallas_call(last_kernel, in_specs=[pl.BlockSpec(memory_space=pltpu.SME...]
    ppermute x4 -> x5, starting transfers between devices: 25.5 us -> 23.6 us  [swapped(): return lax.ppermute(value, axis, pairs)]
    ppermute x4 -> x5, waiting for transfers between devices: 19 us -> 20.5 us  [swapped(): return lax.ppermute(value, axis, pairs)]
  transfers between devices with their start and end apart: 8 -> 9, of which waited for: 4 -> 5; matrix products, arithmetic and copies ran while one was open for 3% -> 2% of each run, Pallas kernels for 5% -> 5%
where the time goes in v5:
time: 177 us; the launch traced here: 175 us
  starting transfers between devices  60.1 us (34%)
  blocking collectives  56.2 us (32%)
  waiting for transfers between devices  30.2 us (17%)
  Pallas kernels  18.8 us (11%)
  local copies, waits for them, and re-layouts  5.14 us (3%)
  matrix products  1.77 us (1%)
    all_gather x1, blocking collectives, shards(): main = lax.all_gather(main, 'z', axis=0, tiled=False)  36.6 us
    all_to_all x4, starting transfers between devices, exchanged(): return lax.all_to_all(value, axes, 0, 0, tiled=True)  36.6 us
    ppermute x5, starting transfers between devices, swapped(): return lax.ppermute(value, axis, pairs)  23.6 us
    ppermute x5, waiting for transfers between devices, swapped(): return lax.ppermute(value, axis, pairs)  20.5 us
    all_to_all x1, blocking collectives, exchanged(): return lax.all_to_all(value, axes, 0, 0, tiled=True)  19.6 us
    all_to_all x4, waiting for transfers between devices, exchanged(): return lax.all_to_all(value, axes, 0, 0, tiled=True)  9.69 us
    pallas_call x1, Pallas kernels, attention_backward(): pl.pallas_call(first_kernel, in_specs=[in_vmem()] * 2, out_specs=[in_vmem...  9.25 us
    pallas_call x1, Pallas kernels, attention_backward(): pl.pallas_call(last_kernel, in_specs=[pl.BlockSpec(memory_space=pltpu.SME...  7.21 us
  transfers between devices with their start and end apart: 9, of which 5 were waited for; matrix products, arithmetic and copies ran while one was open for 2% of the time, Pallas kernels for 5%

profile of v5, /device:TPU:6, one launch (start us, length us, event | category | flops | bytes accessed | tf_op | source)
XLA Modules:
  0.0 174.7 jit_solution(17206593143926412639)
XLA Ops:
  0.6 0.0 copy-start
  0.7 2.3 %pack_rows.1 = (bf16[240,128]{1,0:T(8,128)(2,1)}, bf16[16,32,128]{2,1,0:T(8,128)(2,1)}, bf16[4,1024,128]{2,1,0:T(8,128)(2,1)}) custom-call(s32[1]{0:T(128)} %bitcast.1.head_ref, bf16[128,128]{1,0:T(8,128)(2,1)} %q_ref.1, bf16[128,128]{1,0:T(8,128)(2,1)} %o_ref.1, bf16[128,128]{1,0:T(8,128)(2,1)} %do_ref.1, f32[1,128]{1,0:T(1,128)} %bitcast.25, ...), custom_call_target="tpu_custom_call" | custom-call | tf_op jit(solution)/shard_map/pack_rows/pallas_call | solution.py:63
  2.9 19.6 %all_to_all.25.kv_ref = bf16[4,1024,128]{2,1,0:T(8,128)(2,1)S(1)} all-to-all(bf16[4,1024,128]{2,1,0:T(8,128)(2,1)} %get-tuple-element.16), channel_id=1, replica_groups=mesh['z'=16,'y'=4,'g'=2,'h'=2,'c'=2] {'y'}, dimensions={0} | all-to-all | bytes 2097152 | tf_op jit(solution)/shard_map/all_to_all | solution.py:227
  22.5 0.0 copy-start.1
  22.5 15.3 %all-to-all-start.1 = ((bf16[16,32,128]{2,1,0:T(8,128)(2,1)}), bf16[16,32,128]{2,1,0:T(8,128)(2,1)S(1)}, u32[]{:S(2)}, u32[]{:S(2)}) async-start(bf16[16,32,128]{2,1,0:T(8,128)(2,1)} %get-tuple-element.17), calls=%async_computation.1 | async-start | bytes 262144 | tf_op jit(solution)/shard_map/all_to_all | solution.py:227
  37.8 0.0 copy-done.8
  37.9 36.6 %all-gather = bf16[3840,128]{1,0:T(8,128)(2,1)S(1)} all-gather(bf16[240,128]{1,0:T(8,128)(2,1)S(1)} %copy-done.8), channel_id=2, replica_groups=mesh['z'=16,'y'=4,'g'=2,'h'=2,'c'=2] {'z'}, dimensions={0}, use_global_device_ids=true | all-gather | bytes 1044480 | tf_op jit(solution)/shard_map/all_gather | solution.py:262
  74.5 9.3 %attention_first.1 = (bf16[16,256,128]{2,1,0:T(8,128)(2,1)S(1)}, bf16[16,96,128]{2,1,0:T(8,128)(2,1)S(1)}) custom-call(bf16[16,240,128]{2,1,0:T(8,128)(2,1)S(1)} %bitcast.16, bf16[4,1024,128]{2,1,0:T(8,128)(2,1)S(1)} %all_to_all.25.kv_ref), custom_call_target="tpu_custom_call" | custom-call | tf_op jit(solution)/shard_map/attention_first/pallas_call | solution.py:200
  83.8 0.0 copy-done.1
  83.8 0.0 copy-done.2
  83.8 0.0 copy-start.3
  83.8 1.0 copy-done.3
  84.8 0.8 copy-done.4
  85.6 0.0 all-to-all-done.1.last_ref
  85.6 0.7 copy-done.6
  86.2 7.2 %attention_last.1 = (bf16[8,128,128]{2,1,0:T(8,128)(2,1)}, bf16[8,128,128]{2,1,0:T(8,128)(2,1)}, bf16[16,256,128]{2,1,0:T(8,128)(2,1)}) custom-call(s32[1]{0:T(128)} %bitcast.me_ref, bf16[16,240,128]{2,1,0:T(8,128)(2,1)} %bitcast.17, bf16[4,1024,128]{2,1,0:T(8,128)(2,1)} %copy-done.1, bf16[16,32,128]{2,1,0:T(8,128)(2,1)} %copy-done.6, ...), custom_call_target="tpu_custom_call" | custom-call | tf_op jit(solution)/shard_map/attention_last/pallas_call | solution.py:210
  93.4 4.4 %all-to-all-start.2 = ((bf16[16,256,128]{2,1,0:T(8,128)(2,1)}), bf16[16,256,128]{2,1,0:T(8,128)(2,1)S(1)}, u32[]{:S(2)}, u32[]{:S(2)}) async-start(bf16[16,256,128]{2,1,0:T(8,128)(2,1)} %get-tuple-element.26), calls=%async_computation.2 | async-start | bytes 2097152 | tf_op jit(solution)/shard_map/all_to_all | solution.py:227
  97.8 0.0 copy-done.11
  97.8 3.0 %collective-permute-start = (bf16[8,128,128]{2,1,0:T(8,128)(2,1)S(1)}, bf16[8,128,128]{2,1,0:T(8,128)(2,1)S(1)}, u32[]{:S(2)}, u32[]{:S(2)}) collective-permute-start(bf16[8,128,128]{2,1,0:T(8,128)(2,1)S(1)} %copy-done.11), channel_id=1, source_target_pairs={{0,32},{32,0},{64,96},{96,64},{128,160},{160,128},{192,224},{224,1... | collective-permute-start | bytes 786440 | tf_op jit(solution)/shard_map/ppermute | solution.py:232
  100.8 7.2 %collective-permute-done = bf16[8,128,128]{2,1,0:T(8,128)(2,1)S(1)} collective-permute-done((bf16[8,128,128]{2,1,0:T(8,128)(2,1)S(1)}, bf16[8,128,128]{2,1,0:T(8,128)(2,1)S(1)}, u32[]{:S(2)}, u32[]{:S(2)}) %collective-permute-start) | collective-permute-done | bytes 262176 | tf_op jit(solution)/shard_map/ppermute | solution.py:232
  108.1 0.0 copy-done.7
  108.1 3.6 %collective-permute-start.1 = (bf16[4,128,128]{2,1,0:T(8,128)(2,1)S(1)}, bf16[4,128,128]{2,1,0:T(8,128)(2,1)S(1)}, u32[]{:S(2)}, u32[]{:S(2)}) collective-permute-start(bf16[4,128,128]{2,1,0:T(8,128)(2,1)S(1)} %add_convert_fusion), channel_id=1, source_target_pairs={{0,64},{32,96},{64,0},{96,32},{128,192},{160,224},{192,128},{224,1... | collective-permute-start | bytes 393224 | tf_op jit(solution)/shard_map/ppermute | solution.py:232
  111.7 1.5 all-to-all-done.2
  113.2 0.1 reduce_sum.21
  113.3 0.9 broadcast_in_dim.2
  114.2 5.3 %all-to-all-start.3 = ((bf16[8,256,128]{2,1,0:T(8,128)(2,1)}), bf16[8,256,128]{2,1,0:T(8,128)(2,1)S(1)}, u32[]{:S(2)}, u32[]{:S(2)}) async-start(bf16[8,256,128]{2,1,0:T(8,128)(2,1)} %broadcast_in_dim.2), calls=%async_computation.3 | async-start | bytes 1048576 | tf_op jit(solution)/shard_map/all_to_all | solution.py:227
  119.6 0.0 copy-start.5
  119.6 0.0 collective-permute-done.1
  119.6 8.2 %all-to-all-done.3 = bf16[8,256,128]{2,1,0:T(8,128)(2,1)S(1)} async-done(((bf16[8,256,128]{2,1,0:T(8,128)(2,1)}), bf16[8,256,128]{2,1,0:T(8,128)(2,1)S(1)}, u32[]{:S(2)}, u32[]{:S(2)}) %all-to-all-start.3) | async-done | bytes 524320 | tf_op jit(solution)/shard_map/all_to_all | solution.py:227
  127.8 0.0 copy-done
  127.8 0.3 fusion
  128.1 0.8 reshape.40
  128.9 11.5 %all-to-all-start.4 = ((bf16[64,4,512]{2,1,0:T(4,128)(2,1)}), bf16[64,4,512]{2,1,0:T(4,128)(2,1)S(1)}, u32[]{:S(2)}, u32[]{:S(2)}) async-start(bf16[64,4,512]{2,1,0:T(4,128)(2,1)} %reshape.40), calls=%async_computation.4 | async-start | bytes 524288 | tf_op jit(solution)/shard_map/all_to_all | solution.py:227
  140.5 7.4 %collective-permute-start.2 = (bf16[1,128,128]{2,1,0:T(8,128)(2,1)S(1)}, bf16[1,128,128]{2,1,0:T(8,128)(2,1)S(1)}, u32[]{:S(2)}, u32[]{:S(2)}) collective-permute-start(bf16[1,128,128]{2,1,0:T(8,128)(2,1)S(1)} %get-tuple-element.31), channel_id=1, source_target_pairs={{0,128},{32,160},{64,192},{96,224},{128,0},{160,32},{192,64},{224,... | collective-permute-start | bytes 98312 | tf_op jit(solution)/shard_map/ppermute | solution.py:232
  147.9 7.4 %collective-permute-start.4 = (bf16[1,128,128]{2,1,0:T(8,128)(2,1)S(1)}, bf16[1,128,128]{2,1,0:T(8,128)(2,1)S(1)}, u32[]{:S(2)}, u32[]{:S(2)}) collective-permute-start(bf16[1,128,128]{2,1,0:T(8,128)(2,1)S(1)} %get-tuple-element.32), channel_id=1, source_target_pairs={{0,384},{32,416},{64,448},{96,480},{128,256},{160,288},{192,320},{... | collective-permute-start | bytes 98312 | tf_op jit(solution)/shard_map/ppermute | solution.py:232
  155.3 2.3 %collective-permute-start.3 = (bf16[1,128,128]{2,1,0:T(8,128)(2,1)S(1)}, bf16[1,128,128]{2,1,0:T(8,128)(2,1)S(1)}, u32[]{:S(2)}, u32[]{:S(2)}) collective-permute-start(bf16[1,128,128]{2,1,0:T(8,128)(2,1)S(1)} %add_convert_fusion.3), channel_id=1, source_target_pairs={{0,256},{32,288},{64,320},{96,352},{128,384},{160,416},{192,448},{... | collective-permute-start | bytes 98312 | tf_op jit(solution)/shard_map/ppermute | solution.py:232
  157.5 0.0 copy-done.5
  157.5 0.0 slice-start
  157.6 1.3 collective-permute-done.2
  158.9 0.0 collective-permute-done.4
  158.9 11.9 %collective-permute-done.3 = bf16[1,128,128]{2,1,0:T(8,128)(2,1)S(1)} collective-permute-done((bf16[1,128,128]{2,1,0:T(8,128)(2,1)S(1)}, bf16[1,128,128]{2,1,0:T(8,128)(2,1)S(1)}, u32[]{:S(2)}, u32[]{:S(2)}) %collective-permute-start.3) | collective-permute-done | bytes 32800 | tf_op jit(solution)/shard_map/ppermute | solution.py:232
  170.8 0.0 slice-done
  170.8 0.7 add_bitcast_fusion
  171.5 0.9 copy-done.9
  172.4 0.1 copy-done.10
  172.5 1.4 fusion.1
  173.9 0.0 all-to-all-done.4
  174.0 0.7 convert_reduce_fusion
  (16 shorter events, 0.2 us)
Async XLA Ops:
  0.6 127.2 %copy-start = (bf16[512,512]{1,0:T(8,128)(2,1)S(1)}, bf16[512,512]{1,0:T(8,128)(2,1)}, u32[]{:S(2)}) copy-start(bf16[512,512]{1,0:T(8,128)(2,1)} %param.13) | copy-start | bytes 1572868
  22.5 61.3 %copy-start.1 = (bf16[4,1024,128]{2,1,0:T(8,128)(2,1)}, bf16[4,1024,128]{2,1,0:T(8,128)(2,1)S(1)}, u32[]{:S(2)}) copy-start(bf16[4,1024,128]{2,1,0:T(8,128)(2,1)S(1)} %all_to_all.25.kv_ref) | copy-start | bytes 3145732
  22.5 15.3 %copy-start.8 = (bf16[240,128]{1,0:T(8,128)(2,1)S(1)}, bf16[240,128]{1,0:T(8,128)(2,1)}, u32[]{:S(2)}) copy-start(bf16[240,128]{1,0:T(8,128)(2,1)} %get-tuple-element.15) | copy-start | bytes 184324
  22.5 63.0 %all-to-all-start.1 = ((bf16[16,32,128]{2,1,0:T(8,128)(2,1)}), bf16[16,32,128]{2,1,0:T(8,128)(2,1)S(1)}, u32[]{:S(2)}, u32[]{:S(2)}) async-start(bf16[16,32,128]{2,1,0:T(8,128)(2,1)} %get-tuple-element.17), calls=%async_computation.1 | async-start | bytes 262144 | tf_op jit(solution)/shard_map/all_to_all | solution.py:227
  74.5 9.3 %copy-start.2 = (bf16[3840,128]{1,0:T(8,128)(2,1)}, bf16[3840,128]{1,0:T(8,128)(2,1)S(1)}, u32[]{:S(2)}) copy-start(bf16[3840,128]{1,0:T(8,128)(2,1)S(1)} %all-gather) | copy-start | bytes 2949124
  83.8 1.0 copy-start.3
  84.8 0.8 copy-start.4
  85.6 0.7 copy-start.6
  93.4 4.4 %copy-start.11 = (bf16[8,128,128]{2,1,0:T(8,128)(2,1)S(1)}, bf16[8,128,128]{2,1,0:T(8,128)(2,1)}, u32[]{:S(2)}) copy-start(bf16[8,128,128]{2,1,0:T(8,128)(2,1)} %get-tuple-element.21) | copy-start | bytes 786436
  93.4 14.6 %copy-start.7 = (bf16[8,128,128]{2,1,0:T(8,128)(2,1)S(1)}, bf16[8,128,128]{2,1,0:T(8,128)(2,1)}, u32[]{:S(2)}) copy-start(bf16[8,128,128]{2,1,0:T(8,128)(2,1)} %get-tuple-element.22) | copy-start | bytes 786436
  93.4 19.8 %all-to-all-start.2 = ((bf16[16,256,128]{2,1,0:T(8,128)(2,1)}), bf16[16,256,128]{2,1,0:T(8,128)(2,1)S(1)}, u32[]{:S(2)}, u32[]{:S(2)}) async-start(bf16[16,256,128]{2,1,0:T(8,128)(2,1)} %get-tuple-element.26), calls=%async_computation.2 | async-start | bytes 2097152 | tf_op jit(solution)/shard_map/all_to_all | solution.py:227
  97.8 10.2 %collective-permute-start = (bf16[8,128,128]{2,1,0:T(8,128)(2,1)S(1)}, bf16[8,128,128]{2,1,0:T(8,128)(2,1)S(1)}, u32[]{:S(2)}, u32[]{:S(2)}) collective-permute-start(bf16[8,128,128]{2,1,0:T(8,128)(2,1)S(1)} %copy-done.11), channel_id=1, source_target_pairs={{0,32},{32,0},{64,96},{96,64},{128,160},{160,128},{192,224},{224,1... | collective-permute-start | bytes 786440 | tf_op jit(solution)/shard_map/ppermute | solution.py:232
  108.1 11.4 %collective-permute-start.1 = (bf16[4,128,128]{2,1,0:T(8,128)(2,1)S(1)}, bf16[4,128,128]{2,1,0:T(8,128)(2,1)S(1)}, u32[]{:S(2)}, u32[]{:S(2)}) collective-permute-start(bf16[4,128,128]{2,1,0:T(8,128)(2,1)S(1)} %add_convert_fusion), channel_id=1, source_target_pairs={{0,64},{32,96},{64,0},{96,32},{128,192},{160,224},{192,128},{224,1... | collective-permute-start | bytes 393224 | tf_op jit(solution)/shard_map/ppermute | solution.py:232
  114.2 13.6 %all-to-all-start.3 = ((bf16[8,256,128]{2,1,0:T(8,128)(2,1)}), bf16[8,256,128]{2,1,0:T(8,128)(2,1)S(1)}, u32[]{:S(2)}, u32[]{:S(2)}) async-start(bf16[8,256,128]{2,1,0:T(8,128)(2,1)} %broadcast_in_dim.2), calls=%async_computation.3 | async-start | bytes 1048576 | tf_op jit(solution)/shard_map/all_to_all | solution.py:227
  119.6 38.0 %copy-start.5 = (bf16[4,128,128]{2,1,0:T(8,128)(2,1)}, bf16[4,128,128]{2,1,0:T(8,128)(2,1)S(1)}, u32[]{:S(2)}) copy-start(bf16[4,128,128]{2,1,0:T(8,128)(2,1)S(1)} %add_convert_fusion.1) | copy-start | bytes 393220
  128.9 45.1 %all-to-all-start.4 = ((bf16[64,4,512]{2,1,0:T(4,128)(2,1)}), bf16[64,4,512]{2,1,0:T(4,128)(2,1)S(1)}, u32[]{:S(2)}, u32[]{:S(2)}) async-start(bf16[64,4,512]{2,1,0:T(4,128)(2,1)} %reshape.40), calls=%async_computation.4 | async-start | bytes 524288 | tf_op jit(solution)/shard_map/all_to_all | solution.py:227
  140.5 18.5 %collective-permute-start.2 = (bf16[1,128,128]{2,1,0:T(8,128)(2,1)S(1)}, bf16[1,128,128]{2,1,0:T(8,128)(2,1)S(1)}, u32[]{:S(2)}, u32[]{:S(2)}) collective-permute-start(bf16[1,128,128]{2,1,0:T(8,128)(2,1)S(1)} %get-tuple-element.31), channel_id=1, source_target_pairs={{0,128},{32,160},{64,192},{96,224},{128,0},{160,32},{192,64},{224,... | collective-permute-start | bytes 98312 | tf_op jit(solution)/shard_map/ppermute | solution.py:232
  147.9 11.1 %collective-permute-start.4 = (bf16[1,128,128]{2,1,0:T(8,128)(2,1)S(1)}, bf16[1,128,128]{2,1,0:T(8,128)(2,1)S(1)}, u32[]{:S(2)}, u32[]{:S(2)}) collective-permute-start(bf16[1,128,128]{2,1,0:T(8,128)(2,1)S(1)} %get-tuple-element.32), channel_id=1, source_target_pairs={{0,384},{32,416},{64,448},{96,480},{128,256},{160,288},{192,320},{... | collective-permute-start | bytes 98312 | tf_op jit(solution)/shard_map/ppermute | solution.py:232
  155.3 15.6 %collective-permute-start.3 = (bf16[1,128,128]{2,1,0:T(8,128)(2,1)S(1)}, bf16[1,128,128]{2,1,0:T(8,128)(2,1)S(1)}, u32[]{:S(2)}, u32[]{:S(2)}) collective-permute-start(bf16[1,128,128]{2,1,0:T(8,128)(2,1)S(1)} %add_convert_fusion.3), channel_id=1, source_target_pairs={{0,256},{32,288},{64,320},{96,352},{128,384},{160,416},{192,448},{... | collective-permute-start | bytes 98312 | tf_op jit(solution)/shard_map/ppermute | solution.py:232
  157.5 13.3 %slice-start = ((bf16[4,128,128]{2,1,0:T(8,128)(2,1)}), bf16[1,128,128]{2,1,0:T(8,128)(2,1)S(1)}, s32[]{:S(2)}) async-start(bf16[4,128,128]{2,1,0:T(8,128)(2,1)} %copy-done.5), calls=%async_computation.5 | async-start | bytes 65536 | tf_op jit(solution)/shard_map/slice | solution.py:244
  171.5 0.9 copy-start.9
  171.5 1.0 copy-start.10

commit v6 on v5

--- a/solution.py
+++ b/solution.py
@@ -20,6 +20,7 @@
 STAT_ROWS = 16
 FIRST_VMEM_LIMIT = 18 * 2**20
 LAST_VMEM_LIMIT = 56 * 2**20
+SMALL_VMEM_LIMIT = 8 * 2**20
 
 
 def in_vmem():
@@ -97,7 +98,6 @@
     src_tile, tgt_tile = (512, 512)
     team = y_count * SPLIT[3] * SPLIT[4]
     piece = sources // team
-    bits = z_count.bit_length() - 1
 
     def prepare(main_ref, kv_ref, last_ref, k_wide, v_wide, k_turned, q_turned, do_turned, q_rows, do_rows):
         lane = lax.broadcasted_iota(jnp.int32, (src, dim), 1)
@@ -176,12 +176,14 @@
             turned = (dq_acc[:, at] * scale).T.astype(BF16)
             for i in range(4):
                 dq_rows[z * 4 + i] = turned[i * each : (i + 1) * each, :]
-        for p in range(z_count):
-            turned = sum(((p >> b) & 1) << (bits - 1 - b) for b in range(bits))
-            z = jnp.bitwise_xor(me_ref[0], turned)
-            out = keep_ref if p < z_count // 2 else send_ref
-            out[p % (z_count // 2), :FIRST, :] = dq_in[z]
-            out[p % (z_count // 2), FIRST:, :] = dq_rows[z]
+        half_rows = rows // 2
+        for odd, (low_ref, high_ref) in enumerate(((keep_ref, send_ref), (send_ref, keep_ref))):
+
+            @pl.when(me_ref[0] == odd)
+            def _(low_ref=low_ref, high_ref=high_ref):
+                low_ref[...] = dq_in[:, :half_rows, :]
+                high_ref[:, : FIRST - half_rows, :] = dq_in[:, half_rows:, :]
+                high_ref[:, FIRST - half_rows :, :] = dq_rows[...]
 
     dkv = jax.ShapeDtypeStruct((team, 2 * piece, dim), BF16)
     scratch = [
@@ -206,7 +208,7 @@
             compiler_params=pltpu.CompilerParams(vmem_limit_bytes=FIRST_VMEM_LIMIT),
             name="attention_first",
         )(main, keyvals)
-    half = jax.ShapeDtypeStruct((z_count // 2, rows, dim), BF16)
+    half = jax.ShapeDtypeStruct((z_count, rows // 2, dim), BF16)
     return pl.pallas_call(
         last_kernel,
         in_specs=[pl.BlockSpec(memory_space=pltpu.SMEM)] + [in_vmem()] * 5,
@@ -232,20 +234,109 @@
     return lax.ppermute(value, axis, pairs)
 
 
-def summed_to_owner(send, keep):
-    for distance in (1, 2):
-        arrived = swapped(send, "z", distance)
-        count = keep.shape[0] // 2
-        send = (keep[count:].astype(F32) + arrived[count:].astype(F32)).astype(BF16)
-        if count == 4:
-            keep, arrived = lax.optimization_barrier((keep, arrived))
-        else:
-            middle = (keep[1:2].astype(F32) + arrived[1:2].astype(F32)).astype(BF16)
-            keep, arrived = lax.optimization_barrier((keep[:1], arrived[:1]))
-        keep = keep[: send.shape[0]].astype(F32) + arrived[: send.shape[0]].astype(F32)
-        keep = keep.astype(BF16) if count == 4 else keep[0]
-    arrived = [swapped(send[:1], "z", 4), swapped(middle, "z", 8), swapped(send[1:], "z", 12)]
-    return keep + sum(a[0].astype(F32) for a in arrived)
+def rows_by_turns(send, keep):
+    arrived = swapped(send, "z", 1)
+    count = keep.shape[1] // 2
+    mine = jnp.bitwise_and(lax.shift_right_logical(lax.axis_index("z"), 1), 1)
+
+    def part(index):
+        a, b = (jnp.where(index > 0, v[:, count:], v[:, :count]) for v in (keep, arrived))
+        return (a.astype(F32) + b.astype(F32)).astype(BF16)
+
+    send = part(1 - mine)
+    keep, arrived = lax.optimization_barrier((keep, arrived))
+    keep = part(mine)
+    return keep, swapped(send, "z", 2)
+
+
+def shuffled(value, outer, middle, inner):
+    rows = outer * middle * inner
+    new = lax.broadcasted_iota(jnp.int32, (rows, rows), 0)
+    old = lax.broadcasted_iota(jnp.int32, (rows, rows), 1)
+    m, o, i = (new // (outer * inner), new // inner % outer, new % inner)
+    take = old == (o * middle + m) * inner + i
+    return dot(jnp.where(take, 1.0, 0.0).astype(BF16), value).astype(BF16)
+
+
+def key_products(halves, source, weight_scale):
+    parts, rows, dim = halves.shape
+    z_count, y_count = (SPLIT[0], SPLIT[1])
+    own = 2 * dim // (z_count * y_count)
+
+    def kernel(halves_ref, source_ref, out_ref):
+        terms = []
+        for g in range(2):
+            key = jnp.concatenate(
+                [halves_ref[g * parts // 2 + p, : rows // 2, :] for p in range(parts // 2)], axis=0
+            )
+            terms.append(dot(key.T, source_ref[...]))
+        terms = (jnp.concatenate(terms, axis=0) * weight_scale).astype(BF16)
+        terms = shuffled(terms, z_count, y_count, own)
+        for y in range(y_count):
+            out_ref[y] = terms[y * z_count * own : (y + 1) * z_count * own, :]
+
+    return pl.pallas_call(
+        kernel,
+        in_specs=[in_vmem()] * 2,
+        out_specs=in_vmem(),
+        out_shape=jax.ShapeDtypeStruct((y_count, z_count * own, source.shape[1]), BF16),
+        compiler_params=pltpu.CompilerParams(vmem_limit_bytes=SMALL_VMEM_LIMIT),
+        name="key_products",
+    )(halves, source)
+
+
+def joined(keys, keep, arrived):
+    y_count, rows, width = keys.shape
+    z_count, quarter, dim = keep.shape
+    own = rows // z_count
+    wide = width // dim
+
+    def kernel(keys_ref, keep_ref, arrived_ref, out_ref):
+        total = sum(keys_ref[y].astype(F32) for y in range(y_count)).astype(BF16)
+        blocks = [total[:, b * dim : (b + 1) * dim] for b in range(wide)]
+        blocks = shuffled(jnp.concatenate(blocks, axis=0), wide, z_count, own)
+        dq = keep_ref[...].astype(F32) + arrived_ref[...].astype(F32)
+        out_ref[:, :quarter, :] = dq.astype(BF16)
+        for z in range(z_count):
+            out_ref[z, quarter:, :] = blocks[z * wide * own : (z + 1) * wide * own, :]
+
+    return pl.pallas_call(
+        kernel,
+        in_specs=[in_vmem()] * 3,
+        out_specs=in_vmem(),
+        out_shape=jax.ShapeDtypeStruct((z_count, quarter + wide * own, dim), BF16),
+        compiler_params=pltpu.CompilerParams(vmem_limit_bytes=SMALL_VMEM_LIMIT),
+        name="joined",
+    )(keys, keep, arrived)
+
+
+def split_sums(blocks, rows, width):
+    z_count, height, dim = blocks.shape
+    quarter = rows // 4
+    wide = width // dim
+    own = (height - quarter) // wide
+
+    def kernel(blocks_ref, dq_ref, keys_ref):
+        for turn in range(4):
+            first = turn % 2 * 2 + turn // 2
+            dq_ref[first * quarter : (first + 1) * quarter, :] = sum(
+                blocks_ref[z, :quarter, :].astype(F32) for z in range(turn, z_count, 4)
+            )
+        keys = sum(blocks_ref[z, quarter:, :].astype(F32) for z in range(z_count))
+        for b in range(wide):
+            keys_ref[:, b * dim : (b + 1) * dim] = keys[b * own : (b + 1) * own, :]
+
+    return pl.pallas_call(
+        kernel,
+        in_specs=[in_vmem()],
+        out_specs=[in_vmem()] * 2,
+        out_shape=[
+            jax.ShapeDtypeStruct((rows, dim), F32),
+            jax.ShapeDtypeStruct((own, width), F32),
+        ],
+        compiler_params=pltpu.CompilerParams(vmem_limit_bytes=SMALL_VMEM_LIMIT),
+        name="split_sums",
+    )(blocks)
 
 
 def shards(
@@ -262,20 +353,20 @@
     main = lax.all_gather(main, "z", axis=0, tiled=False)
     last = exchanged(last, "z")
     before = attention_backward(main, keyvals)
-    me = lax.axis_index("z").reshape(1)
+    me = jnp.bitwise_and(lax.axis_index("z"), 1).reshape(1)
     dq_send, dq_keep, dkv = attention_backward(main, keyvals, last, before, me)
 
     dkv = exchanged(dkv, TEAM)
     halves = added_up(dkv, tp_count)
-    halves = exchanged(halves, TP).reshape(2, tp_count // 2, 2, -1, HEAD_DIM)
+    halves = exchanged(halves, TP)
+    dq_keep, dq_arrived = rows_by_turns(dq_send, dq_keep)
+    key_terms = key_products(halves, source, weight_scale)
+    key_terms = exchanged(key_terms, "y")
+    blocks = joined(key_terms, dq_keep, dq_arrived)
+    blocks = exchanged(blocks, "z")
+    query_grad, key_grad = split_sums(blocks, queries.shape[0], source.shape[1])
+    halves = halves.reshape(2, tp_count // 2, 2, -1, HEAD_DIM)
     key_half, value_half = (halves[:, :, i].reshape(2, src, HEAD_DIM) for i in range(2))
-    query_grad = summed_to_owner(dq_send, dq_keep)
-    key_terms = lax.dot_general(
-        key_half, source, (((1,), (0,)), ((), ())), preferred_element_type=F32
-    )
-    key_terms = (key_terms * weight_scale).astype(BF16).reshape(sp_count, -1, source.shape[1])
-    key_terms = exchanged(key_terms, SP)
-    key_grad = jnp.sum(key_terms.astype(F32), axis=0)
     weights = jnp.concatenate([key_weight, value_weight], axis=1)
     source_grad = lax.dot_general(
         jnp.concatenate([key_half[0], key_half[1], value_half[0], value_half[1]], axis=1),

time: 177 us -> 169 us (0.955)
  starting transfers between devices: 60.1 us -> 45.4 us
  waiting for transfers between devices: 30.2 us -> 36.7 us
  Pallas kernels: 18.8 us -> 21.7 us
    all_to_all x4 -> x5, waiting for transfers between devices: 9.69 us -> 36.7 us  [exchanged(): return lax.all_to_all(value, axes, 0, 0, tiled=True)]
    ppermute x5 -> x2, waiting for transfers between devices: 20.5 us -> 0.01 us  [swapped(): return lax.ppermute(value, axis, pairs)]
    ppermute x5 -> x2, starting transfers between devices: 23.6 us -> 6.48 us  [swapped(): return lax.ppermute(value, axis, pairs)]
    pallas_call x0 -> x3, Pallas kernels: none -> 2.79 us  [the longest x1 1.24 us: key_products(): pl.pallas_call(kernel, in_specs=[in_vmem()] * 2, out_specs=in_vmem(), out...]
    all_to_all x4 -> x5, starting transfers between devices: 36.6 us -> 39 us  [exchanged(): return lax.all_to_all(value, axes, 0, 0, tiled=True)]
  transfers between devices with their start and end apart: 9 -> 7, of which waited for: 5 -> 4; matrix products, arithmetic and copies ran while one was open for 2% -> 2% of each run, Pallas kernels for 5% -> 6%
where the time goes in v6:
time: 169 us; the launch traced here: 167 us
  blocking collectives  56.2 us (33%)
  starting transfers between devices  45.4 us (27%)
  waiting for transfers between devices  36.7 us (22%)
  Pallas kernels  21.7 us (13%)
  local copies, waits for them, and re-layouts  4.29 us (3%)
    all_to_all x5, starting transfers between devices, exchanged(): return lax.all_to_all(value, axes, 0, 0, tiled=True)  39 us
    all_to_all x5, waiting for transfers between devices, exchanged(): return lax.all_to_all(value, axes, 0, 0, tiled=True)  36.7 us
    all_gather x1, blocking collectives, shards(): main = lax.all_gather(main, 'z', axis=0, tiled=False)  36.6 us
    all_to_all x1, blocking collectives, exchanged(): return lax.all_to_all(value, axes, 0, 0, tiled=True)  19.6 us
    pallas_call x1, Pallas kernels, attention_backward(): pl.pallas_call(first_kernel, in_specs=[in_vmem()] * 2, out_specs=[in_vmem...  9.25 us
    pallas_call x1, Pallas kernels, attention_backward(): pl.pallas_call(last_kernel, in_specs=[pl.BlockSpec(memory_space=pltpu.SME...  7.4 us
    ppermute x2, starting transfers between devices, swapped(): return lax.ppermute(value, axis, pairs)  6.48 us
    unnamed x22, local copies, waits for them, and re-layouts  3.39 us
  transfers between devices with their start and end apart: 7, of which 4 were waited for; matrix products, arithmetic and copies ran while one was open for 2% of the time, Pallas kernels for 6%

profile of v6, /device:TPU:6, one launch (start us, length us, event | category | flops | bytes accessed | tf_op | source)
XLA Modules:
  0.0 166.8 jit_solution(838276193191885320)
XLA Ops:
  0.6 2.2 %pack_rows.1 = (bf16[240,128]{1,0:T(8,128)(2,1)}, bf16[16,32,128]{2,1,0:T(8,128)(2,1)}, bf16[4,1024,128]{2,1,0:T(8,128)(2,1)}) custom-call(s32[1]{0:T(128)} %bitcast.1.head_ref, bf16[128,128]{1,0:T(8,128)(2,1)} %q_ref.1, bf16[128,128]{1,0:T(8,128)(2,1)} %o_ref.1, bf16[128,128]{1,0:T(8,128)(2,1)} %do_ref.1, f32[1,128]{1,0:T(1,128)} %bitcast.16, ...), custom_call_target="tpu_custom_call" | custom-call | tf_op jit(solution)/shard_map/pack_rows/pallas_call | solution.py:64
  2.9 19.6 %all_to_all.30.kv_ref = bf16[4,1024,128]{2,1,0:T(8,128)(2,1)S(1)} all-to-all(bf16[4,1024,128]{2,1,0:T(8,128)(2,1)} %get-tuple-element.16), channel_id=1, replica_groups=mesh['z'=16,'y'=4,'g'=2,'h'=2,'c'=2] {'y'}, dimensions={0} | all-to-all | bytes 2097152 | tf_op jit(solution)/shard_map/all_to_all | solution.py:229
  22.4 0.0 copy-start
  22.4 0.0 copy-start.7
  22.4 15.3 %all-to-all-start.1 = ((bf16[16,32,128]{2,1,0:T(8,128)(2,1)}), bf16[16,32,128]{2,1,0:T(8,128)(2,1)S(1)}, u32[]{:S(2)}, u32[]{:S(2)}) async-start(bf16[16,32,128]{2,1,0:T(8,128)(2,1)} %get-tuple-element.17), calls=%async_computation.1 | async-start | bytes 262144 | tf_op jit(solution)/shard_map/all_to_all | solution.py:229
  37.8 0.0 copy-done.7
  37.8 36.6 %all-gather = bf16[3840,128]{1,0:T(8,128)(2,1)S(1)} all-gather(bf16[240,128]{1,0:T(8,128)(2,1)S(1)} %copy-done.7), channel_id=2, replica_groups=mesh['z'=16,'y'=4,'g'=2,'h'=2,'c'=2] {'z'}, dimensions={0}, use_global_device_ids=true | all-gather | bytes 1044480 | tf_op jit(solution)/shard_map/all_gather | solution.py:353
  74.4 0.0 copy-start.1
  74.4 9.3 %attention_first.1 = (bf16[16,256,128]{2,1,0:T(8,128)(2,1)S(1)}, bf16[16,96,128]{2,1,0:T(8,128)(2,1)S(1)}) custom-call(bf16[16,240,128]{2,1,0:T(8,128)(2,1)S(1)} %bitcast.9, bf16[4,1024,128]{2,1,0:T(8,128)(2,1)S(1)} %all_to_all.30.kv_ref), custom_call_target="tpu_custom_call" | custom-call | tf_op jit(solution)/shard_map/attention_first/pallas_call | solution.py:202
  83.7 0.0 copy-done
  83.7 0.0 copy-done.1
  83.7 0.0 copy-start.2
  83.7 1.0 copy-done.2
  84.7 0.0 copy-start.4
  84.7 0.8 copy-done.4
  85.5 0.0 all-to-all-done.1.last_ref
  85.5 0.0 copy-start.6
  85.5 0.6 copy-done.6
  86.1 7.4 %attention_last.1 = (bf16[16,64,128]{2,1,0:T(8,128)(2,1)}, bf16[16,64,128]{2,1,0:T(8,128)(2,1)}, bf16[16,256,128]{2,1,0:T(8,128)(2,1)}) custom-call(s32[1]{0:T(128)} %bitcast.me_ref, bf16[16,240,128]{2,1,0:T(8,128)(2,1)} %bitcast.10, bf16[4,1024,128]{2,1,0:T(8,128)(2,1)} %copy-done, bf16[16,32,128]{2,1,0:T(8,128)(2,1)} %copy-done.6, ...), custom_call_target="tpu_custom_call" | custom-call | tf_op jit(solution)/shard_map/attention_last/pallas_call | solution.py:212
  93.5 0.0 copy-start.10
  93.5 4.4 %all-to-all-start.2 = ((bf16[16,256,128]{2,1,0:T(8,128)(2,1)}), bf16[16,256,128]{2,1,0:T(8,128)(2,1)S(1)}, u32[]{:S(2)}, u32[]{:S(2)}) async-start(bf16[16,256,128]{2,1,0:T(8,128)(2,1)} %get-tuple-element.20), calls=%async_computation.2 | async-start | bytes 2097152 | tf_op jit(solution)/shard_map/all_to_all | solution.py:229
  97.9 0.0 copy-done.10
  97.9 3.0 %collective-permute-start = (bf16[16,64,128]{2,1,0:T(8,128)(2,1)S(1)}, bf16[16,64,128]{2,1,0:T(8,128)(2,1)S(1)}, u32[]{:S(2)}, u32[]{:S(2)}) collective-permute-start(bf16[16,64,128]{2,1,0:T(8,128)(2,1)S(1)} %copy-done.10), channel_id=1, source_target_pairs={{0,32},{32,0},{64,96},{96,64},{128,160},{160,128},{192,224},{224,1... | collective-permute-start | bytes 786440 | tf_op jit(solution)/shard_map/ppermute | solution.py:234
  100.9 12.4 %all-to-all-done.2 = bf16[16,256,128]{2,1,0:T(8,128)(2,1)S(1)} async-done(((bf16[16,256,128]{2,1,0:T(8,128)(2,1)}), bf16[16,256,128]{2,1,0:T(8,128)(2,1)S(1)}, u32[]{:S(2)}, u32[]{:S(2)}) %all-to-all-start.2) | async-done | bytes 1048608 | tf_op jit(solution)/shard_map/all_to_all | solution.py:229
  113.3 0.1 reduce_sum.12
  113.4 0.9 broadcast_in_dim.2
  114.3 0.0 copy-start.5
  114.3 5.4 %all-to-all-start.3 = ((bf16[8,256,128]{2,1,0:T(8,128)(2,1)}), bf16[8,256,128]{2,1,0:T(8,128)(2,1)S(1)}, u32[]{:S(2)}, u32[]{:S(2)}) async-start(bf16[8,256,128]{2,1,0:T(8,128)(2,1)} %broadcast_in_dim.2), calls=%async_computation.3 | async-start | bytes 1048576 | tf_op jit(solution)/shard_map/all_to_all | solution.py:229
  119.7 0.0 collective-permute-done
  119.7 0.0 copy-done.5
  119.7 0.1 add_convert_fusion
  119.8 3.5 %collective-permute-start.1 = (bf16[16,32,128]{2,1,0:T(8,128)(2,1)S(1)}, bf16[16,32,128]{2,1,0:T(8,128)(2,1)S(1)}, u32[]{:S(2)}, u32[]{:S(2)}) collective-permute-start(bf16[16,32,128]{2,1,0:T(8,128)(2,1)S(1)} %add_convert_fusion), channel_id=1, source_target_pairs={{0,64},{32,96},{64,0},{96,32},{128,192},{160,224},{192,128},{224,1... | collective-permute-start | bytes 393224 | tf_op jit(solution)/shard_map/ppermute | solution.py:234
  123.3 4.6 %all-to-all-done.3.halves_ref = bf16[8,256,128]{2,1,0:T(8,128)(2,1)S(1)} async-done(((bf16[8,256,128]{2,1,0:T(8,128)(2,1)}), bf16[8,256,128]{2,1,0:T(8,128)(2,1)S(1)}, u32[]{:S(2)}, u32[]{:S(2)}) %all-to-all-start.3) | async-done | bytes 524320 | tf_op jit(solution)/shard_map/all_to_all | solution.py:229
  128.0 0.0 copy-done.3
  128.0 1.2 key_products.1
  129.2 3.4 %all-to-all-start.4 = ((bf16[4,64,512]{2,1,0:T(8,128)(2,1)}), bf16[4,64,512]{2,1,0:T(8,128)(2,1)S(1)}, u32[]{:S(2)}, u32[]{:S(2)}) async-start(bf16[4,64,512]{2,1,0:T(8,128)(2,1)} %key_products.1), calls=%async_computation.4 | async-start | bytes 524288 | tf_op jit(solution)/shard_map/all_to_all | solution.py:229
  132.6 0.1 add_convert_fusion.1.keep_ref
  132.7 0.0 collective-permute-done.1.arrived_ref
  132.7 6.6 %all-to-all-done.4.keys_ref = bf16[4,64,512]{2,1,0:T(8,128)(2,1)S(1)} async-done(((bf16[4,64,512]{2,1,0:T(8,128)(2,1)}), bf16[4,64,512]{2,1,0:T(8,128)(2,1)S(1)}, u32[]{:S(2)}, u32[]{:S(2)}) %all-to-all-start.4) | async-done | bytes 262176 | tf_op jit(solution)/shard_map/all_to_all | solution.py:229
  139.3 0.9 joined.1
  140.2 10.4 %all-to-all-start.5 = ((bf16[16,48,128]{2,1,0:T(8,128)(2,1)}), bf16[16,48,128]{2,1,0:T(8,128)(2,1)S(1)}, u32[]{:S(2)}, u32[]{:S(2)}) async-start(bf16[16,48,128]{2,1,0:T(8,128)(2,1)} %joined.1), calls=%async_computation.5 | async-start | bytes 393216 | tf_op jit(solution)/shard_map/all_to_all | solution.py:229
  150.6 0.0 copy-start.8
  150.6 0.0 copy-start.9
  150.6 0.9 copy-done.8
  151.5 0.1 copy-done.9
  151.6 1.4 fusion
  153.0 13.1 %all-to-all-done.5.blocks_ref = bf16[16,48,128]{2,1,0:T(8,128)(2,1)S(1)} async-done(((bf16[16,48,128]{2,1,0:T(8,128)(2,1)}), bf16[16,48,128]{2,1,0:T(8,128)(2,1)S(1)}, u32[]{:S(2)}, u32[]{:S(2)}) %all-to-all-start.5) | async-done | bytes 196640 | tf_op jit(solution)/shard_map/all_to_all | solution.py:229
  166.2 0.6 split_sums.1
  (2 shorter events, 0.0 us)
Async XLA Ops:
  22.4 61.3 %copy-start = (bf16[4,1024,128]{2,1,0:T(8,128)(2,1)}, bf16[4,1024,128]{2,1,0:T(8,128)(2,1)S(1)}, u32[]{:S(2)}) copy-start(bf16[4,1024,128]{2,1,0:T(8,128)(2,1)S(1)} %all_to_all.30.kv_ref) | copy-start | bytes 3145732
  22.4 15.3 %copy-start.7 = (bf16[240,128]{1,0:T(8,128)(2,1)S(1)}, bf16[240,128]{1,0:T(8,128)(2,1)}, u32[]{:S(2)}) copy-start(bf16[240,128]{1,0:T(8,128)(2,1)} %get-tuple-element.15) | copy-start | bytes 184324
  22.4 63.0 %all-to-all-start.1 = ((bf16[16,32,128]{2,1,0:T(8,128)(2,1)}), bf16[16,32,128]{2,1,0:T(8,128)(2,1)S(1)}, u32[]{:S(2)}, u32[]{:S(2)}) async-start(bf16[16,32,128]{2,1,0:T(8,128)(2,1)} %get-tuple-element.17), calls=%async_computation.1 | async-start | bytes 262144 | tf_op jit(solution)/shard_map/all_to_all | solution.py:229
  74.4 9.3 %copy-start.1 = (bf16[3840,128]{1,0:T(8,128)(2,1)}, bf16[3840,128]{1,0:T(8,128)(2,1)S(1)}, u32[]{:S(2)}) copy-start(bf16[3840,128]{1,0:T(8,128)(2,1)S(1)} %all-gather) | copy-start | bytes 2949124
  83.7 1.0 copy-start.2
  84.7 0.8 copy-start.4
  85.5 0.6 copy-start.6
  93.5 4.4 %copy-start.10 = (bf16[16,64,128]{2,1,0:T(8,128)(2,1)S(1)}, bf16[16,64,128]{2,1,0:T(8,128)(2,1)}, u32[]{:S(2)}) copy-start(bf16[16,64,128]{2,1,0:T(8,128)(2,1)} %get-tuple-element.22) | copy-start | bytes 786436
  93.5 19.8 %all-to-all-start.2 = ((bf16[16,256,128]{2,1,0:T(8,128)(2,1)}), bf16[16,256,128]{2,1,0:T(8,128)(2,1)S(1)}, u32[]{:S(2)}, u32[]{:S(2)}) async-start(bf16[16,256,128]{2,1,0:T(8,128)(2,1)} %get-tuple-element.20), calls=%async_computation.2 | async-start | bytes 2097152 | tf_op jit(solution)/shard_map/all_to_all | solution.py:229
  97.9 21.8 %collective-permute-start = (bf16[16,64,128]{2,1,0:T(8,128)(2,1)S(1)}, bf16[16,64,128]{2,1,0:T(8,128)(2,1)S(1)}, u32[]{:S(2)}, u32[]{:S(2)}) collective-permute-start(bf16[16,64,128]{2,1,0:T(8,128)(2,1)S(1)} %copy-done.10), channel_id=1, source_target_pairs={{0,32},{32,0},{64,96},{96,64},{128,160},{160,128},{192,224},{224,1... | collective-permute-start | bytes 786440 | tf_op jit(solution)/shard_map/ppermute | solution.py:234
  114.3 5.4 %copy-start.5 = (bf16[16,64,128]{2,1,0:T(8,128)(2,1)S(1)}, bf16[16,64,128]{2,1,0:T(8,128)(2,1)}, u32[]{:S(2)}) copy-start(bf16[16,64,128]{2,1,0:T(8,128)(2,1)} %get-tuple-element.23) | copy-start | bytes 786436
  114.3 13.7 %all-to-all-start.3 = ((bf16[8,256,128]{2,1,0:T(8,128)(2,1)}), bf16[8,256,128]{2,1,0:T(8,128)(2,1)S(1)}, u32[]{:S(2)}, u32[]{:S(2)}) async-start(bf16[8,256,128]{2,1,0:T(8,128)(2,1)} %broadcast_in_dim.2), calls=%async_computation.3 | async-start | bytes 1048576 | tf_op jit(solution)/shard_map/all_to_all | solution.py:229
  119.7 8.3 %copy-start.3 = (bf16[512,512]{1,0:T(8,128)(2,1)S(1)}, bf16[512,512]{1,0:T(8,128)(2,1)}, u32[]{:S(2)}) copy-start(bf16[512,512]{1,0:T(8,128)(2,1)} %source_ref.1) | copy-start | bytes 1572868
  119.8 12.9 %collective-permute-start.1 = (bf16[16,32,128]{2,1,0:T(8,128)(2,1)S(1)}, bf16[16,32,128]{2,1,0:T(8,128)(2,1)S(1)}, u32[]{:S(2)}, u32[]{:S(2)}) collective-permute-start(bf16[16,32,128]{2,1,0:T(8,128)(2,1)S(1)} %add_convert_fusion), channel_id=1, source_target_pairs={{0,64},{32,96},{64,0},{96,32},{128,192},{160,224},{192,128},{224,1... | collective-permute-start | bytes 393224 | tf_op jit(solution)/shard_map/ppermute | solution.py:234
  129.2 10.1 %all-to-all-start.4 = ((bf16[4,64,512]{2,1,0:T(8,128)(2,1)}), bf16[4,64,512]{2,1,0:T(8,128)(2,1)S(1)}, u32[]{:S(2)}, u32[]{:S(2)}) async-start(bf16[4,64,512]{2,1,0:T(8,128)(2,1)} %key_products.1), calls=%async_computation.4 | async-start | bytes 524288 | tf_op jit(solution)/shard_map/all_to_all | solution.py:229
  140.2 26.0 %all-to-all-start.5 = ((bf16[16,48,128]{2,1,0:T(8,128)(2,1)}), bf16[16,48,128]{2,1,0:T(8,128)(2,1)S(1)}, u32[]{:S(2)}, u32[]{:S(2)}) async-start(bf16[16,48,128]{2,1,0:T(8,128)(2,1)} %joined.1), calls=%async_computation.5 | async-start | bytes 393216 | tf_op jit(solution)/shard_map/all_to_all | solution.py:229
  150.6 1.0 copy-start.8
  150.6 1.0 copy-start.9

commit v7 on v6

--- a/solution.py
+++ b/solution.py
@@ -19,7 +19,7 @@
 FIRST = 96
 STAT_ROWS = 16
 FIRST_VMEM_LIMIT = 18 * 2**20
-LAST_VMEM_LIMIT = 56 * 2**20
+LAST_VMEM_LIMIT = 20 * 2**20
 SMALL_VMEM_LIMIT = 8 * 2**20
 
 
@@ -145,30 +145,26 @@
         dq_acc[...] = jnp.zeros_like(dq_acc)
         lax.fori_loop(0, sources // src_tile, step, 0)
 
-    def first_kernel(main_ref, kv_ref, dkv_ref, dq_ref, *scratch):
+    def first_kernel(main_ref, kv_ref, out_ref, *scratch):
         dk_acc, dv_acc, dq_acc = scratch[-3:]
         prepare(main_ref, kv_ref, None, *scratch[:-3])
         work(*scratch)
-        for i in range(team):
-            at = slice(i * piece, (i + 1) * piece)
-            dkv_ref[i, :piece, :] = (dk_acc[at, :] * scale).astype(BF16)
-            dkv_ref[i, piece:, :] = dv_acc[at, :].astype(BF16)
-        for z in range(z_count // 4):
-            at = slice(z * 4 * each, (z + 1) * 4 * each)
-            turned = (dq_acc[:, at] * scale).T.astype(BF16)
-            for i in range(4):
-                dq_ref[z * 4 + i] = turned[i * each : (i + 1) * each, :]
+        out_ref[:sources, :] = (dk_acc[...] * scale).astype(BF16)
+        out_ref[sources : 2 * sources, :] = dv_acc[...].astype(BF16)
+        for b in range(0, targets, dim):
+            turned = (dq_acc[:, b : b + dim] * scale).T.astype(BF16)
+            out_ref[2 * sources + b : 2 * sources + b + dim, :] = turned
 
     def last_kernel(
-        me_ref, main_ref, kv_ref, last_ref, dkv_in, dq_in, send_ref, keep_ref, dkv_ref, *scratch
+        me_ref, main_ref, kv_ref, last_ref, before_ref, send_ref, keep_ref, dkv_ref, *scratch
     ):
         dk_acc, dv_acc, dq_acc, dq_rows = scratch[-4:]
         prepare(main_ref, kv_ref, last_ref, *scratch[:-4])
         work(*scratch[:-1])
         for i in range(team):
             at = slice(i * piece, (i + 1) * piece)
-            dk_before = dkv_in[i, :piece, :].astype(F32)
-            dv_before = dkv_in[i, piece:, :].astype(F32)
+            dk_before = before_ref[at, :].astype(F32)
+            dv_before = before_ref[sources + i * piece : sources + (i + 1) * piece, :].astype(F32)
             dkv_ref[i, :piece, :] = (dk_acc[at, :] * scale + dk_before).astype(BF16)
             dkv_ref[i, piece:, :] = (dv_acc[at, :] + dv_before).astype(BF16)
         for z in range(z_count // 4):
@@ -181,11 +177,13 @@
 
             @pl.when(me_ref[0] == odd)
             def _(low_ref=low_ref, high_ref=high_ref):
-                low_ref[...] = dq_in[:, :half_rows, :]
-                high_ref[:, : FIRST - half_rows, :] = dq_in[:, half_rows:, :]
+                for z in range(z_count):
+                    at = 2 * sources + z * FIRST
+                    low_ref[z] = before_ref[at : at + half_rows, :]
+                    high_ref[z, : FIRST - half_rows, :] = before_ref[at + half_rows : at + FIRST, :]
                 high_ref[:, FIRST - half_rows :, :] = dq_rows[...]
 
-    dkv = jax.ShapeDtypeStruct((team, 2 * piece, dim), BF16)
+    dkv = pltpu.MemorySpace.HBM((team, 2 * piece, dim), BF16)
     scratch = [
         pltpu.VMEM((sources, 2 * dim), BF16),
         pltpu.VMEM((sources, 2 * dim), BF16),
@@ -202,22 +200,22 @@
         return pl.pallas_call(
             first_kernel,
             in_specs=[in_vmem()] * 2,
-            out_specs=[in_vmem()] * 2,
-            out_shape=[dkv, jax.ShapeDtypeStruct((z_count, each, dim), BF16)],
+            out_specs=in_vmem(),
+            out_shape=jax.ShapeDtypeStruct((2 * sources + targets, dim), BF16),
             scratch_shapes=scratch,
             compiler_params=pltpu.CompilerParams(vmem_limit_bytes=FIRST_VMEM_LIMIT),
             name="attention_first",
         )(main, keyvals)
-    half = jax.ShapeDtypeStruct((z_count, rows // 2, dim), BF16)
+    half = pltpu.MemorySpace.HBM((z_count, rows // 2, dim), BF16)
     return pl.pallas_call(
         last_kernel,
-        in_specs=[pl.BlockSpec(memory_space=pltpu.SMEM)] + [in_vmem()] * 5,
+        in_specs=[pl.BlockSpec(memory_space=pltpu.SMEM)] + [in_vmem()] * 4,
         out_specs=[in_vmem()] * 3,
         out_shape=[half, half, dkv],
         scratch_shapes=scratch + [pltpu.VMEM((z_count, each, dim), BF16)],
         compiler_params=pltpu.CompilerParams(vmem_limit_bytes=LAST_VMEM_LIMIT),
         name="attention_last",
-    )(me, main, keyvals, last, *before)
+    )(me, main, keyvals, last, before)
 
 
 def added_up(arrived, copies):
@@ -236,17 +234,19 @@
 
 def rows_by_turns(send, keep):
     arrived = swapped(send, "z", 1)
-    count = keep.shape[1] // 2
-    mine = jnp.bitwise_and(lax.shift_right_logical(lax.axis_index("z"), 1), 1)
-
-    def part(index):
-        a, b = (jnp.where(index > 0, v[:, count:], v[:, :count]) for v in (keep, arrived))
-        return (a.astype(F32) + b.astype(F32)).astype(BF16)
-
-    send = part(1 - mine)
-    keep, arrived = lax.optimization_barrier((keep, arrived))
-    keep = part(mine)
-    return keep, swapped(send, "z", 2)
+    for distance in (1, 2):
+        count = keep.shape[1] // 2
+        mine = jnp.bitwise_and(lax.axis_index("z"), 2 * distance)
+
+        def part(first):
+            a, b = (jnp.where(first, v[:, :count], v[:, count:]) for v in (keep, arrived))
+            return (a.astype(F32) + b.astype(F32)).astype(BF16)
+
+        send = part(mine > 0)
+        keep, arrived = lax.optimization_barrier((keep, arrived))
+        keep = part(mine == 0)
+        arrived = swapped(send, "z", 2 * distance)
+    return keep, arrived
 
 
 def shuffled(value, outer, middle, inner):
@@ -287,7 +287,7 @@
 
 def joined(keys, keep, arrived):
     y_count, rows, width = keys.shape
-    z_count, quarter, dim = keep.shape
+    z_count, share, dim = keep.shape
     own = rows // z_count
     wide = width // dim
 
@@ -296,15 +296,15 @@
         blocks = [total[:, b * dim : (b + 1) * dim] for b in range(wide)]
         blocks = shuffled(jnp.concatenate(blocks, axis=0), wide, z_count, own)
         dq = keep_ref[...].astype(F32) + arrived_ref[...].astype(F32)
-        out_ref[:, :quarter, :] = dq.astype(BF16)
+        out_ref[:, :share, :] = dq.astype(BF16)
         for z in range(z_count):
-            out_ref[z, quarter:, :] = blocks[z * wide * own : (z + 1) * wide * own, :]
+            out_ref[z, share:, :] = blocks[z * wide * own : (z + 1) * wide * own, :]
 
     return pl.pallas_call(
         kernel,
         in_specs=[in_vmem()] * 3,
         out_specs=in_vmem(),
-        out_shape=jax.ShapeDtypeStruct((z_count, quarter + wide * own, dim), BF16),
+        out_shape=jax.ShapeDtypeStruct((z_count, share + wide * own, dim), BF16),
         compiler_params=pltpu.CompilerParams(vmem_limit_bytes=SMALL_VMEM_LIMIT),
         name="joined",
     )(keys, keep, arrived)
@@ -312,17 +312,17 @@
 
 def split_sums(blocks, rows, width):
     z_count, height, dim = blocks.shape
-    quarter = rows // 4
+    share = rows // 8
     wide = width // dim
-    own = (height - quarter) // wide
+    own = (height - share) // wide
 
     def kernel(blocks_ref, dq_ref, keys_ref):
-        for turn in range(4):
-            first = turn % 2 * 2 + turn // 2
-            dq_ref[first * quarter : (first + 1) * quarter, :] = sum(
-                blocks_ref[z, :quarter, :].astype(F32) for z in range(turn, z_count, 4)
+        for turn in range(8):
+            first = turn % 2 * 4 + turn // 2 % 2 * 2 + turn // 4
+            dq_ref[first * share : (first + 1) * share, :] = sum(
+                blocks_ref[z, :share, :].astype(F32) for z in range(turn, z_count, 8)
             )
-        keys = sum(blocks_ref[z, quarter:, :].astype(F32) for z in range(z_count))
+        keys = sum(blocks_ref[z, share:, :].astype(F32) for z in range(z_count))
         for b in range(wide):
             keys_ref[:, b * dim : (b + 1) * dim] = keys[b * own : (b + 1) * own, :]
 

time: 169 us -> 163 us (0.964)
  waiting for transfers between devices: 36.7 us -> 29 us
  starting transfers between devices: 45.4 us -> 51.6 us
  local copies, waits for them, and re-layouts: 4.29 us -> 0.92 us
    all_to_all x5, waiting for transfers between devices: 36.7 us -> 20.5 us  [exchanged(): return lax.all_to_all(value, axes, 0, 0, tiled=True)]
    ppermute x2 -> x3, waiting for transfers between devices: 0.01 us -> 8.52 us  [swapped(): return lax.ppermute(value, axis, pairs)]
    ppermute x2 -> x3, starting transfers between devices: 6.48 us -> 12.9 us  [swapped(): return lax.ppermute(value, axis, pairs)]
    unnamed x22 -> x12, local copies, waits for them, and re-layouts: 3.39 us -> 0.02 us
  transfers between devices with their start and end apart: 7 -> 8, of which waited for: 4 -> 6; matrix products, arithmetic and copies ran while one was open for 2% -> 2% of each run, Pallas kernels for 6% -> 7%
where the time goes in v7:
time: 163 us; the launch traced here: 161 us
  blocking collectives  56.4 us (35%)
  starting transfers between devices  51.6 us (32%)
  waiting for transfers between devices  29 us (18%)
  Pallas kernels  20.6 us (13%)
    all_to_all x5, starting transfers between devices, exchanged(): return lax.all_to_all(value, axes, 0, 0, tiled=True)  38.8 us
    all_gather x1, blocking collectives, shards(): main = lax.all_gather(main, 'z', axis=0, tiled=False)  36.7 us
    all_to_all x5, waiting for transfers between devices, exchanged(): return lax.all_to_all(value, axes, 0, 0, tiled=True)  20.5 us
    all_to_all x1, blocking collectives, exchanged(): return lax.all_to_all(value, axes, 0, 0, tiled=True)  19.7 us
    ppermute x3, starting transfers between devices, swapped(): return lax.ppermute(value, axis, pairs)  12.9 us
    pallas_call x1, Pallas kernels, attention_backward(): pl.pallas_call(first_kernel, in_specs=[in_vmem()] * 2, out_specs=in_vmem(...  9.3 us
    ppermute x3, waiting for transfers between devices, swapped(): return lax.ppermute(value, axis, pairs)  8.52 us
    pallas_call x1, Pallas kernels, attention_backward(): pl.pallas_call(last_kernel, in_specs=[pl.BlockSpec(memory_space=pltpu.SME...  6.33 us
  transfers between devices with their start and end apart: 8, of which 6 were waited for; matrix products, arithmetic and copies ran while one was open for 2% of the time, Pallas kernels for 7%

profile of v7, /device:TPU:6, one launch (start us, length us, event | category | flops | bytes accessed | tf_op | source)
XLA Modules:
  0.0 161.2 jit_solution(15692550695462893029)
XLA Ops:
  0.6 2.2 %pack_rows.1 = (bf16[240,128]{1,0:T(8,128)(2,1)}, bf16[16,32,128]{2,1,0:T(8,128)(2,1)}, bf16[4,1024,128]{2,1,0:T(8,128)(2,1)}) custom-call(s32[1]{0:T(128)} %bitcast.1.head_ref, bf16[128,128]{1,0:T(8,128)(2,1)} %q_ref.1, bf16[128,128]{1,0:T(8,128)(2,1)} %o_ref.1, bf16[128,128]{1,0:T(8,128)(2,1)} %do_ref.1, f32[1,128]{1,0:T(1,128)} %bitcast.16, ...), custom_call_target="tpu_custom_call" | custom-call | tf_op jit(solution)/shard_map/pack_rows/pallas_call | solution.py:64
  2.9 0.0 copy-start.2
  2.9 19.7 %all_to_all.30.kv_ref = bf16[4,1024,128]{2,1,0:T(8,128)(2,1)S(1)} all-to-all(bf16[4,1024,128]{2,1,0:T(8,128)(2,1)} %get-tuple-element.16), channel_id=1, replica_groups=mesh['z'=16,'y'=4,'g'=2,'h'=2,'c'=2] {'y'}, dimensions={0} | all-to-all | bytes 2097152 | tf_op jit(solution)/shard_map/all_to_all | solution.py:227
  22.6 15.2 %all-to-all-start.1 = ((bf16[16,32,128]{2,1,0:T(8,128)(2,1)}), bf16[16,32,128]{2,1,0:T(8,128)(2,1)}, u32[]{:S(2)}, u32[]{:S(2)}) async-start(bf16[16,32,128]{2,1,0:T(8,128)(2,1)} %get-tuple-element.17), calls=%async_computation.1 | async-start | bytes 262144 | tf_op jit(solution)/shard_map/all_to_all | solution.py:227
  37.8 0.0 copy-done.2
  37.8 36.7 %all-gather = bf16[3840,128]{1,0:T(8,128)(2,1)S(1)} all-gather(bf16[240,128]{1,0:T(8,128)(2,1)S(1)} %copy-done.2), channel_id=2, replica_groups=mesh['z'=16,'y'=4,'g'=2,'h'=2,'c'=2] {'z'}, dimensions={0}, use_global_device_ids=true | all-gather | bytes 1044480 | tf_op jit(solution)/shard_map/all_gather | solution.py:353
  74.5 9.3 %attention_first.1.before_ref = bf16[5632,128]{1,0:T(8,128)(2,1)S(1)} custom-call(bf16[16,240,128]{2,1,0:T(8,128)(2,1)S(1)} %bitcast.9, bf16[4,1024,128]{2,1,0:T(8,128)(2,1)S(1)} %all_to_all.30.kv_ref), custom_call_target="tpu_custom_call" | custom-call | tf_op jit(solution)/shard_map/attention_first/pallas_call | solution.py:200
  83.8 0.0 all-to-all-done.1.last_ref
  83.9 6.3 %attention_last.1 = (bf16[16,64,128]{2,1,0:T(8,128)(2,1)}, bf16[16,64,128]{2,1,0:T(8,128)(2,1)}, bf16[16,256,128]{2,1,0:T(8,128)(2,1)}) custom-call(s32[1]{0:T(128)} %bitcast.me_ref, bf16[16,240,128]{2,1,0:T(8,128)(2,1)S(1)} %bitcast.10, bf16[4,1024,128]{2,1,0:T(8,128)(2,1)S(1)} %all_to_all.30.kv_ref, bf16[16,32,128]{2,1,0:T(8,128)(2,1)} %all-to-all-done.1.last_ref, ...), custom_call_target="tpu_custom_call" | custom-call | tf_op jit(solution)/shard_map/attention_last/pallas_call | solution.py:210
  90.2 0.0 copy-start.5
  90.2 0.0 copy-start.1
  90.2 4.4 %all-to-all-start.2 = ((bf16[16,256,128]{2,1,0:T(8,128)(2,1)}), bf16[16,256,128]{2,1,0:T(8,128)(2,1)S(1)}, u32[]{:S(2)}, u32[]{:S(2)}) async-start(bf16[16,256,128]{2,1,0:T(8,128)(2,1)} %get-tuple-element.18), calls=%async_computation.2 | async-start | bytes 2097152 | tf_op jit(solution)/shard_map/all_to_all | solution.py:227
  94.6 0.0 copy-done.5
  94.6 2.9 %collective-permute-start = (bf16[16,64,128]{2,1,0:T(8,128)(2,1)S(1)}, bf16[16,64,128]{2,1,0:T(8,128)(2,1)S(1)}, u32[]{:S(2)}, u32[]{:S(2)}) collective-permute-start(bf16[16,64,128]{2,1,0:T(8,128)(2,1)S(1)} %copy-done.5), channel_id=1, source_target_pairs={{0,32},{32,0},{64,96},{96,64},{128,160},{160,128},{192,224},{224,1... | collective-permute-start | bytes 786440 | tf_op jit(solution)/shard_map/ppermute | solution.py:232
  97.5 7.3 %collective-permute-done = bf16[16,64,128]{2,1,0:T(8,128)(2,1)S(1)} collective-permute-done((bf16[16,64,128]{2,1,0:T(8,128)(2,1)S(1)}, bf16[16,64,128]{2,1,0:T(8,128)(2,1)S(1)}, u32[]{:S(2)}, u32[]{:S(2)}) %collective-permute-start) | collective-permute-done | bytes 262176 | tf_op jit(solution)/shard_map/ppermute | solution.py:232
  104.8 0.0 copy-done.1
  104.8 0.1 add_convert_fusion
  104.9 3.4 %collective-permute-start.1 = (bf16[16,32,128]{2,1,0:T(8,128)(2,1)S(1)}, bf16[16,32,128]{2,1,0:T(8,128)(2,1)S(1)}, u32[]{:S(2)}, u32[]{:S(2)}) collective-permute-start(bf16[16,32,128]{2,1,0:T(8,128)(2,1)S(1)} %add_convert_fusion), channel_id=1, source_target_pairs={{0,64},{32,96},{64,0},{96,32},{128,192},{160,224},{192,128},{224,1... | collective-permute-start | bytes 393224 | tf_op jit(solution)/shard_map/ppermute | solution.py:232
  108.4 1.6 all-to-all-done.2
  110.0 0.1 reduce_sum.12
  110.1 0.0 copy-start
  110.1 0.9 broadcast_in_dim.2
  111.0 5.3 %all-to-all-start.3 = ((bf16[8,256,128]{2,1,0:T(8,128)(2,1)}), bf16[8,256,128]{2,1,0:T(8,128)(2,1)S(1)}, u32[]{:S(2)}, u32[]{:S(2)}) async-start(bf16[8,256,128]{2,1,0:T(8,128)(2,1)} %broadcast_in_dim.2), calls=%async_computation.3 | async-start | bytes 1048576 | tf_op jit(solution)/shard_map/all_to_all | solution.py:227
  116.3 0.1 add_convert_fusion.1
  116.4 0.0 collective-permute-done.1
  116.4 6.6 %collective-permute-start.2 = (bf16[16,16,128]{2,1,0:T(8,128)(2,1)S(1)}, bf16[16,16,128]{2,1,0:T(8,128)(2,1)S(1)}, u32[]{:S(2)}, u32[]{:S(2)}) collective-permute-start(bf16[16,16,128]{2,1,0:T(8,128)(2,1)S(1)} %add_convert_fusion.2), channel_id=1, source_target_pairs={{0,128},{32,160},{64,192},{96,224},{128,0},{160,32},{192,64},{224,... | collective-permute-start | bytes 196616 | tf_op jit(solution)/shard_map/ppermute | solution.py:232
  123.0 1.5 all-to-all-done.3.halves_ref
  124.5 0.0 copy-done
  124.5 1.2 key_products.1
  125.8 0.0 copy-start.3
  125.8 0.0 copy-start.4
  125.8 3.5 %all-to-all-start.4 = ((bf16[4,64,512]{2,1,0:T(8,128)(2,1)}), bf16[4,64,512]{2,1,0:T(8,128)(2,1)S(1)}, u32[]{:S(2)}, u32[]{:S(2)}) async-start(bf16[4,64,512]{2,1,0:T(8,128)(2,1)} %key_products.1), calls=%async_computation.4 | async-start | bytes 524288 | tf_op jit(solution)/shard_map/all_to_all | solution.py:227
  129.4 1.2 collective-permute-done.2.arrived_ref
  130.6 5.4 %all-to-all-done.4.keys_ref = bf16[4,64,512]{2,1,0:T(8,128)(2,1)S(1)} async-done(((bf16[4,64,512]{2,1,0:T(8,128)(2,1)}), bf16[4,64,512]{2,1,0:T(8,128)(2,1)S(1)}, u32[]{:S(2)}, u32[]{:S(2)}) %all-to-all-start.4) | async-done | bytes 262176 | tf_op jit(solution)/shard_map/all_to_all | solution.py:227
  136.0 0.9 joined.1
  136.8 10.3 %all-to-all-start.5 = ((bf16[16,32,128]{2,1,0:T(8,128)(2,1)}), bf16[16,32,128]{2,1,0:T(8,128)(2,1)S(1)}, u32[]{:S(2)}, u32[]{:S(2)}) async-start(bf16[16,32,128]{2,1,0:T(8,128)(2,1)} %joined.1), calls=%async_computation.5 | async-start | bytes 262144 | tf_op jit(solution)/shard_map/all_to_all | solution.py:227
  147.2 0.0 copy-done.3
  147.2 0.0 copy-done.4
  147.2 1.4 fusion
  148.6 11.9 %all-to-all-done.5.blocks_ref = bf16[16,32,128]{2,1,0:T(8,128)(2,1)S(1)} async-done(((bf16[16,32,128]{2,1,0:T(8,128)(2,1)}), bf16[16,32,128]{2,1,0:T(8,128)(2,1)S(1)}, u32[]{:S(2)}, u32[]{:S(2)}) %all-to-all-start.5) | async-done | bytes 131104 | tf_op jit(solution)/shard_map/all_to_all | solution.py:227
  160.5 0.6 split_sums.1
  (3 shorter events, 0.1 us)
Async XLA Ops:
  2.9 35.0 %copy-start.2 = (bf16[240,128]{1,0:T(8,128)(2,1)S(1)}, bf16[240,128]{1,0:T(8,128)(2,1)}, u32[]{:S(2)}) copy-start(bf16[240,128]{1,0:T(8,128)(2,1)} %get-tuple-element.15) | copy-start | bytes 184324
  22.6 61.3 %all-to-all-start.1 = ((bf16[16,32,128]{2,1,0:T(8,128)(2,1)}), bf16[16,32,128]{2,1,0:T(8,128)(2,1)}, u32[]{:S(2)}, u32[]{:S(2)}) async-start(bf16[16,32,128]{2,1,0:T(8,128)(2,1)} %get-tuple-element.17), calls=%async_computation.1 | async-start | bytes 262144 | tf_op jit(solution)/shard_map/all_to_all | solution.py:227
  90.2 4.4 %copy-start.5 = (bf16[16,64,128]{2,1,0:T(8,128)(2,1)S(1)}, bf16[16,64,128]{2,1,0:T(8,128)(2,1)}, u32[]{:S(2)}) copy-start(bf16[16,64,128]{2,1,0:T(8,128)(2,1)} %get-tuple-element.20) | copy-start | bytes 786436
  90.2 14.6 %copy-start.1 = (bf16[16,64,128]{2,1,0:T(8,128)(2,1)S(1)}, bf16[16,64,128]{2,1,0:T(8,128)(2,1)}, u32[]{:S(2)}) copy-start(bf16[16,64,128]{2,1,0:T(8,128)(2,1)} %get-tuple-element.21) | copy-start | bytes 786436
  90.2 19.8 %all-to-all-start.2 = ((bf16[16,256,128]{2,1,0:T(8,128)(2,1)}), bf16[16,256,128]{2,1,0:T(8,128)(2,1)S(1)}, u32[]{:S(2)}, u32[]{:S(2)}) async-start(bf16[16,256,128]{2,1,0:T(8,128)(2,1)} %get-tuple-element.18), calls=%async_computation.2 | async-start | bytes 2097152 | tf_op jit(solution)/shard_map/all_to_all | solution.py:227
  94.6 10.2 %collective-permute-start = (bf16[16,64,128]{2,1,0:T(8,128)(2,1)S(1)}, bf16[16,64,128]{2,1,0:T(8,128)(2,1)S(1)}, u32[]{:S(2)}, u32[]{:S(2)}) collective-permute-start(bf16[16,64,128]{2,1,0:T(8,128)(2,1)S(1)} %copy-done.5), channel_id=1, source_target_pairs={{0,32},{32,0},{64,96},{96,64},{128,160},{160,128},{192,224},{224,1... | collective-permute-start | bytes 786440 | tf_op jit(solution)/shard_map/ppermute | solution.py:232
  104.9 11.5 %collective-permute-start.1 = (bf16[16,32,128]{2,1,0:T(8,128)(2,1)S(1)}, bf16[16,32,128]{2,1,0:T(8,128)(2,1)S(1)}, u32[]{:S(2)}, u32[]{:S(2)}) collective-permute-start(bf16[16,32,128]{2,1,0:T(8,128)(2,1)S(1)} %add_convert_fusion), channel_id=1, source_target_pairs={{0,64},{32,96},{64,0},{96,32},{128,192},{160,224},{192,128},{224,1... | collective-permute-start | bytes 393224 | tf_op jit(solution)/shard_map/ppermute | solution.py:232
  110.1 14.4 %copy-start = (bf16[512,512]{1,0:T(8,128)(2,1)S(1)}, bf16[512,512]{1,0:T(8,128)(2,1)}, u32[]{:S(2)}) copy-start(bf16[512,512]{1,0:T(8,128)(2,1)} %source_ref.1) | copy-start | bytes 1572868
  111.0 13.6 %all-to-all-start.3 = ((bf16[8,256,128]{2,1,0:T(8,128)(2,1)}), bf16[8,256,128]{2,1,0:T(8,128)(2,1)S(1)}, u32[]{:S(2)}, u32[]{:S(2)}) async-start(bf16[8,256,128]{2,1,0:T(8,128)(2,1)} %broadcast_in_dim.2), calls=%async_computation.3 | async-start | bytes 1048576 | tf_op jit(solution)/shard_map/all_to_all | solution.py:227
  116.4 14.1 %collective-permute-start.2 = (bf16[16,16,128]{2,1,0:T(8,128)(2,1)S(1)}, bf16[16,16,128]{2,1,0:T(8,128)(2,1)S(1)}, u32[]{:S(2)}, u32[]{:S(2)}) collective-permute-start(bf16[16,16,128]{2,1,0:T(8,128)(2,1)S(1)} %add_convert_fusion.2), channel_id=1, source_target_pairs={{0,128},{32,160},{64,192},{96,224},{128,0},{160,32},{192,64},{224,... | collective-permute-start | bytes 196616 | tf_op jit(solution)/shard_map/ppermute | solution.py:232
  125.8 21.4 %copy-start.3 = (bf16[512,256]{1,0:T(8,128)(2,1)S(1)}, bf16[512,256]{1,0:T(8,128)(2,1)}, u32[]{:S(2)}) copy-start(bf16[512,256]{1,0:T(8,128)(2,1)} %param.17) | copy-start | bytes 786436
  125.8 21.4 %copy-start.4 = (bf16[512,256]{1,0:T(8,128)(2,1)S(1)}, bf16[512,256]{1,0:T(8,128)(2,1)}, u32[]{:S(2)}) copy-start(bf16[512,256]{1,0:T(8,128)(2,1)} %param.16) | copy-start | bytes 786436
  125.8 10.2 %all-to-all-start.4 = ((bf16[4,64,512]{2,1,0:T(8,128)(2,1)}), bf16[4,64,512]{2,1,0:T(8,128)(2,1)S(1)}, u32[]{:S(2)}, u32[]{:S(2)}) async-start(bf16[4,64,512]{2,1,0:T(8,128)(2,1)} %key_products.1), calls=%async_computation.4 | async-start | bytes 524288 | tf_op jit(solution)/shard_map/all_to_all | solution.py:227
  136.8 23.7 %all-to-all-start.5 = ((bf16[16,32,128]{2,1,0:T(8,128)(2,1)}), bf16[16,32,128]{2,1,0:T(8,128)(2,1)S(1)}, u32[]{:S(2)}, u32[]{:S(2)}) async-start(bf16[16,32,128]{2,1,0:T(8,128)(2,1)} %joined.1), calls=%async_computation.5 | async-start | bytes 262144 | tf_op jit(solution)/shard_map/all_to_all | solution.py:227

commit v8 on v7

--- a/solution.py
+++ b/solution.py
@@ -18,8 +18,8 @@
 BF16 = jnp.bfloat16
 FIRST = 96
 STAT_ROWS = 16
-FIRST_VMEM_LIMIT = 18 * 2**20
-LAST_VMEM_LIMIT = 20 * 2**20
+FIRST_VMEM_LIMIT = 24 * 2**20
+LAST_VMEM_LIMIT = 24 * 2**20
 SMALL_VMEM_LIMIT = 8 * 2**20
 
 
@@ -95,7 +95,7 @@
     sources, targets = (y_count * src, z_count * each)
     scale = 1.0 / math.sqrt(HEAD_DIM)
     exp_scale = math.log2(math.e) * scale
-    src_tile, tgt_tile = (512, 512)
+    src_tile, tgt_tile = (1024, 512)
     team = y_count * SPLIT[3] * SPLIT[4]
     piece = sources // team
 
@@ -219,8 +219,21 @@
 
 
 def added_up(arrived, copies):
-    total = jnp.sum(arrived.astype(F32), axis=0).astype(BF16)
-    return jnp.broadcast_to(total[None], (copies, *total.shape))
+    count, rows, width = arrived.shape
+
+    def kernel(arrived_ref, out_ref):
+        total = sum(arrived_ref[i].astype(F32) for i in range(count)).astype(BF16)
+        for i in range(copies):
+            out_ref[i] = total
+
+    return pl.pallas_call(
+        kernel,
+        in_specs=[in_vmem()],
+        out_specs=in_vmem(),
+        out_shape=pltpu.MemorySpace.HBM((copies, rows, width), BF16),
+        compiler_params=pltpu.CompilerParams(vmem_limit_bytes=SMALL_VMEM_LIMIT),
+        name="added_up",
+    )(arrived)
 
 
 def exchanged(value, axes):

time: 163 us -> 162 us (level)
  transfers between devices with their start and end apart: 8 -> 8, of which waited for: 6 -> 6; matrix products, arithmetic and copies ran while one was open for 2% -> 1% of each run, Pallas kernels for 7% -> 7%
where the time goes in v8:
time: 162 us; the launch traced here: 160 us
  blocking collectives  56.4 us (35%)
  starting transfers between devices  51.8 us (32%)
  waiting for transfers between devices  28.9 us (18%)
  Pallas kernels  20.9 us (13%)
    all_to_all x5, starting transfers between devices, exchanged(): return lax.all_to_all(value, axes, 0, 0, tiled=True)  38.8 us
    all_gather x1, blocking collectives, shards(): main = lax.all_gather(main, 'z', axis=0, tiled=False)  36.7 us
    all_to_all x5, waiting for transfers between devices, exchanged(): return lax.all_to_all(value, axes, 0, 0, tiled=True)  20.3 us
    all_to_all x1, blocking collectives, exchanged(): return lax.all_to_all(value, axes, 0, 0, tiled=True)  19.7 us
    ppermute x3, starting transfers between devices, swapped(): return lax.ppermute(value, axis, pairs)  13 us
    pallas_call x1, Pallas kernels, attention_backward(): pl.pallas_call(first_kernel, in_specs=[in_vmem()] * 2, out_specs=in_vmem(...  8.95 us
    ppermute x3, waiting for transfers between devices, swapped(): return lax.ppermute(value, axis, pairs)  8.53 us
    pallas_call x1, Pallas kernels, attention_backward(): pl.pallas_call(last_kernel, in_specs=[pl.BlockSpec(memory_space=pltpu.SME...  5.99 us
  transfers between devices with their start and end apart: 8, of which 6 were waited for; matrix products, arithmetic and copies ran while one was open for 1% of the time, Pallas kernels for 7%

profile of v8, /device:TPU:6, one launch (start us, length us, event | category | flops | bytes accessed | tf_op | source)
XLA Modules:
  0.0 160.4 jit_solution(4744488186557297546)
XLA Ops:
  0.6 2.2 %pack_rows.1 = (bf16[240,128]{1,0:T(8,128)(2,1)}, bf16[16,32,128]{2,1,0:T(8,128)(2,1)}, bf16[4,1024,128]{2,1,0:T(8,128)(2,1)}) custom-call(s32[1]{0:T(128)} %bitcast.1.head_ref, bf16[128,128]{1,0:T(8,128)(2,1)} %q_ref.1, bf16[128,128]{1,0:T(8,128)(2,1)} %o_ref.1, bf16[128,128]{1,0:T(8,128)(2,1)} %do_ref.1, f32[1,128]{1,0:T(1,128)} %bitcast.16, ...), custom_call_target="tpu_custom_call" | custom-call | tf_op jit(solution)/shard_map/pack_rows/pallas_call | solution.py:64
  2.9 0.0 copy-start.2
  2.9 19.7 %all_to_all.30.kv_ref = bf16[4,1024,128]{2,1,0:T(8,128)(2,1)S(1)} all-to-all(bf16[4,1024,128]{2,1,0:T(8,128)(2,1)} %get-tuple-element.16), channel_id=1, replica_groups=mesh['z'=16,'y'=4,'g'=2,'h'=2,'c'=2] {'y'}, dimensions={0} | all-to-all | bytes 2097152 | tf_op jit(solution)/shard_map/all_to_all | solution.py:240
  22.6 15.2 %all-to-all-start.1 = ((bf16[16,32,128]{2,1,0:T(8,128)(2,1)}), bf16[16,32,128]{2,1,0:T(8,128)(2,1)}, u32[]{:S(2)}, u32[]{:S(2)}) async-start(bf16[16,32,128]{2,1,0:T(8,128)(2,1)} %get-tuple-element.17), calls=%async_computation.1 | async-start | bytes 262144 | tf_op jit(solution)/shard_map/all_to_all | solution.py:240
  37.8 0.0 copy-done.2
  37.8 36.7 %all-gather = bf16[3840,128]{1,0:T(8,128)(2,1)S(1)} all-gather(bf16[240,128]{1,0:T(8,128)(2,1)S(1)} %copy-done.2), channel_id=2, replica_groups=mesh['z'=16,'y'=4,'g'=2,'h'=2,'c'=2] {'z'}, dimensions={0}, use_global_device_ids=true | all-gather | bytes 1044480 | tf_op jit(solution)/shard_map/all_gather | solution.py:366
  74.5 9.0 %attention_first.1.before_ref = bf16[5632,128]{1,0:T(8,128)(2,1)S(1)} custom-call(bf16[16,240,128]{2,1,0:T(8,128)(2,1)S(1)} %bitcast.9, bf16[4,1024,128]{2,1,0:T(8,128)(2,1)S(1)} %all_to_all.30.kv_ref), custom_call_target="tpu_custom_call" | custom-call | tf_op jit(solution)/shard_map/attention_first/pallas_call | solution.py:200
  83.5 0.0 all-to-all-done.1.last_ref
  83.5 6.0 %attention_last.1 = (bf16[16,64,128]{2,1,0:T(8,128)(2,1)}, bf16[16,64,128]{2,1,0:T(8,128)(2,1)}, bf16[16,256,128]{2,1,0:T(8,128)(2,1)}) custom-call(s32[1]{0:T(128)} %bitcast.me_ref, bf16[16,240,128]{2,1,0:T(8,128)(2,1)S(1)} %bitcast.10, bf16[4,1024,128]{2,1,0:T(8,128)(2,1)S(1)} %all_to_all.30.kv_ref, bf16[16,32,128]{2,1,0:T(8,128)(2,1)} %all-to-all-done.1.last_ref, ...), custom_call_target="tpu_custom_call" | custom-call | tf_op jit(solution)/shard_map/attention_last/pallas_call | solution.py:210
  89.5 0.0 copy-start.5
  89.5 0.0 copy-start.1
  89.5 4.4 %all-to-all-start.2 = ((bf16[16,256,128]{2,1,0:T(8,128)(2,1)}), bf16[16,256,128]{2,1,0:T(8,128)(2,1)S(1)}, u32[]{:S(2)}, u32[]{:S(2)}) async-start(bf16[16,256,128]{2,1,0:T(8,128)(2,1)} %get-tuple-element.18), calls=%async_computation.2 | async-start | bytes 2097152 | tf_op jit(solution)/shard_map/all_to_all | solution.py:240
  93.9 0.0 copy-done.5
  93.9 2.9 %collective-permute-start = (bf16[16,64,128]{2,1,0:T(8,128)(2,1)S(1)}, bf16[16,64,128]{2,1,0:T(8,128)(2,1)S(1)}, u32[]{:S(2)}, u32[]{:S(2)}) collective-permute-start(bf16[16,64,128]{2,1,0:T(8,128)(2,1)S(1)} %copy-done.5), channel_id=1, source_target_pairs={{0,32},{32,0},{64,96},{96,64},{128,160},{160,128},{192,224},{224,1... | collective-permute-start | bytes 786440 | tf_op jit(solution)/shard_map/ppermute | solution.py:245
  96.8 7.4 %collective-permute-done = bf16[16,64,128]{2,1,0:T(8,128)(2,1)S(1)} collective-permute-done((bf16[16,64,128]{2,1,0:T(8,128)(2,1)S(1)}, bf16[16,64,128]{2,1,0:T(8,128)(2,1)S(1)}, u32[]{:S(2)}, u32[]{:S(2)}) %collective-permute-start) | collective-permute-done | bytes 262176 | tf_op jit(solution)/shard_map/ppermute | solution.py:245
  104.1 0.0 copy-done.1
  104.2 0.1 add_convert_fusion
  104.2 0.0 copy-start
  104.2 3.6 %collective-permute-start.1 = (bf16[16,32,128]{2,1,0:T(8,128)(2,1)S(1)}, bf16[16,32,128]{2,1,0:T(8,128)(2,1)S(1)}, u32[]{:S(2)}, u32[]{:S(2)}) collective-permute-start(bf16[16,32,128]{2,1,0:T(8,128)(2,1)S(1)} %add_convert_fusion), channel_id=1, source_target_pairs={{0,64},{32,96},{64,0},{96,32},{128,192},{160,224},{192,128},{224,1... | collective-permute-start | bytes 393224 | tf_op jit(solution)/shard_map/ppermute | solution.py:245
  107.8 1.5 all-to-all-done.2.arrived_ref
  109.3 0.9 added_up.1
  110.2 5.3 %all-to-all-start.3 = ((bf16[8,256,128]{2,1,0:T(8,128)(2,1)}), bf16[8,256,128]{2,1,0:T(8,128)(2,1)S(1)}, u32[]{:S(2)}, u32[]{:S(2)}) async-start(bf16[8,256,128]{2,1,0:T(8,128)(2,1)} %added_up.1), calls=%async_computation.3 | async-start | bytes 1048576 | tf_op jit(solution)/shard_map/all_to_all | solution.py:240
  115.5 0.1 add_convert_fusion.1
  115.6 0.0 collective-permute-done.1
  115.7 6.6 %collective-permute-start.2 = (bf16[16,16,128]{2,1,0:T(8,128)(2,1)S(1)}, bf16[16,16,128]{2,1,0:T(8,128)(2,1)S(1)}, u32[]{:S(2)}, u32[]{:S(2)}) collective-permute-start(bf16[16,16,128]{2,1,0:T(8,128)(2,1)S(1)} %add_convert_fusion.2), channel_id=1, source_target_pairs={{0,128},{32,160},{64,192},{96,224},{128,0},{160,32},{192,64},{224,... | collective-permute-start | bytes 196616 | tf_op jit(solution)/shard_map/ppermute | solution.py:245
  122.2 1.5 all-to-all-done.3.halves_ref
  123.8 0.0 copy-done
  123.8 1.2 key_products.1
  125.0 0.0 copy-start.3
  125.0 0.0 copy-start.4
  125.0 3.5 %all-to-all-start.4 = ((bf16[4,64,512]{2,1,0:T(8,128)(2,1)}), bf16[4,64,512]{2,1,0:T(8,128)(2,1)S(1)}, u32[]{:S(2)}, u32[]{:S(2)}) async-start(bf16[4,64,512]{2,1,0:T(8,128)(2,1)} %key_products.1), calls=%async_computation.4 | async-start | bytes 524288 | tf_op jit(solution)/shard_map/all_to_all | solution.py:240
  128.6 1.2 collective-permute-done.2.arrived_ref
  129.8 5.4 %all-to-all-done.4.keys_ref = bf16[4,64,512]{2,1,0:T(8,128)(2,1)S(1)} async-done(((bf16[4,64,512]{2,1,0:T(8,128)(2,1)}), bf16[4,64,512]{2,1,0:T(8,128)(2,1)S(1)}, u32[]{:S(2)}, u32[]{:S(2)}) %all-to-all-start.4) | async-done | bytes 262176 | tf_op jit(solution)/shard_map/all_to_all | solution.py:240
  135.2 0.9 joined.1
  136.1 10.3 %all-to-all-start.5 = ((bf16[16,32,128]{2,1,0:T(8,128)(2,1)}), bf16[16,32,128]{2,1,0:T(8,128)(2,1)S(1)}, u32[]{:S(2)}, u32[]{:S(2)}) async-start(bf16[16,32,128]{2,1,0:T(8,128)(2,1)} %joined.1), calls=%async_computation.5 | async-start | bytes 262144 | tf_op jit(solution)/shard_map/all_to_all | solution.py:240
  146.4 0.0 copy-done.3
  146.4 0.0 copy-done.4
  146.4 1.4 fusion
  147.8 11.9 %all-to-all-done.5.blocks_ref = bf16[16,32,128]{2,1,0:T(8,128)(2,1)S(1)} async-done(((bf16[16,32,128]{2,1,0:T(8,128)(2,1)}), bf16[16,32,128]{2,1,0:T(8,128)(2,1)S(1)}, u32[]{:S(2)}, u32[]{:S(2)}) %all-to-all-start.5) | async-done | bytes 131104 | tf_op jit(solution)/shard_map/all_to_all | solution.py:240
  159.8 0.6 split_sums.1
  (3 shorter events, 0.1 us)
Async XLA Ops:
  2.9 35.0 %copy-start.2 = (bf16[240,128]{1,0:T(8,128)(2,1)S(1)}, bf16[240,128]{1,0:T(8,128)(2,1)}, u32[]{:S(2)}) copy-start(bf16[240,128]{1,0:T(8,128)(2,1)} %get-tuple-element.15) | copy-start | bytes 184324
  22.6 60.9 %all-to-all-start.1 = ((bf16[16,32,128]{2,1,0:T(8,128)(2,1)}), bf16[16,32,128]{2,1,0:T(8,128)(2,1)}, u32[]{:S(2)}, u32[]{:S(2)}) async-start(bf16[16,32,128]{2,1,0:T(8,128)(2,1)} %get-tuple-element.17), calls=%async_computation.1 | async-start | bytes 262144 | tf_op jit(solution)/shard_map/all_to_all | solution.py:240
  89.5 4.4 %copy-start.5 = (bf16[16,64,128]{2,1,0:T(8,128)(2,1)S(1)}, bf16[16,64,128]{2,1,0:T(8,128)(2,1)}, u32[]{:S(2)}) copy-start(bf16[16,64,128]{2,1,0:T(8,128)(2,1)} %get-tuple-element.20) | copy-start | bytes 786436
  89.5 14.6 %copy-start.1 = (bf16[16,64,128]{2,1,0:T(8,128)(2,1)S(1)}, bf16[16,64,128]{2,1,0:T(8,128)(2,1)}, u32[]{:S(2)}) copy-start(bf16[16,64,128]{2,1,0:T(8,128)(2,1)} %get-tuple-element.21) | copy-start | bytes 786436
  89.5 19.8 %all-to-all-start.2 = ((bf16[16,256,128]{2,1,0:T(8,128)(2,1)}), bf16[16,256,128]{2,1,0:T(8,128)(2,1)S(1)}, u32[]{:S(2)}, u32[]{:S(2)}) async-start(bf16[16,256,128]{2,1,0:T(8,128)(2,1)} %get-tuple-element.18), calls=%async_computation.2 | async-start | bytes 2097152 | tf_op jit(solution)/shard_map/all_to_all | solution.py:240
  93.9 10.2 %collective-permute-start = (bf16[16,64,128]{2,1,0:T(8,128)(2,1)S(1)}, bf16[16,64,128]{2,1,0:T(8,128)(2,1)S(1)}, u32[]{:S(2)}, u32[]{:S(2)}) collective-permute-start(bf16[16,64,128]{2,1,0:T(8,128)(2,1)S(1)} %copy-done.5), channel_id=1, source_target_pairs={{0,32},{32,0},{64,96},{96,64},{128,160},{160,128},{192,224},{224,1... | collective-permute-start | bytes 786440 | tf_op jit(solution)/shard_map/ppermute | solution.py:245
  104.2 19.5 %copy-start = (bf16[512,512]{1,0:T(8,128)(2,1)S(1)}, bf16[512,512]{1,0:T(8,128)(2,1)}, u32[]{:S(2)}) copy-start(bf16[512,512]{1,0:T(8,128)(2,1)} %source_ref.1) | copy-start | bytes 1572868
  104.2 11.4 %collective-permute-start.1 = (bf16[16,32,128]{2,1,0:T(8,128)(2,1)S(1)}, bf16[16,32,128]{2,1,0:T(8,128)(2,1)S(1)}, u32[]{:S(2)}, u32[]{:S(2)}) collective-permute-start(bf16[16,32,128]{2,1,0:T(8,128)(2,1)S(1)} %add_convert_fusion), channel_id=1, source_target_pairs={{0,64},{32,96},{64,0},{96,32},{128,192},{160,224},{192,128},{224,1... | collective-permute-start | bytes 393224 | tf_op jit(solution)/shard_map/ppermute | solution.py:245
  110.2 13.6 %all-to-all-start.3 = ((bf16[8,256,128]{2,1,0:T(8,128)(2,1)}), bf16[8,256,128]{2,1,0:T(8,128)(2,1)S(1)}, u32[]{:S(2)}, u32[]{:S(2)}) async-start(bf16[8,256,128]{2,1,0:T(8,128)(2,1)} %added_up.1), calls=%async_computation.3 | async-start | bytes 1048576 | tf_op jit(solution)/shard_map/all_to_all | solution.py:240
  115.7 14.1 %collective-permute-start.2 = (bf16[16,16,128]{2,1,0:T(8,128)(2,1)S(1)}, bf16[16,16,128]{2,1,0:T(8,128)(2,1)S(1)}, u32[]{:S(2)}, u32[]{:S(2)}) collective-permute-start(bf16[16,16,128]{2,1,0:T(8,128)(2,1)S(1)} %add_convert_fusion.2), channel_id=1, source_target_pairs={{0,128},{32,160},{64,192},{96,224},{128,0},{160,32},{192,64},{224,... | collective-permute-start | bytes 196616 | tf_op jit(solution)/shard_map/ppermute | solution.py:245
  125.0 21.4 %copy-start.3 = (bf16[512,256]{1,0:T(8,128)(2,1)S(1)}, bf16[512,256]{1,0:T(8,128)(2,1)}, u32[]{:S(2)}) copy-start(bf16[512,256]{1,0:T(8,128)(2,1)} %param.17) | copy-start | bytes 786436
  125.0 21.4 %copy-start.4 = (bf16[512,256]{1,0:T(8,128)(2,1)S(1)}, bf16[512,256]{1,0:T(8,128)(2,1)}, u32[]{:S(2)}) copy-start(bf16[512,256]{1,0:T(8,128)(2,1)} %param.16) | copy-start | bytes 786436
  125.0 10.2 %all-to-all-start.4 = ((bf16[4,64,512]{2,1,0:T(8,128)(2,1)}), bf16[4,64,512]{2,1,0:T(8,128)(2,1)S(1)}, u32[]{:S(2)}, u32[]{:S(2)}) async-start(bf16[4,64,512]{2,1,0:T(8,128)(2,1)} %key_products.1), calls=%async_computation.4 | async-start | bytes 524288 | tf_op jit(solution)/shard_map/all_to_all | solution.py:240
  136.1 23.7 %all-to-all-start.5 = ((bf16[16,32,128]{2,1,0:T(8,128)(2,1)}), bf16[16,32,128]{2,1,0:T(8,128)(2,1)S(1)}, u32[]{:S(2)}, u32[]{:S(2)}) async-start(bf16[16,32,128]{2,1,0:T(8,128)(2,1)} %joined.1), calls=%async_computation.5 | async-start | bytes 262144 | tf_op jit(solution)/shard_map/all_to_all | solution.py:240

commit v9 on v8

--- a/solution.py
+++ b/solution.py
@@ -99,7 +99,12 @@
     team = y_count * SPLIT[3] * SPLIT[4]
     piece = sources // team
 
-    def prepare(main_ref, kv_ref, last_ref, k_wide, v_wide, k_turned, q_turned, do_turned, q_rows, do_rows):
+    turned_at = 2 * sources + z_count * FIRST
+    queries_at = turned_at + sources
+    stats_at = queries_at + z_count * (rows - FIRST)
+    handed_rows = stats_at + z_count * (rows - FIRST)
+
+    def prepare(main_ref, kv_ref, last_ref, handed, k_wide, v_wide, k_turned, q_turned, do_turned, q_rows, do_rows):
         lane = lax.broadcasted_iota(jnp.int32, (src, dim), 1)
         lse_lanes = jnp.where(lane < 3, -1.0, 0.0).astype(BF16)
         delta_lanes = jnp.where((lane >= 3) & (lane < 6), -1.0, 0.0).astype(BF16)
@@ -110,14 +115,29 @@
             k_wide[at, dim:] = lse_lanes
             v_wide[at, :dim] = kv_ref[y, src:, :]
             v_wide[at, dim:] = delta_lanes
-            k_turned[:, at] = k.T
+            if last_ref is None:
+                k_turned[:, at] = k.T
+        if last_ref is None:
+            for b in range(0, sources, dim):
+                handed[turned_at + b : turned_at + b + dim, :] = k_turned[:, b : b + dim]
+        else:
+            for b in range(0, sources, dim):
+                k_turned[:, b : b + dim] = handed[turned_at + b : turned_at + b + dim, :]
+            q_rows[:, :dim] = handed[queries_at:stats_at, :]
+            q_rows[:, dim:] = handed[stats_at:handed_rows, :]
         blank = jnp.zeros((dim - STAT_ROWS, dim), BF16)
         for z in range(z_count):
             at = slice(z * each, (z + 1) * each)
-            q_rows[at, :dim] = main_ref[z, low:high, :]
-            stats = jnp.concatenate([main_ref[z, rows + FIRST :, :], blank], axis=0)
-            q_rows[at, dim:] = stats.T[low:high, :]
-            do_rows[at, :] = main_ref[z, rows : rows + FIRST, :] if last_ref is None else last_ref[z]
+            if last_ref is not None:
+                do_rows[at, :] = last_ref[z]
+                continue
+            stats = jnp.concatenate([main_ref[z, rows + FIRST :, :], blank], axis=0).T
+            q_rows[at, :dim] = main_ref[z, :FIRST, :]
+            q_rows[at, dim:] = stats[:FIRST, :]
+            do_rows[at, :] = main_ref[z, rows : rows + FIRST, :]
+            other = slice(z * (rows - FIRST), (z + 1) * (rows - FIRST))
+            handed[queries_at + other.start : queries_at + other.stop, :] = main_ref[z, FIRST:rows, :]
+            handed[stats_at + other.start : stats_at + other.stop, :] = stats[FIRST:, :]
         for b in range(0, targets, dim):
             at = slice(b, b + dim)
             q_turned[:dim, at] = q_rows[at, :dim].T
@@ -147,7 +167,7 @@
 
     def first_kernel(main_ref, kv_ref, out_ref, *scratch):
         dk_acc, dv_acc, dq_acc = scratch[-3:]
-        prepare(main_ref, kv_ref, None, *scratch[:-3])
+        prepare(main_ref, kv_ref, None, out_ref, *scratch[:-3])
         work(*scratch)
         out_ref[:sources, :] = (dk_acc[...] * scale).astype(BF16)
         out_ref[sources : 2 * sources, :] = dv_acc[...].astype(BF16)
@@ -156,10 +176,10 @@
             out_ref[2 * sources + b : 2 * sources + b + dim, :] = turned
 
     def last_kernel(
-        me_ref, main_ref, kv_ref, last_ref, before_ref, send_ref, keep_ref, dkv_ref, *scratch
+        me_ref, kv_ref, last_ref, before_ref, send_ref, keep_ref, dkv_ref, *scratch
     ):
         dk_acc, dv_acc, dq_acc, dq_rows = scratch[-4:]
-        prepare(main_ref, kv_ref, last_ref, *scratch[:-4])
+        prepare(None, kv_ref, last_ref, before_ref, *scratch[:-4])
         work(*scratch[:-1])
         for i in range(team):
             at = slice(i * piece, (i + 1) * piece)
@@ -201,7 +221,7 @@
             first_kernel,
             in_specs=[in_vmem()] * 2,
             out_specs=in_vmem(),
-            out_shape=jax.ShapeDtypeStruct((2 * sources + targets, dim), BF16),
+            out_shape=jax.ShapeDtypeStruct((handed_rows, dim), BF16),
             scratch_shapes=scratch,
             compiler_params=pltpu.CompilerParams(vmem_limit_bytes=FIRST_VMEM_LIMIT),
             name="attention_first",
@@ -209,13 +229,13 @@
     half = pltpu.MemorySpace.HBM((z_count, rows // 2, dim), BF16)
     return pl.pallas_call(
         last_kernel,
-        in_specs=[pl.BlockSpec(memory_space=pltpu.SMEM)] + [in_vmem()] * 4,
+        in_specs=[pl.BlockSpec(memory_space=pltpu.SMEM)] + [in_vmem()] * 3,
         out_specs=[in_vmem()] * 3,
         out_shape=[half, half, dkv],
         scratch_shapes=scratch + [pltpu.VMEM((z_count, each, dim), BF16)],
         compiler_params=pltpu.CompilerParams(vmem_limit_bytes=LAST_VMEM_LIMIT),
         name="attention_last",
-    )(me, main, keyvals, last, before)
+    )(me, keyvals, last, before)
 
 
 def added_up(arrived, copies):

time: 162 us -> 161 us (level)
  no operation moved by 1% of the time
where the time goes in v9:
time: 161 us; the launch traced here: 159 us
  blocking collectives  56.3 us (35%)
  starting transfers between devices  52.2 us (32%)
  waiting for transfers between devices  28.3 us (18%)
  Pallas kernels  19.9 us (12%)
    all_to_all x5, starting transfers between devices, exchanged(): return lax.all_to_all(value, axes, 0, 0, tiled=True)  38.7 us
    all_gather x1, blocking collectives, shards(): main = lax.all_gather(main, 'z', axis=0, tiled=False)  36.6 us
    all_to_all x1, blocking collectives, exchanged(): return lax.all_to_all(value, axes, 0, 0, tiled=True)  19.7 us
    all_to_all x5, waiting for transfers between devices, exchanged(): return lax.all_to_all(value, axes, 0, 0, tiled=True)  19.4 us
    ppermute x3, starting transfers between devices, swapped(): return lax.ppermute(value, axis, pairs)  13.5 us
    pallas_call x1, Pallas kernels, attention_backward(): pl.pallas_call(first_kernel, in_specs=[in_vmem()] * 2, out_specs=in_vmem(...  9.07 us
    ppermute x3, waiting for transfers between devices, swapped(): return lax.ppermute(value, axis, pairs)  8.91 us
    pallas_call x1, Pallas kernels, attention_backward(): pl.pallas_call(last_kernel, in_specs=[pl.BlockSpec(memory_space=pltpu.SME...  4.95 us
  transfers between devices with their start and end apart: 8, of which 6 were waited for; matrix products, arithmetic and copies ran while one was open for 1% of the time, Pallas kernels for 7%

profile of v9, /device:TPU:6, one launch (start us, length us, event | category | flops | bytes accessed | tf_op | source)
XLA Modules:
  0.0 159.3 jit_solution(18338620113253884211)
XLA Ops:
  0.6 2.2 %pack_rows.1 = (bf16[240,128]{1,0:T(8,128)(2,1)}, bf16[16,32,128]{2,1,0:T(8,128)(2,1)}, bf16[4,1024,128]{2,1,0:T(8,128)(2,1)}) custom-call(s32[1]{0:T(128)} %bitcast.1.head_ref, bf16[128,128]{1,0:T(8,128)(2,1)} %q_ref.1, bf16[128,128]{1,0:T(8,128)(2,1)} %o_ref.1, bf16[128,128]{1,0:T(8,128)(2,1)} %do_ref.1, f32[1,128]{1,0:T(1,128)} %bitcast.15, ...), custom_call_target="tpu_custom_call" | custom-call | tf_op jit(solution)/shard_map/pack_rows/pallas_call | solution.py:64
  2.9 0.0 copy-start.2
  2.9 19.7 %all_to_all.30.kv_ref = bf16[4,1024,128]{2,1,0:T(8,128)(2,1)S(1)} all-to-all(bf16[4,1024,128]{2,1,0:T(8,128)(2,1)} %get-tuple-element.15), channel_id=1, replica_groups=mesh['z'=16,'y'=4,'g'=2,'h'=2,'c'=2] {'y'}, dimensions={0} | all-to-all | bytes 2097152 | tf_op jit(solution)/shard_map/all_to_all | solution.py:260
  22.6 15.2 %all-to-all-start.1 = ((bf16[16,32,128]{2,1,0:T(8,128)(2,1)}), bf16[16,32,128]{2,1,0:T(8,128)(2,1)S(1)}, u32[]{:S(2)}, u32[]{:S(2)}) async-start(bf16[16,32,128]{2,1,0:T(8,128)(2,1)} %get-tuple-element.16), calls=%async_computation.1 | async-start | bytes 262144 | tf_op jit(solution)/shard_map/all_to_all | solution.py:260
  37.8 0.0 copy-done.2
  37.8 36.6 %all-gather = bf16[3840,128]{1,0:T(8,128)(2,1)S(1)} all-gather(bf16[240,128]{1,0:T(8,128)(2,1)S(1)} %copy-done.2), channel_id=2, replica_groups=mesh['z'=16,'y'=4,'g'=2,'h'=2,'c'=2] {'z'}, dimensions={0}, use_global_device_ids=true | all-gather | bytes 1044480 | tf_op jit(solution)/shard_map/all_gather | solution.py:386
  74.4 9.1 %attention_first.1.before_ref = bf16[8704,128]{1,0:T(8,128)(2,1)S(1)} custom-call(bf16[16,240,128]{2,1,0:T(8,128)(2,1)S(1)} %bitcast.10, bf16[4,1024,128]{2,1,0:T(8,128)(2,1)S(1)} %all_to_all.30.kv_ref), custom_call_target="tpu_custom_call" | custom-call | tf_op jit(solution)/shard_map/attention_first/pallas_call | solution.py:220
  83.5 0.0 all-to-all-done.1.last_ref
  83.5 5.0 %attention_last.1 = (bf16[16,64,128]{2,1,0:T(8,128)(2,1)}, bf16[16,64,128]{2,1,0:T(8,128)(2,1)}, bf16[16,256,128]{2,1,0:T(8,128)(2,1)}) custom-call(s32[1]{0:T(128)} %bitcast.me_ref, bf16[4,1024,128]{2,1,0:T(8,128)(2,1)S(1)} %all_to_all.30.kv_ref, bf16[16,32,128]{2,1,0:T(8,128)(2,1)S(1)} %all-to-all-done.1.last_ref, ...), custom_call_target="tpu_custom_call" | custom-call | tf_op jit(solution)/shard_map/attention_last/pallas_call | solution.py:230
  88.5 0.0 copy-start.1
  88.5 4.4 %all-to-all-start.2 = ((bf16[16,256,128]{2,1,0:T(8,128)(2,1)}), bf16[16,256,128]{2,1,0:T(8,128)(2,1)S(1)}, u32[]{:S(2)}, u32[]{:S(2)}) async-start(bf16[16,256,128]{2,1,0:T(8,128)(2,1)} %get-tuple-element.18), calls=%async_computation.2 | async-start | bytes 2097152 | tf_op jit(solution)/shard_map/all_to_all | solution.py:260
  92.9 0.0 copy-start
  92.9 3.1 %collective-permute-start = (bf16[16,64,128]{2,1,0:T(8,128)(2,1)}, bf16[16,64,128]{2,1,0:T(8,128)(2,1)S(1)}, u32[]{:S(2)}, u32[]{:S(2)}) collective-permute-start(bf16[16,64,128]{2,1,0:T(8,128)(2,1)} %get-tuple-element.20), channel_id=1, source_target_pairs={{0,32},{32,0},{64,96},{96,64},{128,160},{160,128},{192,224},{224,1... | collective-permute-start | bytes 786440 | tf_op jit(solution)/shard_map/ppermute | solution.py:265
  96.0 7.4 %collective-permute-done = bf16[16,64,128]{2,1,0:T(8,128)(2,1)S(1)} collective-permute-done((bf16[16,64,128]{2,1,0:T(8,128)(2,1)}, bf16[16,64,128]{2,1,0:T(8,128)(2,1)S(1)}, u32[]{:S(2)}, u32[]{:S(2)}) %collective-permute-start) | collective-permute-done | bytes 262176 | tf_op jit(solution)/shard_map/ppermute | solution.py:265
  103.5 0.0 copy-done.1
  103.5 0.1 add_convert_fusion
  103.5 3.6 %collective-permute-start.1 = (bf16[16,32,128]{2,1,0:T(8,128)(2,1)S(1)}, bf16[16,32,128]{2,1,0:T(8,128)(2,1)S(1)}, u32[]{:S(2)}, u32[]{:S(2)}) collective-permute-start(bf16[16,32,128]{2,1,0:T(8,128)(2,1)S(1)} %add_convert_fusion), channel_id=1, source_target_pairs={{0,64},{32,96},{64,0},{96,32},{128,192},{160,224},{192,128},{224,1... | collective-permute-start | bytes 393224 | tf_op jit(solution)/shard_map/ppermute | solution.py:265
  107.1 1.1 all-to-all-done.2.arrived_ref
  108.2 0.9 added_up.1
  109.2 5.3 %all-to-all-start.3 = ((bf16[8,256,128]{2,1,0:T(8,128)(2,1)}), bf16[8,256,128]{2,1,0:T(8,128)(2,1)S(1)}, u32[]{:S(2)}, u32[]{:S(2)}) async-start(bf16[8,256,128]{2,1,0:T(8,128)(2,1)} %added_up.1), calls=%async_computation.3 | async-start | bytes 1048576 | tf_op jit(solution)/shard_map/all_to_all | solution.py:260
  114.5 0.1 add_convert_fusion.1
  114.6 0.0 copy-start.3
  114.6 0.0 copy-start.4
  114.6 0.0 collective-permute-done.1
  114.6 6.8 %collective-permute-start.2 = (bf16[16,16,128]{2,1,0:T(8,128)(2,1)S(1)}, bf16[16,16,128]{2,1,0:T(8,128)(2,1)S(1)}, u32[]{:S(2)}, u32[]{:S(2)}) collective-permute-start(bf16[16,16,128]{2,1,0:T(8,128)(2,1)S(1)} %add_convert_fusion.2), channel_id=1, source_target_pairs={{0,128},{32,160},{64,192},{96,224},{128,0},{160,32},{192,64},{224,... | collective-permute-start | bytes 196616 | tf_op jit(solution)/shard_map/ppermute | solution.py:265
  121.5 1.3 all-to-all-done.3.halves_ref
  122.7 0.0 copy-done
  122.7 1.2 key_products.1
  124.0 3.4 %all-to-all-start.4 = ((bf16[4,64,512]{2,1,0:T(8,128)(2,1)}), bf16[4,64,512]{2,1,0:T(8,128)(2,1)S(1)}, u32[]{:S(2)}, u32[]{:S(2)}) async-start(bf16[4,64,512]{2,1,0:T(8,128)(2,1)} %key_products.1), calls=%async_computation.4 | async-start | bytes 524288 | tf_op jit(solution)/shard_map/all_to_all | solution.py:260
  127.4 1.5 collective-permute-done.2.arrived_ref
  128.9 5.1 %all-to-all-done.4.keys_ref = bf16[4,64,512]{2,1,0:T(8,128)(2,1)S(1)} async-done(((bf16[4,64,512]{2,1,0:T(8,128)(2,1)}), bf16[4,64,512]{2,1,0:T(8,128)(2,1)S(1)}, u32[]{:S(2)}, u32[]{:S(2)}) %all-to-all-start.4) | async-done | bytes 262176 | tf_op jit(solution)/shard_map/all_to_all | solution.py:260
  134.0 0.9 joined.1
  134.9 10.4 %all-to-all-start.5 = ((bf16[16,32,128]{2,1,0:T(8,128)(2,1)}), bf16[16,32,128]{2,1,0:T(8,128)(2,1)S(1)}, u32[]{:S(2)}, u32[]{:S(2)}) async-start(bf16[16,32,128]{2,1,0:T(8,128)(2,1)} %joined.1), calls=%async_computation.5 | async-start | bytes 262144 | tf_op jit(solution)/shard_map/all_to_all | solution.py:260
  145.3 0.0 copy-done.3
  145.3 0.0 copy-done.4
  145.4 1.4 fusion
  146.8 11.9 %all-to-all-done.5.blocks_ref = bf16[16,32,128]{2,1,0:T(8,128)(2,1)S(1)} async-done(((bf16[16,32,128]{2,1,0:T(8,128)(2,1)}), bf16[16,32,128]{2,1,0:T(8,128)(2,1)S(1)}, u32[]{:S(2)}, u32[]{:S(2)}) %all-to-all-start.5) | async-done | bytes 131104 | tf_op jit(solution)/shard_map/all_to_all | solution.py:260
  158.7 0.6 split_sums.1
  (3 shorter events, 0.1 us)
Async XLA Ops:
  2.9 34.9 %copy-start.2 = (bf16[240,128]{1,0:T(8,128)(2,1)S(1)}, bf16[240,128]{1,0:T(8,128)(2,1)}, u32[]{:S(2)}) copy-start(bf16[240,128]{1,0:T(8,128)(2,1)} %get-tuple-element.17) | copy-start | bytes 184324
  22.6 60.9 %all-to-all-start.1 = ((bf16[16,32,128]{2,1,0:T(8,128)(2,1)}), bf16[16,32,128]{2,1,0:T(8,128)(2,1)S(1)}, u32[]{:S(2)}, u32[]{:S(2)}) async-start(bf16[16,32,128]{2,1,0:T(8,128)(2,1)} %get-tuple-element.16), calls=%async_computation.1 | async-start | bytes 262144 | tf_op jit(solution)/shard_map/all_to_all | solution.py:260
  88.5 15.0 %copy-start.1 = (bf16[16,64,128]{2,1,0:T(8,128)(2,1)S(1)}, bf16[16,64,128]{2,1,0:T(8,128)(2,1)}, u32[]{:S(2)}) copy-start(bf16[16,64,128]{2,1,0:T(8,128)(2,1)} %get-tuple-element.21) | copy-start | bytes 786436
  88.5 19.8 %all-to-all-start.2 = ((bf16[16,256,128]{2,1,0:T(8,128)(2,1)}), bf16[16,256,128]{2,1,0:T(8,128)(2,1)S(1)}, u32[]{:S(2)}, u32[]{:S(2)}) async-start(bf16[16,256,128]{2,1,0:T(8,128)(2,1)} %get-tuple-element.18), calls=%async_computation.2 | async-start | bytes 2097152 | tf_op jit(solution)/shard_map/all_to_all | solution.py:260
  92.9 29.9 %copy-start = (bf16[512,512]{1,0:T(8,128)(2,1)S(1)}, bf16[512,512]{1,0:T(8,128)(2,1)}, u32[]{:S(2)}) copy-start(bf16[512,512]{1,0:T(8,128)(2,1)} %source_ref.1) | copy-start | bytes 1572868
  92.9 10.6 %collective-permute-start = (bf16[16,64,128]{2,1,0:T(8,128)(2,1)}, bf16[16,64,128]{2,1,0:T(8,128)(2,1)S(1)}, u32[]{:S(2)}, u32[]{:S(2)}) collective-permute-start(bf16[16,64,128]{2,1,0:T(8,128)(2,1)} %get-tuple-element.20), channel_id=1, source_target_pairs={{0,32},{32,0},{64,96},{96,64},{128,160},{160,128},{192,224},{224,1... | collective-permute-start | bytes 786440 | tf_op jit(solution)/shard_map/ppermute | solution.py:265
  103.5 11.0 %collective-permute-start.1 = (bf16[16,32,128]{2,1,0:T(8,128)(2,1)S(1)}, bf16[16,32,128]{2,1,0:T(8,128)(2,1)S(1)}, u32[]{:S(2)}, u32[]{:S(2)}) collective-permute-start(bf16[16,32,128]{2,1,0:T(8,128)(2,1)S(1)} %add_convert_fusion), channel_id=1, source_target_pairs={{0,64},{32,96},{64,0},{96,32},{128,192},{160,224},{192,128},{224,1... | collective-permute-start | bytes 393224 | tf_op jit(solution)/shard_map/ppermute | solution.py:265
  109.2 13.6 %all-to-all-start.3 = ((bf16[8,256,128]{2,1,0:T(8,128)(2,1)}), bf16[8,256,128]{2,1,0:T(8,128)(2,1)S(1)}, u32[]{:S(2)}, u32[]{:S(2)}) async-start(bf16[8,256,128]{2,1,0:T(8,128)(2,1)} %added_up.1), calls=%async_computation.3 | async-start | bytes 1048576 | tf_op jit(solution)/shard_map/all_to_all | solution.py:260
  114.6 30.8 %copy-start.3 = (bf16[512,256]{1,0:T(8,128)(2,1)S(1)}, bf16[512,256]{1,0:T(8,128)(2,1)}, u32[]{:S(2)}) copy-start(bf16[512,256]{1,0:T(8,128)(2,1)} %param.17) | copy-start | bytes 786436
  114.6 30.8 %copy-start.4 = (bf16[512,256]{1,0:T(8,128)(2,1)S(1)}, bf16[512,256]{1,0:T(8,128)(2,1)}, u32[]{:S(2)}) copy-start(bf16[512,256]{1,0:T(8,128)(2,1)} %param.16) | copy-start | bytes 786436
  114.6 14.3 %collective-permute-start.2 = (bf16[16,16,128]{2,1,0:T(8,128)(2,1)S(1)}, bf16[16,16,128]{2,1,0:T(8,128)(2,1)S(1)}, u32[]{:S(2)}, u32[]{:S(2)}) collective-permute-start(bf16[16,16,128]{2,1,0:T(8,128)(2,1)S(1)} %add_convert_fusion.2), channel_id=1, source_target_pairs={{0,128},{32,160},{64,192},{96,224},{128,0},{160,32},{192,64},{224,... | collective-permute-start | bytes 196616 | tf_op jit(solution)/shard_map/ppermute | solution.py:265
  124.0 10.1 %all-to-all-start.4 = ((bf16[4,64,512]{2,1,0:T(8,128)(2,1)}), bf16[4,64,512]{2,1,0:T(8,128)(2,1)S(1)}, u32[]{:S(2)}, u32[]{:S(2)}) async-start(bf16[4,64,512]{2,1,0:T(8,128)(2,1)} %key_products.1), calls=%async_computation.4 | async-start | bytes 524288 | tf_op jit(solution)/shard_map/all_to_all | solution.py:260
  134.9 23.8 %all-to-all-start.5 = ((bf16[16,32,128]{2,1,0:T(8,128)(2,1)}), bf16[16,32,128]{2,1,0:T(8,128)(2,1)S(1)}, u32[]{:S(2)}, u32[]{:S(2)}) async-start(bf16[16,32,128]{2,1,0:T(8,128)(2,1)} %joined.1), calls=%async_computation.5 | async-start | bytes 262144 | tf_op jit(solution)/shard_map/all_to_all | solution.py:260
